TPU v7x, 512 devices: a whole 4x4x16 slice. The times are simulated.
512 devices in a mesh: ep: 128 (over z, x, core), tp: 4 (over y).
Axes of the slice: x: 4, y: 4, z: 16, core: 2. Of those that a mesh axis runs over, the one named last changes fastest.
Arguments:
- tokens: bfloat16 [2048, 1024], P('ep'), may hold values from -6 to 6
- state: float32 [2048, 16, 64, 64], P('ep', 'tp'), may hold values from -6 to 6
- w_recep: bfloat16 [1024, 1024], P(None, 'tp'), may hold values from -0.1875 to 0.1875
- w_key: bfloat16 [1024, 1024], P(None, 'tp'), may hold values from -0.1875 to 0.1875
- w_value: bfloat16 [1024, 1024], P(None, 'tp'), may hold values from -0.1875 to 0.1875
- w_out: bfloat16 [1024, 1024], P('tp'), may hold values from -0.1875 to 0.1875
- decay_base: float32 [1024], P('tp'), may hold values from -5 to 1
- decay_down: bfloat16 [1024, 64], replicated, may hold values from -0.1875 to 0.1875
- decay_up: bfloat16 [64, 1024], P(None, 'tp'), may hold values from -1 to 1
- rate_base: float32 [1024], P('tp'), may hold values from -4 to 4
- rate_down: bfloat16 [1024, 64], replicated, may hold values from -0.1875 to 0.1875
- rate_up: bfloat16 [64, 1024], P(None, 'tp'), may hold values from -1 to 1
- head_gain: float32 [1024], P('tp'), may hold values from 0.1 to 1.9
- first_gain: float32 [1024], replicated, may hold values from 0.2 to 4.8
- expert_gate: bfloat16 [128, 1024, 1408], P('ep', None, 'tp'), may hold values from -0.1875 to 0.1875
- expert_up: bfloat16 [128, 1024, 1408], P('ep', None, 'tp'), may hold values from -0.1875 to 0.1875
- expert_down: bfloat16 [128, 1408, 1024], P('ep', 'tp'), may hold values from -0.078125 to 0.078125
- dense_gate: bfloat16 [2816, 1024], P('ep'), may hold values from -0.1875 to 0.1875
- dense_up: bfloat16 [2816, 1024], P('ep'), may hold values from -0.1875 to 0.1875
- dense_down: bfloat16 [2816, 1024], P('ep', 'tp'), may hold values from -0.21875 to 0.21875
- branch_gate: bfloat16 [1024], replicated, may hold values from -0.1875 to 0.1875
- second_gain: float32 [1024], P('tp'), may hold values from 0.1 to 1.9
- routes: int32 [2048, 2], P('ep'), may hold values from 0 to 31, all different within a row; in each aligned block of 16 rows (0 to 15, 16 to 31, ...) at most 2 rows name the same one
- route_weights: float32 [2048, 2], P('ep'), may hold values from 0.2 to 1
Outputs:
- layer_output: bfloat16 [2048, 1024], P('ep', 'tp')
Inputs may be any that keep to these rules, and one draw needn't show every extreme that they name: `routes`: each row names 2 different experts. In each aligned block of 16 rows no expert is named by more than 2 rows, a bound that some block reaches.
All inputs are finite; a program needn't handle non-finite values.
Results may differ from a plain program's by a relative error of at most 0.018.
Values may be sent and summed in bfloat16 or wider, within the bound.
No kernel may reach another device: no remote copies, remote signals or barrier semaphores. Data moves between devices by JAX's collectives and lax.ppermute only.
A program may use at most 64 MiB of HBM per device.

v0:
```python
import jax
import jax.numpy as jnp
from jax import lax
from jax.sharding import Mesh
from jax.sharding import PartitionSpec as P

SPLIT = 4
EP = ("ep_0", "ep_1", "ep_2")


residual_scale = 1.4142135623730951
norm_epsilon = 1e-05
head_epsilon = 0.00064
key_epsilon = 1e-06


def sent_to_all(value, axis):
    copies = jnp.broadcast_to(value, (lax.axis_size(axis), *value.shape))
    return lax.all_to_all(copies, axis, split_axis=0, concat_axis=0, tiled=True)


def of_everyone(value, axis):
    return sent_to_all(value, axis).sum(axis=0)


def joined_along(parts, dim):
    parts = jnp.moveaxis(parts, 0, dim)
    shape = parts.shape
    return parts.reshape(*shape[:dim], shape[dim] * shape[dim + 1], *shape[dim + 2 :])


def collect(value, axis, dim):
    parts = sent_to_all(value, axis)
    return joined_along(parts, dim)


def cut_along(value, dim, length):
    shape = value.shape
    parts = value.reshape(*shape[:dim], length, shape[dim] // length, *shape[dim + 1 :])
    return jnp.moveaxis(parts, dim, 0)


def sent_and_summed(value, axis, dim):
    parts = cut_along(value, dim, lax.axis_size(axis))
    arrived = lax.all_to_all(parts, axis, split_axis=0, concat_axis=0, tiled=True)
    return arrived.astype(jnp.float32).sum(axis=0)


def gather_axes(value, axes, dim):
    far, near = axes
    parts = sent_to_all(sent_to_all(value, far), near)
    return joined_along(parts.swapaxes(0, 1).reshape(-1, *value.shape), dim)


def of_everyone_2(value, axis):
    everything = sent_to_all(value, axis)
    return jnp.sum(everything.astype(jnp.float32), axis=0)


def sum_in_two_steps(value, axes, dim):
    far, near = axes
    parts = cut_along(value, dim, lax.axis_size(far))
    nearer = sent_and_summed(parts, near, dim + 1)
    arrived = lax.all_to_all(
        nearer.astype(jnp.bfloat16), far, split_axis=0, concat_axis=0, tiled=True
    )
    return arrived.astype(jnp.float32).sum(axis=0)


def in_one(arrays, axis):
    vector, at, done = (jnp.concatenate([a.reshape(-1) for a in arrays]), 0, [])
    running = of_everyone(vector, axis)
    for a in arrays:
        done.append(running[at : at + a.size].reshape(a.shape))
        at += a.size
    return tuple(done)


def time_mixer(
    tokens,
    state,
    w_recep,
    w_key,
    w_value,
    w_out,
    decay_base,
    decay_down,
    decay_up,
    rate_base,
    rate_down,
    rate_up,
    head_gain,
):
    row_count = tokens.shape[0]
    head_count = state.shape[1]
    head_size = state.shape[3]
    recep = jnp.dot(tokens, w_recep, preferred_element_type=jnp.float32).reshape(
        row_count, head_count, head_size
    )
    key_vecs = jnp.dot(tokens, w_key, preferred_element_type=jnp.float32).reshape(
        row_count, head_count, head_size
    )
    value_vecs = jnp.dot(tokens, w_value, preferred_element_type=jnp.float32).reshape(
        row_count, head_count, head_size
    )
    decay_low = jnp.tanh(jnp.dot(tokens, decay_down, preferred_element_type=jnp.float32)).astype(
        jnp.bfloat16
    )
    decay_pre = decay_base + jnp.dot(decay_low, decay_up, preferred_element_type=jnp.float32)
    log_rate = -jax.nn.softplus(-decay_pre) - 0.5
    decay = jnp.exp(-jnp.exp(log_rate)).reshape(row_count, head_count, head_size)
    rate_low = jnp.dot(tokens, rate_down, preferred_element_type=jnp.float32).astype(jnp.bfloat16)
    in_rate = jax.nn.sigmoid(
        rate_base + jnp.dot(rate_low, rate_up, preferred_element_type=jnp.float32)
    ).reshape(row_count, head_count, head_size)
    unit_keys = key_vecs * lax.rsqrt(jnp.sum(key_vecs * key_vecs, -1, keepdims=True) + key_epsilon)
    removed = jnp.einsum("bhij,bhj->bhi", state, -unit_keys)
    updated = (
        state * decay[:, :, None, :]
        + removed[..., None] * (unit_keys * in_rate)[:, :, None, :]
        + value_vecs[..., None] * key_vecs[:, :, None, :]
    )
    read_out = jnp.einsum("bhij,bhj->bhi", updated, recep)
    centre = jnp.mean(read_out, -1, keepdims=True)
    spread = jnp.mean(jnp.square(read_out - centre), -1, keepdims=True)
    normed = ((read_out - centre) * lax.rsqrt(spread + head_epsilon)).reshape(
        row_count, head_count * head_size
    ) * head_gain
    return jnp.dot(normed.astype(jnp.bfloat16), w_out, preferred_element_type=jnp.float32)


def first_norm(values, gain):
    centre = jnp.mean(values, -1, keepdims=True)
    spread = jnp.mean(jnp.square(values - centre), -1, keepdims=True)
    return ((values - centre) * lax.rsqrt(spread + norm_epsilon) * gain).astype(jnp.bfloat16)


def route_tables(routes, route_weights, experts, capacity):
    expert_hits = (
        routes[:, :, None] == jnp.arange(experts, dtype=jnp.int32)[None, None, :]
    ).astype(jnp.int32)
    row_hits = jnp.sum(expert_hits, 1, dtype=jnp.int32)
    earlier = jnp.cumsum(row_hits, 0, dtype=jnp.int32) - row_hits
    slot_index = jnp.sum(earlier[:, None, :] * expert_hits, 2, dtype=jnp.int32)
    target = routes * capacity + slot_index
    places = jnp.arange(experts * capacity, dtype=jnp.int32)
    slot_match = target[:, :, None] == places[None, None, :]
    dispatch_tokens = jnp.any(slot_match, 1).astype(jnp.bfloat16)
    combine_experts = jnp.sum(jnp.where(slot_match, route_weights[:, :, None], 0.0), 1)
    return (dispatch_tokens, combine_experts)


def shards(
    tokens,
    state,
    w_recep,
    w_key,
    w_value,
    w_out,
    decay_base,
    decay_down,
    decay_up,
    rate_base,
    rate_down,
    rate_up,
    head_gain,
    first_gain,
    expert_gate,
    expert_up,
    expert_down,
    dense_gate,
    dense_up,
    dense_down,
    branch_gate,
    second_gain,
    routes,
    route_weights,
):
    row_count = tokens.shape[0]
    model_width = tokens.shape[1]
    quarter = w_recep.shape[1]
    tp_index = lax.axis_index("tp")
    partial_mix = time_mixer(
        tokens,
        state,
        w_recep,
        w_key,
        w_value,
        w_out,
        decay_base,
        decay_down,
        decay_up,
        rate_base,
        rate_down,
        rate_up,
        head_gain,
    )
    mixed = of_everyone(partial_mix, "tp")
    x_mid = first_norm(residual_scale * tokens.astype(jnp.float32) + mixed, first_gain)
    own_columns = lax.dynamic_slice_in_dim(x_mid, tp_index * quarter, quarter, 1)
    experts = lax.axis_size(EP) // SPLIT
    capacity = min(row_count, max(2, 2 * row_count * routes.shape[1] // experts))
    dispatch_tokens, combine_experts = route_tables(routes, route_weights, experts, capacity)
    packed_rows = lax.dot_general(
        dispatch_tokens, own_columns, (((0,), (0,)), ((), ())), preferred_element_type=jnp.float32
    ).astype(jnp.bfloat16)
    outgoing = jnp.repeat(
        packed_rows.reshape(experts, capacity, own_columns.shape[1]), SPLIT, axis=0
    )
    arrived = lax.all_to_all(outgoing, EP, split_axis=0, concat_axis=0, tiled=True)
    arrived = collect(arrived, "tp", 2)
    sources = arrived.shape[0]
    slot_count = arrived.shape[1]
    flat_rows = arrived.reshape(sources * slot_count, model_width)
    gate_pre = jnp.dot(flat_rows, expert_gate[0], preferred_element_type=jnp.float32)
    up_pre = jnp.dot(flat_rows, expert_up[0], preferred_element_type=jnp.float32)
    hidden = (jax.nn.silu(gate_pre) * up_pre).astype(jnp.bfloat16)
    partial_out = jnp.dot(hidden, expert_down[0], preferred_element_type=jnp.float32).reshape(
        sources, slot_count, model_width
    )
    summed = sent_and_summed(partial_out.astype(jnp.bfloat16), "tp", 2)
    returned = lax.all_to_all(
        summed.astype(jnp.bfloat16), EP, split_axis=0, concat_axis=0, tiled=True
    ).astype(summed.dtype)
    expert_out = jnp.sum(returned.reshape(experts, SPLIT, capacity, quarter), 1).reshape(
        experts * capacity, quarter
    )
    routed_part = jnp.dot(
        combine_experts,
        expert_out,
        precision=lax.Precision.HIGHEST,
        preferred_element_type=jnp.float32,
    )
    branch = jax.nn.sigmoid(jnp.dot(x_mid, branch_gate, preferred_element_type=jnp.float32))
    gate_columns = lax.dynamic_slice_in_dim(dense_gate, tp_index * quarter, quarter, 1)
    up_columns = lax.dynamic_slice_in_dim(dense_up, tp_index * quarter, quarter, 1)
    shard_rows = gather_axes(own_columns, (("ep_0", "ep_1"), "ep_2"), 0)
    gate_pre = lax.dot_general(
        shard_rows, gate_columns, (((1,), (1,)), ((), ())), preferred_element_type=jnp.float32
    )
    up_pre = lax.dot_general(
        shard_rows, up_columns, (((1,), (1,)), ((), ())), preferred_element_type=jnp.float32
    )
    partials = jnp.stack([gate_pre, up_pre])
    summed_pre = of_everyone_2(partials.astype(jnp.bfloat16), "tp").astype(jnp.float32)
    dense_hidden = (jax.nn.silu(summed_pre[0]) * summed_pre[1]).astype(jnp.bfloat16)
    dense_part = sum_in_two_steps(
        jnp.dot(dense_hidden, dense_down, preferred_element_type=jnp.float32).astype(jnp.bfloat16),
        (("ep_0", "ep_1"), "ep_2"),
        0,
    )
    second_sum = (
        residual_scale * own_columns.astype(jnp.float32)
        + routed_part
        + branch[:, None] * dense_part
    )
    row_sums, square_sums = in_one(
        (jnp.sum(second_sum, 1), jnp.sum(second_sum * second_sum, 1)), "tp"
    )
    average = row_sums / model_width
    spread = square_sums / model_width - average * average
    return (
        (second_sum - average[:, None]) * lax.rsqrt(spread + norm_epsilon)[:, None] * second_gain
    ).astype(jnp.bfloat16)


def solution(mesh):
    finer = Mesh(mesh.devices.reshape(16, 4, 2, mesh.shape["tp"]), ("ep_0", "ep_1", "ep_2", "tp"))
    return jax.shard_map(
        shards,
        mesh=finer,
        in_specs=(
            P(EP, None),
            P(EP, "tp", None, None),
            P(None, "tp"),
            P(None, "tp"),
            P(None, "tp"),
            P("tp", None),
            P("tp"),
            P(),
            P(None, "tp"),
            P("tp"),
            P(),
            P(None, "tp"),
            P("tp"),
            P(),
            P(EP, None, "tp"),
            P(EP, None, "tp"),
            P(EP, "tp", None),
            P(EP, None),
            P(EP, None),
            P(EP, "tp"),
            P(),
            P("tp"),
            P(EP, None),
            P(EP, None),
        ),
        out_specs=P(EP, "tp"),
        check_vma=False,
    )
```

profile of v0, /device:TPU:2, one launch (start us, length us, event | category | flops | bytes accessed | tf_op | source)
XLA Modules:
  0.0 221.2 jit_solution(14173997141924158910)
XLA Ops:
  0.0 1.4 fusion.49
  1.4 0.1 reshape.100
  1.5 0.1 multiply_reduce_fusion.2
  1.6 1.2 fusion.13
  2.9 1.2 fusion.52
  4.1 0.1 reshape.114
  4.2 1.2 fusion.38
  5.5 1.2 fusion.51
  6.8 0.1 mul.179
  6.8 0.1 multiply_negate_fusion
  6.9 0.6 fusion.50
  7.6 1.5 fusion.2
  9.1 0.1 reduce_sum.160
  9.2 0.2 multiply_reduce_fusion.1
  9.4 0.1 subtract_multiply_fusion
  9.5 0.1 reshape.103
  9.6 0.2 fusion.42
  9.8 0.7 broadcast_in_dim.26
  10.5 4.5 %all-to-all-start = ((f32[4,16,1024]{2,1,0:T(8,128)}), f32[4,16,1024]{2,1,0:T(8,128)S(1)}, u32[]{:S(2)}, u32[]{:S(2)}) async-start(f32[4,16,1024]{2,1,0:T(8,128)} %broadcast_in_dim.26), calls=%async_computation | async-start | bytes 524288 | tf_op jit(solution)/shard_map/all_to_all | solution.py:19
  15.1 0.2 select_reduce_fusion.1
  15.3 6.3 %all-to-all-done = f32[4,16,1024]{2,1,0:T(8,128)S(1)} async-done(((f32[4,16,1024]{2,1,0:T(8,128)}), f32[4,16,1024]{2,1,0:T(8,128)S(1)}, u32[]{:S(2)}, u32[]{:S(2)}) %all-to-all-start) | async-done | bytes 262176 | tf_op jit(solution)/shard_map/all_to_all | solution.py:19
  21.6 0.1 fusion.33
  21.8 0.2 multiply_reduce_fusion
  22.1 0.2 convolution_convert_fusion.4
  22.4 35.4 %all_to_all.56 = bf16[128,2,256]{2,1,0:T(2,128)(2,1)S(1)} all-to-all(bf16[128,2,256]{2,1,0:T(2,128)(2,1)S(1)} %bitcast.101), channel_id=1, replica_groups=mesh['ep_0'=16,'ep_1'=4,'ep_2'=2,'tp'=4] {'ep_0','ep_1','ep_2'}, dimensions={0} | all-to-all | bytes 262144 | tf_op jit(solution)/shard_map/all_to_all | solution.py:210
  57.8 0.3 broadcast_in_dim.30
  58.1 12.4 %all_to_all.57 = bf16[4,128,2,256]{3,2,1,0:T(2,128)(2,1)S(1)} all-to-all(bf16[4,128,2,256]{3,2,1,0:T(2,128)(2,1)S(1)} %broadcast_in_dim.30), channel_id=1, replica_groups=mesh['ep_0'=16,'ep_1'=4,'ep_2'=2,'tp'=4] {'tp'}, dimensions={0} | all-to-all | bytes 1048576 | tf_op jit(solution)/shard_map/all_to_all | solution.py:19
  70.6 0.8 broadcast_in_dim.31
  71.4 6.1 %all-to-all-start.5 = ((bf16[64,16,256]{2,1,0:T(8,128)(2,1)}), bf16[64,16,256]{2,1,0:T(8,128)(2,1)S(1)}, u32[]{:S(2)}, u32[]{:S(2)}) async-start(bf16[64,16,256]{2,1,0:T(8,128)(2,1)} %broadcast_in_dim.31), calls=%async_computation.5 | async-start | bytes 1048576 | tf_op jit(solution)/shard_map/all_to_all | solution.py:19
  77.6 0.7 copy.108
  78.2 0.1 copy.132
  78.4 0.4 fusion.27
  78.8 0.4 fusion.8
  79.2 0.2 copy.109
  79.3 0.1 dot_general.72
  79.4 0.4 convolution_convert_fusion.3
  79.9 0.8 copy.146
  80.7 28.9 %all-to-all-done.5 = bf16[64,16,256]{2,1,0:T(8,128)(2,1)S(1)} async-done(((bf16[64,16,256]{2,1,0:T(8,128)(2,1)}), bf16[64,16,256]{2,1,0:T(8,128)(2,1)S(1)}, u32[]{:S(2)}, u32[]{:S(2)}) %all-to-all-start.5) | async-done | bytes 524320 | tf_op jit(solution)/shard_map/all_to_all | solution.py:19
  109.7 4.6 %all_to_all.58 = bf16[2,64,16,256]{3,2,1,0:T(8,128)(2,1)S(1)} all-to-all(bf16[2,64,16,256]{3,2,1,0:T(8,128)(2,1)S(1)} %broadcast_in_dim.32), channel_id=1, replica_groups=mesh['ep_0'=16,'ep_1'=4,'ep_2'=2,'tp'=4] {'ep_2'}, dimensions={0} | all-to-all | bytes 2097152 | tf_op jit(solution)/shard_map/all_to_all | solution.py:19
  114.3 3.5 %all-to-all-start.3 = ((bf16[4,128,2,256]{3,1,2,0:T(8,128)(2,1)}), bf16[4,128,2,256]{3,1,2,0:T(8,128)(2,1)S(1)}, u32[]{:S(2)}, u32[]{:S(2)}) async-start(bf16[4,128,2,256]{3,1,2,0:T(8,128)(2,1)} %bitcast.91), calls=%async_computation.3 | async-start | bytes 1048576 | tf_op jit(solution)/shard_map/all_to_all | solution.py:45
  117.8 0.1 copy.116
  117.9 1.1 fusion
  119.0 1.1 fusion.1
  120.2 0.2 copy.117
  120.4 7.4 %all-to-all-done.3 = bf16[4,128,2,256]{3,1,2,0:T(8,128)(2,1)S(1)} async-done(((bf16[4,128,2,256]{3,1,2,0:T(8,128)(2,1)}), bf16[4,128,2,256]{3,1,2,0:T(8,128)(2,1)S(1)}, u32[]{:S(2)}, u32[]{:S(2)}) %all-to-all-start.3) | async-done | bytes 524320 | tf_op jit(solution)/shard_map/all_to_all | solution.py:45
  127.8 1.3 broadcast_in_dim.33
  129.1 3.6 %all-to-all-start.7 = ((bf16[4,2,2048,22]{2,1,3,0:T(2,128)(2,1)}), bf16[4,2,2048,22]{2,1,3,0:T(2,128)(2,1)S(1)}, u32[]{:S(2)}, u32[]{:S(2)}) async-start(bf16[4,2,2048,22]{2,1,3,0:T(2,128)(2,1)} %broadcast_in_dim.33), calls=%async_computation.7 | async-start | bytes 1441792 | tf_op jit(solution)/shard_map/all_to_all | solution.py:19
  132.8 0.8 copy.113
  133.6 10.4 %all-to-all-done.7 = bf16[4,2,2048,22]{2,1,3,0:T(2,128)(2,1)S(1)} async-done(((bf16[4,2,2048,22]{2,1,3,0:T(2,128)(2,1)}), bf16[4,2,2048,22]{2,1,3,0:T(2,128)(2,1)S(1)}, u32[]{:S(2)}, u32[]{:S(2)}) %all-to-all-start.7) | async-done | bytes 720928 | tf_op jit(solution)/shard_map/all_to_all | solution.py:19
  144.0 0.7 convert_reduce_fusion
  144.7 0.3 fusion.48
  145.0 0.5 convolution_convert_fusion
  145.6 4.6 %all_to_all.59 = bf16[2,64,16,256]{3,2,1,0:T(8,128)(2,1)S(1)} all-to-all(bf16[2,64,16,256]{3,2,1,0:T(8,128)(2,1)S(1)} %bitcast.94), channel_id=1, replica_groups=mesh['ep_0'=16,'ep_1'=4,'ep_2'=2,'tp'=4] {'ep_2'}, dimensions={0} | all-to-all | bytes 2097152 | tf_op jit(solution)/shard_map/all_to_all | solution.py:45
  150.2 6.9 %all-to-all-start.4 = ((bf16[128,2,256]{2,1,0:T(2,128)(2,1)}), bf16[128,2,256]{2,1,0:T(2,128)(2,1)S(1)}, u32[]{:S(2)}, u32[]{:S(2)}) async-start(bf16[128,2,256]{2,1,0:T(2,128)(2,1)} %copy.113), calls=%async_computation.4 | async-start | bytes 262144 | tf_op jit(solution)/shard_map/all_to_all | solution.py:222
  157.1 1.1 reduce_sum.171
  158.2 15.0 %all-to-all-done.4 = bf16[128,2,256]{2,1,0:T(2,128)(2,1)S(1)} async-done(((bf16[128,2,256]{2,1,0:T(2,128)(2,1)}), bf16[128,2,256]{2,1,0:T(2,128)(2,1)S(1)}, u32[]{:S(2)}, u32[]{:S(2)}) %all-to-all-start.4) | async-done | bytes 131104 | tf_op jit(solution)/shard_map/all_to_all | solution.py:222
  173.2 6.3 %all-to-all-start.9 = ((bf16[64,16,256]{2,1,0:T(8,128)(2,1)}), bf16[64,16,256]{2,1,0:T(8,128)(2,1)S(1)}, u32[]{:S(2)}, u32[]{:S(2)}) async-start(bf16[64,16,256]{2,1,0:T(8,128)(2,1)} %reduce_sum.171), calls=%async_computation.9 | async-start | bytes 1048576 | tf_op jit(solution)/shard_map/all_to_all | solution.py:64
  179.6 0.1 fusion.19
  179.7 0.1 convert_reduce_fusion.2
  179.9 32.5 %all-to-all-done.9 = bf16[64,16,256]{2,1,0:T(8,128)(2,1)S(1)} async-done(((bf16[64,16,256]{2,1,0:T(8,128)(2,1)}), bf16[64,16,256]{2,1,0:T(8,128)(2,1)S(1)}, u32[]{:S(2)}, u32[]{:S(2)}) %all-to-all-start.9) | async-done | bytes 524320 | tf_op jit(solution)/shard_map/all_to_all | solution.py:64
  212.4 0.1 convert_reduce_fusion.1
  212.5 0.3 fusion.47
  212.8 7.6 %all_to_all.60 = f32[4,1,32]{2,1,0:T(1,128)S(1)} all-to-all(f32[4,1,32]{2,1,0:T(1,128)S(1)} %broadcast_in_dim.34), channel_id=1, replica_groups=mesh['ep_0'=16,'ep_1'=4,'ep_2'=2,'tp'=4] {'tp'}, dimensions={0} | all-to-all | bytes 1024 | tf_op jit(solution)/shard_map/all_to_all | solution.py:19
  220.5 0.7 multiply_convert_fusion.1
  (54 shorter events, 1.2 us)
Async XLA Ops:
  0.0 79.4 %copy-start = (bf16[1,352,1024]{2,1,0:T(8,128)(2,1)S(1)}, bf16[1,352,1024]{2,1,0:T(8,128)(2,1)}, u32[]{:S(2)}) copy-start(bf16[1,352,1024]{2,1,0:T(8,128)(2,1)} %param.40) | copy-start | bytes 2162692
  0.0 6.9 %copy-start.2 = (f32[16,4,64,64]{3,2,1,0:T(8,128)S(1)}, f32[16,4,64,64]{3,2,1,0:T(8,128)}, u32[]{:S(2)}) copy-start(f32[16,4,64,64]{3,2,1,0:T(8,128)} %param.25) | copy-start | bytes 3145732
  7.6 2.0 copy-start.4
  7.6 2.0 copy-start.8
  7.6 7.4 %copy-start.5 = (s32[16,2]{0,1:T(2,128)S(1)}, s32[16,2]{0,1:T(2,128)}, u32[]{:S(2)}) copy-start(s32[16,2]{0,1:T(2,128)} %param.46) | copy-start | bytes 388
  7.6 14.1 %copy-start.1 = (bf16[16,1024]{1,0:T(8,128)(2,1)S(1)}, bf16[16,1024]{1,0:T(8,128)(2,1)}, u32[]{:S(2)}) copy-start(bf16[16,1024]{1,0:T(8,128)(2,1)} %param.24) | copy-start | bytes 98308
  7.6 14.4 %copy-start.6 = (f32[1024]{0:T(1024)S(1)}, f32[1024]{0:T(1024)}, u32[]{:S(2)}) copy-start(f32[1024]{0:T(1024)} %param.37) | copy-start | bytes 12292
  10.5 11.1 %all-to-all-start = ((f32[4,16,1024]{2,1,0:T(8,128)}), f32[4,16,1024]{2,1,0:T(8,128)S(1)}, u32[]{:S(2)}, u32[]{:S(2)}) async-start(f32[4,16,1024]{2,1,0:T(8,128)} %broadcast_in_dim.26), calls=%async_computation | async-start | bytes 524288 | tf_op jit(solution)/shard_map/all_to_all | solution.py:19
  70.6 7.8 %copy-start.3 = (bf16[1,1024,352]{1,2,0:T(8,128)(2,1)S(1)}, bf16[1,1024,352]{1,2,0:T(8,128)(2,1)}, u32[]{:S(2)}) copy-start(bf16[1,1024,352]{1,2,0:T(8,128)(2,1)} %param.38) | copy-start | bytes 2162692
  71.4 38.3 %all-to-all-start.5 = ((bf16[64,16,256]{2,1,0:T(8,128)(2,1)}), bf16[64,16,256]{2,1,0:T(8,128)(2,1)S(1)}, u32[]{:S(2)}, u32[]{:S(2)}) async-start(bf16[64,16,256]{2,1,0:T(8,128)(2,1)} %broadcast_in_dim.31), calls=%async_computation.5 | async-start | bytes 1048576 | tf_op jit(solution)/shard_map/all_to_all | solution.py:19
  77.5 1.2 copy-start.11
  114.3 13.5 %all-to-all-start.3 = ((bf16[4,128,2,256]{3,1,2,0:T(8,128)(2,1)}), bf16[4,128,2,256]{3,1,2,0:T(8,128)(2,1)S(1)}, u32[]{:S(2)}, u32[]{:S(2)}) async-start(bf16[4,128,2,256]{3,1,2,0:T(8,128)(2,1)} %bitcast.91), calls=%async_computation.3 | async-start | bytes 1048576 | tf_op jit(solution)/shard_map/all_to_all | solution.py:45
  129.1 15.9 %copy-start.12 = (bf16[22,256]{1,0:T(8,128)(2,1)S(1)}, bf16[22,256]{1,0:T(8,128)(2,1)}, u32[]{:S(2)}) copy-start(bf16[22,256]{1,0:T(8,128)(2,1)} %param.43) | copy-start | bytes 33796
  129.1 14.9 %all-to-all-start.7 = ((bf16[4,2,2048,22]{2,1,3,0:T(2,128)(2,1)}), bf16[4,2,2048,22]{2,1,3,0:T(2,128)(2,1)S(1)}, u32[]{:S(2)}, u32[]{:S(2)}) async-start(bf16[4,2,2048,22]{2,1,3,0:T(2,128)(2,1)} %broadcast_in_dim.33), calls=%async_computation.7 | async-start | bytes 1441792 | tf_op jit(solution)/shard_map/all_to_all | solution.py:19
  145.6 33.9 %copy-start.7 = (bf16[1024]{0:T(1024)(128)(2,1)S(1)}, bf16[1024]{0:T(1024)(128)(2,1)}, u32[]{:S(2)}) copy-start(bf16[1024]{0:T(1024)(128)(2,1)} %param.44) | copy-start | bytes 6148
  145.6 33.9 %copy-start.9 = (f32[16,2]{0,1:T(2,128)S(1)}, f32[16,2]{0,1:T(2,128)}, u32[]{:S(2)}) copy-start(f32[16,2]{0,1:T(2,128)} %param.47) | copy-start | bytes 388
  150.2 70.3 %copy-start.10 = (f32[256]{0:T(256)S(1)}, f32[256]{0:T(256)}, u32[]{:S(2)}) copy-start(f32[256]{0:T(256)} %param.45) | copy-start | bytes 3076
  150.2 23.0 %all-to-all-start.4 = ((bf16[128,2,256]{2,1,0:T(2,128)(2,1)}), bf16[128,2,256]{2,1,0:T(2,128)(2,1)S(1)}, u32[]{:S(2)}, u32[]{:S(2)}) async-start(bf16[128,2,256]{2,1,0:T(2,128)(2,1)} %copy.113), calls=%async_computation.4 | async-start | bytes 262144 | tf_op jit(solution)/shard_map/all_to_all | solution.py:222
  173.2 39.2 %all-to-all-start.9 = ((bf16[64,16,256]{2,1,0:T(8,128)(2,1)}), bf16[64,16,256]{2,1,0:T(8,128)(2,1)S(1)}, u32[]{:S(2)}, u32[]{:S(2)}) async-start(bf16[64,16,256]{2,1,0:T(8,128)(2,1)} %reduce_sum.171), calls=%async_computation.9 | async-start | bytes 1048576 | tf_op jit(solution)/shard_map/all_to_all | solution.py:64
where the time goes:
time: 222 us; the launch traced here: 221 us
  waiting for transfers between devices  100 us (45%)
  blocking collectives  64.6 us (29%)
  starting transfers between devices  30.9 us (14%)
  matrix products  13 us (6%)
  local copies, waits for them, and re-layouts  7.25 us (3%)
  other arithmetic  4.43 us (2%)
    all_to_all x3, waiting for transfers between devices, sent_to_all(): return lax.all_to_all(copies, axis, split_axis=0, concat_axis=0, tiled=True)  45.6 us
    all_to_all x1, blocking collectives, shards(): lax.all_to_all(outgoing, EP, split_axis=0, concat_axis=0, tiled=True)  35.4 us
    all_to_all x1, waiting for transfers between devices, sum_in_two_steps(): lax.all_to_all(nearer.astype(jnp.bfloat16), far, split_axis=0, concat_axi...  32.5 us
    all_to_all x3, blocking collectives, sent_to_all(): return lax.all_to_all(copies, axis, split_axis=0, concat_axis=0, tiled=True)  24.6 us
    all_to_all x1, waiting for transfers between devices, shards(): lax.all_to_all(summed.astype(jnp.bfloat16), EP, split_axis=0, concat_axis...  15 us
    all_to_all x3, starting transfers between devices, sent_to_all(): return lax.all_to_all(copies, axis, split_axis=0, concat_axis=0, tiled=True)  14.2 us
    all_to_all x1, waiting for transfers between devices, sent_and_summed(): lax.all_to_all(parts, axis, split_axis=0, concat_axis=0, tiled=True)  7.44 us
    all_to_all x1, starting transfers between devices, shards(): lax.all_to_all(summed.astype(jnp.bfloat16), EP, split_axis=0, concat_axis...  6.86 us
  transfers between devices with their start and end apart: 6, of which 6 were waited for; matrix products, arithmetic and copies ran while one was open for 4% of the time, Pallas kernels for 0%

commit v1 on v0

--- a/solution.py
+++ b/solution.py
@@ -5,7 +5,8 @@
 from jax.sharding import PartitionSpec as P
 
 SPLIT = 4
-EP = ("ep_0", "ep_1", "ep_2")
+EP = ("z", "x", "c")
+PLANE = ("x", "c", "tp")
 
 
 residual_scale = 1.4142135623730951
@@ -20,51 +21,11 @@
 
 
 def of_everyone(value, axis):
-    return sent_to_all(value, axis).sum(axis=0)
-
-
-def joined_along(parts, dim):
-    parts = jnp.moveaxis(parts, 0, dim)
-    shape = parts.shape
-    return parts.reshape(*shape[:dim], shape[dim] * shape[dim + 1], *shape[dim + 2 :])
-
-
-def collect(value, axis, dim):
-    parts = sent_to_all(value, axis)
-    return joined_along(parts, dim)
-
-
-def cut_along(value, dim, length):
-    shape = value.shape
-    parts = value.reshape(*shape[:dim], length, shape[dim] // length, *shape[dim + 1 :])
-    return jnp.moveaxis(parts, dim, 0)
-
-
-def sent_and_summed(value, axis, dim):
-    parts = cut_along(value, dim, lax.axis_size(axis))
-    arrived = lax.all_to_all(parts, axis, split_axis=0, concat_axis=0, tiled=True)
-    return arrived.astype(jnp.float32).sum(axis=0)
-
-
-def gather_axes(value, axes, dim):
-    far, near = axes
-    parts = sent_to_all(sent_to_all(value, far), near)
-    return joined_along(parts.swapaxes(0, 1).reshape(-1, *value.shape), dim)
-
-
-def of_everyone_2(value, axis):
-    everything = sent_to_all(value, axis)
-    return jnp.sum(everything.astype(jnp.float32), axis=0)
-
-
-def sum_in_two_steps(value, axes, dim):
-    far, near = axes
-    parts = cut_along(value, dim, lax.axis_size(far))
-    nearer = sent_and_summed(parts, near, dim + 1)
-    arrived = lax.all_to_all(
-        nearer.astype(jnp.bfloat16), far, split_axis=0, concat_axis=0, tiled=True
-    )
-    return arrived.astype(jnp.float32).sum(axis=0)
+    return sent_to_all(value, axis).astype(jnp.float32).sum(axis=0)
+
+
+def exchange(parts, axis):
+    return lax.all_to_all(parts, axis, split_axis=0, concat_axis=0, tiled=True)
 
 
 def in_one(arrays, axis):
@@ -74,6 +35,24 @@
         done.append(running[at : at + a.size].reshape(a.shape))
         at += a.size
     return tuple(done)
+
+
+def plane_weights(dense_gate, dense_up, dense_down, quarter):
+    y = lax.axis_size("tp")
+    z = lax.axis_size("z")
+    tp_index = lax.axis_index("tp")
+    gate = lax.dynamic_slice_in_dim(dense_gate, tp_index * quarter, quarter, 1)
+    up = lax.dynamic_slice_in_dim(dense_up, tp_index * quarter, quarter, 1)
+    units = gate.shape[0]
+    part = -(-units // y)
+    three = jnp.stack([gate, up, dense_down])
+    three = jnp.pad(three, ((0, 0), (0, part * y - units), (0, 0)))
+    three = three.reshape(3, y, part, quarter).swapaxes(0, 1)
+    message = three.reshape(y, 3 * part * quarter // 128, 128)
+    outgoing = jnp.broadcast_to(message, (z, *message.shape)).reshape(z * y, *message.shape[1:])
+    arrived = exchange(outgoing, ("z", "tp"))
+    arrived = arrived.reshape(z, y, 3, part, quarter)
+    return arrived.transpose(2, 0, 3, 1, 4).reshape(3, z * part, y * quarter)
 
 
 def time_mixer(
@@ -180,6 +159,11 @@
     model_width = tokens.shape[1]
     quarter = w_recep.shape[1]
     tp_index = lax.axis_index("tp")
+    planes = lax.axis_size("z")
+    plane_blocks = lax.axis_size(("x", "c"))
+    plane_size = lax.axis_size(PLANE)
+    tp_size = lax.axis_size("tp")
+    weights = plane_weights(dense_gate, dense_up, dense_down, quarter)
     partial_mix = time_mixer(
         tokens,
         state,
@@ -195,36 +179,54 @@
         rate_up,
         head_gain,
     )
-    mixed = of_everyone(partial_mix, "tp")
+    mixed = of_everyone(partial_mix.astype(jnp.bfloat16), "tp")
     x_mid = first_norm(residual_scale * tokens.astype(jnp.float32) + mixed, first_gain)
     own_columns = lax.dynamic_slice_in_dim(x_mid, tp_index * quarter, quarter, 1)
     experts = lax.axis_size(EP) // SPLIT
+    here = experts // planes
     capacity = min(row_count, max(2, 2 * row_count * routes.shape[1] // experts))
     dispatch_tokens, combine_experts = route_tables(routes, route_weights, experts, capacity)
     packed_rows = lax.dot_general(
         dispatch_tokens, own_columns, (((0,), (0,)), ((), ())), preferred_element_type=jnp.float32
     ).astype(jnp.bfloat16)
-    outgoing = jnp.repeat(
-        packed_rows.reshape(experts, capacity, own_columns.shape[1]), SPLIT, axis=0
-    )
-    arrived = lax.all_to_all(outgoing, EP, split_axis=0, concat_axis=0, tiled=True)
-    arrived = collect(arrived, "tp", 2)
-    sources = arrived.shape[0]
-    slot_count = arrived.shape[1]
-    flat_rows = arrived.reshape(sources * slot_count, model_width)
+    arrived = exchange(packed_rows.reshape(planes, here * capacity, quarter), "z")
+    rows = planes * capacity
+    arrived = arrived.reshape(planes, here, capacity, quarter).swapaxes(0, 1)
+    arrived = arrived.reshape(here, rows, quarter)
+    both = jnp.concatenate([arrived, jnp.broadcast_to(own_columns, (here, *own_columns.shape))], 1)
+    outgoing = jnp.repeat(both, plane_size // here, axis=0)
+    everything = exchange(outgoing, PLANE)
+    everything = everything.reshape(plane_blocks, tp_size, rows + row_count, quarter).swapaxes(1, 2)
+    everything = everything.reshape(plane_blocks, rows + row_count, model_width)
+    flat_rows = everything[:, :rows].reshape(plane_blocks * rows, model_width)
+    dense_rows = everything[:, rows:].reshape(plane_blocks * row_count, model_width)
     gate_pre = jnp.dot(flat_rows, expert_gate[0], preferred_element_type=jnp.float32)
     up_pre = jnp.dot(flat_rows, expert_up[0], preferred_element_type=jnp.float32)
     hidden = (jax.nn.silu(gate_pre) * up_pre).astype(jnp.bfloat16)
-    partial_out = jnp.dot(hidden, expert_down[0], preferred_element_type=jnp.float32).reshape(
-        sources, slot_count, model_width
-    )
-    summed = sent_and_summed(partial_out.astype(jnp.bfloat16), "tp", 2)
-    returned = lax.all_to_all(
-        summed.astype(jnp.bfloat16), EP, split_axis=0, concat_axis=0, tiled=True
-    ).astype(summed.dtype)
-    expert_out = jnp.sum(returned.reshape(experts, SPLIT, capacity, quarter), 1).reshape(
-        experts * capacity, quarter
-    )
+    partial_out = jnp.dot(hidden, expert_down[0], preferred_element_type=jnp.float32)
+    dense_pre = [
+        lax.dot_general(
+            dense_rows, weights[i], (((1,), (1,)), ((), ())), preferred_element_type=jnp.float32
+        )
+        for i in range(2)
+    ]
+    dense_hidden = (jax.nn.silu(dense_pre[0]) * dense_pre[1]).astype(jnp.bfloat16)
+    dense_out = jnp.dot(dense_hidden, weights[2], preferred_element_type=jnp.float32)
+    returning = jnp.concatenate(
+        [
+            partial_out.astype(jnp.bfloat16).reshape(plane_blocks, rows, model_width),
+            dense_out.astype(jnp.bfloat16).reshape(plane_blocks, row_count, model_width),
+        ],
+        1,
+    )
+    returning = returning.reshape(plane_blocks, rows + row_count, tp_size, quarter).swapaxes(1, 2)
+    returned = exchange(returning.reshape(plane_size, rows + row_count, quarter), PLANE)
+    returned = returned.astype(jnp.float32)
+    dense_part = jnp.sum(returned[:, rows:], 0)
+    summed = jnp.sum(returned[:, :rows].reshape(here, plane_size // here, rows, quarter), 1)
+    summed = summed.reshape(here, planes, capacity, quarter).swapaxes(0, 1).astype(jnp.bfloat16)
+    expert_out = exchange(summed.reshape(planes, here * capacity, quarter), "z")
+    expert_out = expert_out.reshape(experts * capacity, quarter).astype(jnp.float32)
     routed_part = jnp.dot(
         combine_experts,
         expert_out,
@@ -232,23 +234,6 @@
         preferred_element_type=jnp.float32,
     )
     branch = jax.nn.sigmoid(jnp.dot(x_mid, branch_gate, preferred_element_type=jnp.float32))
-    gate_columns = lax.dynamic_slice_in_dim(dense_gate, tp_index * quarter, quarter, 1)
-    up_columns = lax.dynamic_slice_in_dim(dense_up, tp_index * quarter, quarter, 1)
-    shard_rows = gather_axes(own_columns, (("ep_0", "ep_1"), "ep_2"), 0)
-    gate_pre = lax.dot_general(
-        shard_rows, gate_columns, (((1,), (1,)), ((), ())), preferred_element_type=jnp.float32
-    )
-    up_pre = lax.dot_general(
-        shard_rows, up_columns, (((1,), (1,)), ((), ())), preferred_element_type=jnp.float32
-    )
-    partials = jnp.stack([gate_pre, up_pre])
-    summed_pre = of_everyone_2(partials.astype(jnp.bfloat16), "tp").astype(jnp.float32)
-    dense_hidden = (jax.nn.silu(summed_pre[0]) * summed_pre[1]).astype(jnp.bfloat16)
-    dense_part = sum_in_two_steps(
-        jnp.dot(dense_hidden, dense_down, preferred_element_type=jnp.float32).astype(jnp.bfloat16),
-        (("ep_0", "ep_1"), "ep_2"),
-        0,
-    )
     second_sum = (
         residual_scale * own_columns.astype(jnp.float32)
         + routed_part
@@ -265,7 +250,7 @@
 
 
 def solution(mesh):
-    finer = Mesh(mesh.devices.reshape(16, 4, 2, mesh.shape["tp"]), ("ep_0", "ep_1", "ep_2", "tp"))
+    finer = Mesh(mesh.devices.reshape(16, 4, 2, mesh.shape["tp"]), ("z", "x", "c", "tp"))
     return jax.shard_map(
         shards,
         mesh=finer,

time: 222 us -> 162 us (0.73)
  blocking collectives: 64.6 us -> 35.8 us
  waiting for transfers between devices: 100 us -> 78.5 us
  starting transfers between devices: 30.9 us -> 25.5 us
    all_to_all x3 -> x1, waiting for transfers between devices: 45.6 us -> 5.58 us  [sent_to_all(): return lax.all_to_all(copies, axis, split_axis=0, concat_axis=0, tiled=True)]
    all_to_all x3 -> x4, waiting for transfers between devices: 54.9 us -> 72.9 us  [exchange(): return lax.all_to_all(parts, axis, split_axis=0, concat_axis=0, tiled=True)]
    all_to_all x3 -> x1, blocking collectives: 24.6 us -> 8.2 us  [sent_to_all(): return lax.all_to_all(copies, axis, split_axis=0, concat_axis=0, tiled=True)]
    all_to_all x2 -> x1, blocking collectives: 40 us -> 27.6 us  [exchange(): return lax.all_to_all(parts, axis, split_axis=0, concat_axis=0, tiled=True)]
    all_to_all x3 -> x1, starting transfers between devices: 14.2 us -> 4.46 us  [sent_to_all(): return lax.all_to_all(copies, axis, split_axis=0, concat_axis=0, tiled=True)]
    all_to_all x3 -> x4, starting transfers between devices: 16.7 us -> 21 us  [exchange(): return lax.all_to_all(parts, axis, split_axis=0, concat_axis=0, tiled=True)]
    broadcast_in_dim x6 -> x2, local copies, waits for them, and re-layouts: 3.18 us -> 0.66 us  [sent_to_all(): copies = jnp.broadcast_to(value, (lax.axis_size(axis), *value.shape))]
    dot_general x4 -> x2, matrix products: 3.1 us -> 0.79 us  [the longest x1 0.57 us: shards(): jnp.dot(dense_hidden, weights[2], preferred_element_type=jnp.float32)]
  transfers between devices with their start and end apart: 6 -> 5, of which waited for: 6 -> 5; matrix products, arithmetic and copies ran while one was open for 4% -> 3% of each run, Pallas kernels for 0% -> 0%
where the time goes in v1:
time: 162 us; the launch traced here: 161 us
  waiting for transfers between devices  78.5 us (48%)
  blocking collectives  35.8 us (22%)
  starting transfers between devices  25.5 us (16%)
  matrix products  11.7 us (7%)
  local copies, waits for them, and re-layouts  5.44 us (3%)
  other arithmetic  3.65 us (2%)
    all_to_all x4, waiting for transfers between devices, exchange(): return lax.all_to_all(parts, axis, split_axis=0, concat_axis=0, tiled=True)  72.9 us
    all_to_all x1, blocking collectives, exchange(): return lax.all_to_all(parts, axis, split_axis=0, concat_axis=0, tiled=True)  27.6 us
    all_to_all x4, starting transfers between devices, exchange(): return lax.all_to_all(parts, axis, split_axis=0, concat_axis=0, tiled=True)  21 us
    all_to_all x1, blocking collectives, sent_to_all(): return lax.all_to_all(copies, axis, split_axis=0, concat_axis=0, tiled=True)  8.2 us
    all_to_all x1, waiting for transfers between devices, sent_to_all(): return lax.all_to_all(copies, axis, split_axis=0, concat_axis=0, tiled=True)  5.58 us
    all_to_all x1, starting transfers between devices, sent_to_all(): return lax.all_to_all(copies, axis, split_axis=0, concat_axis=0, tiled=True)  4.46 us
  transfers between devices with their start and end apart: 5, of which 5 were waited for; matrix products, arithmetic and copies ran while one was open for 3% of the time, Pallas kernels for 0%

profile of v1, /device:TPU:2, one launch (start us, length us, event | category | flops | bytes accessed | tf_op | source)
XLA Modules:
  0.0 161.1 jit_solution(12171934072234412635)
XLA Ops:
  0.0 1.4 fusion.65
  1.4 0.1 reshape.168
  1.5 1.2 fusion.62
  2.8 0.1 reshape.144
  2.9 0.1 multiply_reduce_fusion.2
  3.0 1.2 fusion.64
  4.2 0.1 mul.179
  4.3 1.2 fusion.55
  5.5 0.1 mul.169
  5.6 0.3 fusion.12
  5.9 0.1 reshape.145
  6.0 0.1 multiply_negate_fusion
  6.1 0.6 fusion.63
  6.8 0.0 copy-start.9
  6.8 1.5 fusion
  8.2 0.1 reduce_sum.127
  8.4 0.2 multiply_reduce_fusion.1
  8.5 0.1 subtract_multiply_fusion
  8.6 0.1 reshape.147
  8.7 0.2 convolution_convert_fusion.3
  8.9 0.7 broadcast_in_dim.18
  9.6 4.5 %all-to-all-start = ((bf16[4,16,1024]{2,1,0:T(8,128)(2,1)}), bf16[4,16,1024]{2,1,0:T(8,128)(2,1)S(1)}, u32[]{:S(2)}, u32[]{:S(2)}) async-start(bf16[4,16,1024]{2,1,0:T(8,128)(2,1)} %broadcast_in_dim.18), calls=%async_computation | async-start | bytes 262144 | tf_op jit(solution)/shard_map/all_to_all | solution.py:20
  14.0 0.1 convert_reduce_fusion.1
  14.2 0.2 select_reduce_fusion.1
  14.4 0.1 fusion.56
  14.4 5.6 %all-to-all-done = bf16[4,16,1024]{2,1,0:T(8,128)(2,1)S(1)} async-done(((bf16[4,16,1024]{2,1,0:T(8,128)(2,1)}), bf16[4,16,1024]{2,1,0:T(8,128)(2,1)S(1)}, u32[]{:S(2)}, u32[]{:S(2)}) %all-to-all-start) | async-done | bytes 131104 | tf_op jit(solution)/shard_map/all_to_all | solution.py:20
  20.0 0.1 fusion.50
  20.2 0.2 multiply_reduce_fusion
  20.4 0.1 multiply_convert_fusion
  20.5 0.2 convolution_convert_fusion.2
  20.7 27.6 %all_to_all.36 = bf16[16,4,256]{2,1,0:T(4,128)(2,1)S(1)} all-to-all(bf16[16,4,256]{2,1,0:T(4,128)(2,1)S(1)} %reshape.148), channel_id=1, replica_groups=mesh['z'=16,'x'=4,'c'=2,'tp'=4] {'z'}, dimensions={0} | all-to-all | bytes 65536 | tf_op jit(solution)/shard_map/all_to_all | solution.py:28
  48.4 0.1 pad_maximum_fusion.1
  48.5 0.9 broadcast_in_dim.22
  49.4 5.6 %all-to-all-start.2 = ((bf16[32,48,256]{2,1,0:T(8,128)(2,1)}), bf16[32,48,256]{2,1,0:T(8,128)(2,1)S(1)}, u32[]{:S(2)}, u32[]{:S(2)}) async-start(bf16[32,48,256]{2,1,0:T(8,128)(2,1)} %bitcast.10), calls=%async_computation.2 | async-start | bytes 1572864 | tf_op jit(solution)/shard_map/all_to_all | solution.py:28
  55.0 0.7 dynamic-slice_bitcast_fusion
  55.8 11.9 %all-to-all-done.2 = bf16[32,48,256]{2,1,0:T(8,128)(2,1)S(1)} async-done(((bf16[32,48,256]{2,1,0:T(8,128)(2,1)}), bf16[32,48,256]{2,1,0:T(8,128)(2,1)S(1)}, u32[]{:S(2)}, u32[]{:S(2)}) %all-to-all-start.2) | async-done | bytes 786464 | tf_op jit(solution)/shard_map/all_to_all | solution.py:28
  67.8 0.9 broadcast_in_dim.27
  68.7 4.8 %all-to-all-start.3 = ((bf16[64,36,128]{2,1,0:T(8,128)(2,1)}), bf16[64,36,128]{2,1,0:T(8,128)(2,1)S(1)}, u32[]{:S(2)}, u32[]{:S(2)}) async-start(bf16[64,36,128]{2,1,0:T(8,128)(2,1)} %bitcast.23), calls=%async_computation.3 | async-start | bytes 1310720 | tf_op jit(solution)/shard_map/all_to_all | solution.py:28
  73.5 0.1 copy.111
  73.7 0.4 fusion.28
  74.1 2.3 %convolution_convert_fusion = bf16[256,1024]{1,0:T(8,128)(2,1)S(1)} fusion(bf16[256,1024]{1,0:T(8,128)(2,1)S(1)} %bitcast.105, bf16[1,352,1024]{2,1,0:T(8,128)(2,1)S(1)} %copy-done, bf16[1,1024,352]{1,2,0:T(8,128)(2,1)} %param.39, f32[256,352]{0,1:T(8,128)S(1)} %fusion.28), kind=kOutput, calls=%fused_computation.6 | convolution fusion | flops 369901568 | bytes 2850816 | tf_op jit(solution)/shard_map/dot_general | solution.py:206
  76.4 36.1 %all-to-all-done.3 = bf16[64,36,128]{2,1,0:T(8,128)(2,1)S(1)} async-done(((bf16[64,36,128]{2,1,0:T(8,128)(2,1)}), bf16[64,36,128]{2,1,0:T(8,128)(2,1)S(1)}, u32[]{:S(2)}, u32[]{:S(2)}) %all-to-all-start.3) | async-done | bytes 589856 | tf_op jit(solution)/shard_map/all_to_all | solution.py:28
  112.4 0.3 reshape.160
  112.7 0.1 fusion.61
  112.8 0.1 copy.98
  112.9 0.1 copy.100
  113.0 0.1 copy.99
  113.1 0.2 fusion.66
  113.4 0.6 convolution_convert_fusion.1
  114.0 0.9 fusion.24
  115.0 7.1 %all-to-all-start.4 = ((bf16[32,48,256]{2,1,0:T(8,128)(2,1)}), bf16[32,48,256]{2,1,0:T(8,128)(2,1)S(1)}, u32[]{:S(2)}, u32[]{:S(2)}) async-start(bf16[32,48,256]{2,1,0:T(8,128)(2,1)} %bitcast.26), calls=%async_computation.4 | async-start | bytes 1572864 | tf_op jit(solution)/shard_map/all_to_all | solution.py:28
  122.1 0.1 select_reduce_fusion
  122.2 0.1 fusion.18
  122.3 12.5 %all-to-all-done.4 = bf16[32,48,256]{2,1,0:T(8,128)(2,1)S(1)} async-done(((bf16[32,48,256]{2,1,0:T(8,128)(2,1)}), bf16[32,48,256]{2,1,0:T(8,128)(2,1)S(1)}, u32[]{:S(2)}, u32[]{:S(2)}) %all-to-all-start.4) | async-done | bytes 786464 | tf_op jit(solution)/shard_map/all_to_all | solution.py:28
  134.9 0.2 convert_element_type.75
  135.1 0.1 bitcast_reduce_fusion
  135.2 0.6 copy.103
  135.8 3.5 %all-to-all-start.5 = ((bf16[16,4,256]{2,1,0:T(4,128)(2,1)}), bf16[16,4,256]{2,1,0:T(4,128)(2,1)S(1)}, u32[]{:S(2)}, u32[]{:S(2)}) async-start(bf16[16,4,256]{2,1,0:T(4,128)(2,1)} %copy.103), calls=%async_computation.5 | async-start | bytes 65536 | tf_op jit(solution)/shard_map/all_to_all | solution.py:28
  139.3 12.4 %all-to-all-done.5 = bf16[16,4,256]{2,1,0:T(4,128)(2,1)S(1)} async-done(((bf16[16,4,256]{2,1,0:T(4,128)(2,1)}), bf16[16,4,256]{2,1,0:T(4,128)(2,1)S(1)}, u32[]{:S(2)}, u32[]{:S(2)}) %all-to-all-start.5) | async-done | bytes 32800 | tf_op jit(solution)/shard_map/all_to_all | solution.py:28
  151.8 0.2 fusion.60
  152.0 0.1 pad_maximum_fusion.2
  152.1 8.2 %all_to_all.37 = f32[4,1,32]{2,1,0:T(1,128)S(1)} all-to-all(f32[4,1,32]{2,1,0:T(1,128)S(1)} %broadcast_in_dim.28), channel_id=1, replica_groups=mesh['z'=16,'x'=4,'c'=2,'tp'=4] {'tp'}, dimensions={0} | all-to-all | bytes 1024 | tf_op jit(solution)/shard_map/all_to_all | solution.py:20
  160.3 0.1 slice_multiply_fusion
  160.4 0.7 multiply_convert_fusion.1
  (61 shorter events, 0.6 us)
Async XLA Ops:
  0.0 74.1 %copy-start = (bf16[1,352,1024]{2,1,0:T(8,128)(2,1)S(1)}, bf16[1,352,1024]{2,1,0:T(8,128)(2,1)}, u32[]{:S(2)}) copy-start(bf16[1,352,1024]{2,1,0:T(8,128)(2,1)} %param.40) | copy-start | bytes 2162692
  0.0 5.6 %copy-start.1 = (bf16[16,1024]{1,0:T(8,128)(2,1)S(1)}, bf16[16,1024]{1,0:T(8,128)(2,1)}, u32[]{:S(2)}) copy-start(bf16[16,1024]{1,0:T(8,128)(2,1)} %param.24) | copy-start | bytes 98308
  0.0 5.6 %copy-start.6 = (bf16[64,256]{1,0:T(8,128)(2,1)S(1)}, bf16[64,256]{1,0:T(8,128)(2,1)}, u32[]{:S(2)}) copy-start(bf16[64,256]{1,0:T(8,128)(2,1)} %param.35) | copy-start | bytes 98308
  0.0 5.6 %copy-start.5 = (bf16[1024,64]{0,1:T(8,128)(2,1)S(1)}, bf16[1024,64]{0,1:T(8,128)(2,1)}, u32[]{:S(2)}) copy-start(bf16[1024,64]{0,1:T(8,128)(2,1)} %param.34) | copy-start | bytes 393220
  0.0 5.6 %copy-start.11 = (f32[256]{0:T(256)S(1)}, f32[256]{0:T(256)}, u32[]{:S(2)}) copy-start(f32[256]{0:T(256)} %param.33) | copy-start | bytes 3076
  0.0 6.1 %copy-start.2 = (f32[16,4,64,64]{3,2,1,0:T(8,128)S(1)}, f32[16,4,64,64]{3,2,1,0:T(8,128)}, u32[]{:S(2)}) copy-start(f32[16,4,64,64]{3,2,1,0:T(8,128)} %param.25) | copy-start | bytes 3145732
  6.7 2.0 %copy-start.4 = (bf16[256,1024]{1,0:T(8,128)(2,1)S(1)}, bf16[256,1024]{1,0:T(8,128)(2,1)}, u32[]{:S(2)}) copy-start(bf16[256,1024]{1,0:T(8,128)(2,1)} %param.29) | copy-start | bytes 1572868
  6.8 2.0 %copy-start.12 = (f32[256]{0:T(256)S(1)}, f32[256]{0:T(256)}, u32[]{:S(2)}) copy-start(f32[256]{0:T(256)} %param.36) | copy-start | bytes 3076
  6.8 7.3 %copy-start.8 = (s32[16,2]{0,1:T(2,128)S(1)}, s32[16,2]{0,1:T(2,128)}, u32[]{:S(2)}) copy-start(s32[16,2]{0,1:T(2,128)} %param.46) | copy-start | bytes 388
  6.8 13.6 %copy-start.9 = (f32[1024]{0:T(1024)S(1)}, f32[1024]{0:T(1024)}, u32[]{:S(2)}) copy-start(f32[1024]{0:T(1024)} %param.37) | copy-start | bytes 12292
  8.9 46.8 %copy-start.7 = (bf16[22,256]{1,0:T(8,128)(2,1)S(1)}, bf16[22,256]{1,0:T(8,128)(2,1)}, u32[]{:S(2)}) copy-start(bf16[22,256]{1,0:T(8,128)(2,1)} %param.43) | copy-start | bytes 33796
  9.6 10.4 %all-to-all-start = ((bf16[4,16,1024]{2,1,0:T(8,128)(2,1)}), bf16[4,16,1024]{2,1,0:T(8,128)(2,1)S(1)}, u32[]{:S(2)}, u32[]{:S(2)}) async-start(bf16[4,16,1024]{2,1,0:T(8,128)(2,1)} %broadcast_in_dim.18), calls=%async_computation | async-start | bytes 262144 | tf_op jit(solution)/shard_map/all_to_all | solution.py:20
  49.4 18.4 %all-to-all-start.2 = ((bf16[32,48,256]{2,1,0:T(8,128)(2,1)}), bf16[32,48,256]{2,1,0:T(8,128)(2,1)S(1)}, u32[]{:S(2)}, u32[]{:S(2)}) async-start(bf16[32,48,256]{2,1,0:T(8,128)(2,1)} %bitcast.10), calls=%async_computation.2 | async-start | bytes 1572864 | tf_op jit(solution)/shard_map/all_to_all | solution.py:28
  68.7 5.0 %copy-start.3 = (bf16[1,1024,352]{1,2,0:T(8,128)(2,1)S(1)}, bf16[1,1024,352]{1,2,0:T(8,128)(2,1)}, u32[]{:S(2)}) copy-start(bf16[1,1024,352]{1,2,0:T(8,128)(2,1)} %param.38) | copy-start | bytes 2162692
  68.7 43.7 %all-to-all-start.3 = ((bf16[64,36,128]{2,1,0:T(8,128)(2,1)}), bf16[64,36,128]{2,1,0:T(8,128)(2,1)S(1)}, u32[]{:S(2)}, u32[]{:S(2)}) async-start(bf16[64,36,128]{2,1,0:T(8,128)(2,1)} %bitcast.23), calls=%async_computation.3 | async-start | bytes 1310720 | tf_op jit(solution)/shard_map/all_to_all | solution.py:28
  114.0 8.1 %copy-start.10 = (bf16[1024]{0:T(1024)(128)(2,1)S(1)}, bf16[1024]{0:T(1024)(128)(2,1)}, u32[]{:S(2)}) copy-start(bf16[1024]{0:T(1024)(128)(2,1)} %param.44) | copy-start | bytes 6148
  114.0 8.1 %copy-start.13 = (f32[16,2]{0,1:T(2,128)S(1)}, f32[16,2]{0,1:T(2,128)}, u32[]{:S(2)}) copy-start(f32[16,2]{0,1:T(2,128)} %param.47) | copy-start | bytes 388
  115.0 19.9 %all-to-all-start.4 = ((bf16[32,48,256]{2,1,0:T(8,128)(2,1)}), bf16[32,48,256]{2,1,0:T(8,128)(2,1)S(1)}, u32[]{:S(2)}, u32[]{:S(2)}) async-start(bf16[32,48,256]{2,1,0:T(8,128)(2,1)} %bitcast.26), calls=%async_computation.4 | async-start | bytes 1572864 | tf_op jit(solution)/shard_map/all_to_all | solution.py:28
  122.3 38.1 %copy-start.14 = (f32[256]{0:T(256)S(1)}, f32[256]{0:T(256)}, u32[]{:S(2)}) copy-start(f32[256]{0:T(256)} %param.45) | copy-start | bytes 3076
  135.8 15.9 %all-to-all-start.5 = ((bf16[16,4,256]{2,1,0:T(4,128)(2,1)}), bf16[16,4,256]{2,1,0:T(4,128)(2,1)S(1)}, u32[]{:S(2)}, u32[]{:S(2)}) async-start(bf16[16,4,256]{2,1,0:T(4,128)(2,1)} %copy.103), calls=%async_computation.5 | async-start | bytes 65536 | tf_op jit(solution)/shard_map/all_to_all | solution.py:28

commit v2 on v1

--- a/solution.py
+++ b/solution.py
@@ -37,22 +37,14 @@
     return tuple(done)
 
 
-def plane_weights(dense_gate, dense_up, dense_down, quarter):
-    y = lax.axis_size("tp")
-    z = lax.axis_size("z")
-    tp_index = lax.axis_index("tp")
-    gate = lax.dynamic_slice_in_dim(dense_gate, tp_index * quarter, quarter, 1)
-    up = lax.dynamic_slice_in_dim(dense_up, tp_index * quarter, quarter, 1)
-    units = gate.shape[0]
-    part = -(-units // y)
-    three = jnp.stack([gate, up, dense_down])
-    three = jnp.pad(three, ((0, 0), (0, part * y - units), (0, 0)))
-    three = three.reshape(3, y, part, quarter).swapaxes(0, 1)
-    message = three.reshape(y, 3 * part * quarter // 128, 128)
-    outgoing = jnp.broadcast_to(message, (z, *message.shape)).reshape(z * y, *message.shape[1:])
-    arrived = exchange(outgoing, ("z", "tp"))
-    arrived = arrived.reshape(z, y, 3, part, quarter)
-    return arrived.transpose(2, 0, 3, 1, 4).reshape(3, z * part, y * quarter)
+def padded_units(columns, multiple):
+    return jnp.pad(columns, ((0, -columns.shape[0] % multiple), (0, 0)))
+
+
+def with_neighbour(units, step):
+    planes = lax.axis_size("z")
+    other = lax.ppermute(units, "z", [(i, i ^ step) for i in range(planes)])
+    return jnp.concatenate([units, other], 0)
 
 
 def time_mixer(
@@ -114,19 +106,14 @@
     return ((values - centre) * lax.rsqrt(spread + norm_epsilon) * gain).astype(jnp.bfloat16)
 
 
-def route_tables(routes, route_weights, experts, capacity):
+def route_targets(routes, experts, capacity):
     expert_hits = (
         routes[:, :, None] == jnp.arange(experts, dtype=jnp.int32)[None, None, :]
     ).astype(jnp.int32)
     row_hits = jnp.sum(expert_hits, 1, dtype=jnp.int32)
     earlier = jnp.cumsum(row_hits, 0, dtype=jnp.int32) - row_hits
     slot_index = jnp.sum(earlier[:, None, :] * expert_hits, 2, dtype=jnp.int32)
-    target = routes * capacity + slot_index
-    places = jnp.arange(experts * capacity, dtype=jnp.int32)
-    slot_match = target[:, :, None] == places[None, None, :]
-    dispatch_tokens = jnp.any(slot_match, 1).astype(jnp.bfloat16)
-    combine_experts = jnp.sum(jnp.where(slot_match, route_weights[:, :, None], 0.0), 1)
-    return (dispatch_tokens, combine_experts)
+    return routes * capacity + slot_index
 
 
 def shards(
@@ -163,7 +150,8 @@
     plane_blocks = lax.axis_size(("x", "c"))
     plane_size = lax.axis_size(PLANE)
     tp_size = lax.axis_size("tp")
-    weights = plane_weights(dense_gate, dense_up, dense_down, quarter)
+    shared = planes // tp_size
+    own_down = padded_units(dense_down, 8)
     partial_mix = time_mixer(
         tokens,
         state,
@@ -178,66 +166,117 @@
         rate_down,
         rate_up,
         head_gain,
-    )
-    mixed = of_everyone(partial_mix.astype(jnp.bfloat16), "tp")
+    ).astype(jnp.bfloat16)
+    message = jnp.concatenate(
+        [partial_mix[:, i * quarter : (i + 1) * quarter] for i in range(tp_size)]
+        + [own_down],
+        0,
+    )
+    everyone = sent_to_all(message, "tp")
+    mix_rows = tp_size * row_count
+    mixed = jnp.sum(everyone[:, :mix_rows].astype(jnp.float32), 0)
+    mixed = jnp.concatenate(
+        [mixed[i * row_count : (i + 1) * row_count] for i in range(tp_size)], 1
+    )
+    units = jnp.concatenate(
+        [padded_units(dense_gate, 8), padded_units(dense_up, 8)]
+        + [everyone[i, mix_rows:] for i in range(tp_size)],
+        1,
+    )
+    units = with_neighbour(units, 1)
     x_mid = first_norm(residual_scale * tokens.astype(jnp.float32) + mixed, first_gain)
     own_columns = lax.dynamic_slice_in_dim(x_mid, tp_index * quarter, quarter, 1)
     experts = lax.axis_size(EP) // SPLIT
     here = experts // planes
     capacity = min(row_count, max(2, 2 * row_count * routes.shape[1] // experts))
-    dispatch_tokens, combine_experts = route_tables(routes, route_weights, experts, capacity)
+    slots = here * capacity
+    part = row_count // shared
+    target = route_targets(routes, experts, capacity)
+    place = jnp.arange(planes * (slots + part), dtype=jnp.int32)
+    plane, inner = place // (slots + part), place % (slots + part)
+    routed_place = jnp.where(inner < slots, plane * slots + inner, -1)
+    dense_place = jnp.where(inner < slots, -1, plane % shared * part + inner - slots)
+    slot_match = target[:, :, None] == routed_place[None, None, :]
+    row_match = jnp.arange(row_count, dtype=jnp.int32)[:, None] == dense_place[None, :]
+    chosen = (jnp.any(slot_match, 1) | row_match).astype(jnp.bfloat16)
     packed_rows = lax.dot_general(
-        dispatch_tokens, own_columns, (((0,), (0,)), ((), ())), preferred_element_type=jnp.float32
+        chosen, own_columns, (((0,), (0,)), ((), ())), preferred_element_type=jnp.float32
     ).astype(jnp.bfloat16)
-    arrived = exchange(packed_rows.reshape(planes, here * capacity, quarter), "z")
+    arrived = exchange(packed_rows.reshape(planes, slots + part, quarter), "z")
+    arrived, units = lax.optimization_barrier((arrived, units))
+    units = with_neighbour(units, 2)
     rows = planes * capacity
-    arrived = arrived.reshape(planes, here, capacity, quarter).swapaxes(0, 1)
-    arrived = arrived.reshape(here, rows, quarter)
-    both = jnp.concatenate([arrived, jnp.broadcast_to(own_columns, (here, *own_columns.shape))], 1)
-    outgoing = jnp.repeat(both, plane_size // here, axis=0)
-    everything = exchange(outgoing, PLANE)
-    everything = everything.reshape(plane_blocks, tp_size, rows + row_count, quarter).swapaxes(1, 2)
-    everything = everything.reshape(plane_blocks, rows + row_count, model_width)
+    dense_count = shared * part
+    height = rows + dense_count
+    routed_rows = arrived[:, :slots].reshape(planes, here, capacity, quarter).swapaxes(0, 1)
+    routed_rows = routed_rows.reshape(here, 1, 1, rows, quarter)
+    dense_rows = arrived[:, slots:].reshape(1, 1, tp_size, dense_count, quarter)
+    wide = (here, plane_blocks // here, tp_size)
+    outgoing = jnp.concatenate(
+        [
+            jnp.broadcast_to(routed_rows, (*wide, rows, quarter)),
+            jnp.broadcast_to(dense_rows, (*wide, dense_count, quarter)),
+        ],
+        3,
+    )
+    everything = exchange(outgoing.reshape(plane_size, height, quarter), PLANE)
+    everything = everything.reshape(plane_blocks, tp_size, height, quarter).swapaxes(1, 2)
+    everything = everything.reshape(plane_blocks, height, model_width)
     flat_rows = everything[:, :rows].reshape(plane_blocks * rows, model_width)
-    dense_rows = everything[:, rows:].reshape(plane_blocks * row_count, model_width)
+    dense_rows = everything[:, rows:].reshape(plane_blocks * dense_count, model_width)
     gate_pre = jnp.dot(flat_rows, expert_gate[0], preferred_element_type=jnp.float32)
     up_pre = jnp.dot(flat_rows, expert_up[0], preferred_element_type=jnp.float32)
     hidden = (jax.nn.silu(gate_pre) * up_pre).astype(jnp.bfloat16)
     partial_out = jnp.dot(hidden, expert_down[0], preferred_element_type=jnp.float32)
     dense_pre = [
         lax.dot_general(
-            dense_rows, weights[i], (((1,), (1,)), ((), ())), preferred_element_type=jnp.float32
+            dense_rows,
+            units[:, i * model_width : (i + 1) * model_width],
+            (((1,), (1,)), ((), ())),
+            preferred_element_type=jnp.float32,
         )
         for i in range(2)
     ]
     dense_hidden = (jax.nn.silu(dense_pre[0]) * dense_pre[1]).astype(jnp.bfloat16)
-    dense_out = jnp.dot(dense_hidden, weights[2], preferred_element_type=jnp.float32)
-    returning = jnp.concatenate(
+    partial_out = partial_out.astype(jnp.bfloat16)
+    returning = jnp.stack(
         [
-            partial_out.astype(jnp.bfloat16).reshape(plane_blocks, rows, model_width),
-            dense_out.astype(jnp.bfloat16).reshape(plane_blocks, row_count, model_width),
+            jnp.concatenate(
+                [
+                    partial_out[:, i * quarter : (i + 1) * quarter].reshape(
+                        plane_blocks, rows, quarter
+                    ),
+                    jnp.dot(
+                        dense_hidden,
+                        units[:, 2 * model_width + i * quarter :][:, :quarter],
+                        preferred_element_type=jnp.float32,
+                    )
+                    .astype(jnp.bfloat16)
+                    .reshape(plane_blocks, dense_count, quarter),
+                ],
+                1,
+            )
+            for i in range(tp_size)
         ],
         1,
     )
-    returning = returning.reshape(plane_blocks, rows + row_count, tp_size, quarter).swapaxes(1, 2)
-    returned = exchange(returning.reshape(plane_size, rows + row_count, quarter), PLANE)
+    returned = exchange(returning.reshape(plane_size, height, quarter), PLANE)
     returned = returned.astype(jnp.float32)
-    dense_part = jnp.sum(returned[:, rows:], 0)
     summed = jnp.sum(returned[:, :rows].reshape(here, plane_size // here, rows, quarter), 1)
-    summed = summed.reshape(here, planes, capacity, quarter).swapaxes(0, 1).astype(jnp.bfloat16)
-    expert_out = exchange(summed.reshape(planes, here * capacity, quarter), "z")
-    expert_out = expert_out.reshape(experts * capacity, quarter).astype(jnp.float32)
-    routed_part = jnp.dot(
-        combine_experts,
-        expert_out,
+    summed = summed.reshape(here, planes, capacity, quarter).swapaxes(0, 1)
+    dense_sum = jnp.sum(
+        returned[:, rows:].reshape(plane_blocks, tp_size, dense_count, quarter), 0
+    ).reshape(planes, part, quarter)
+    back = jnp.concatenate([summed.reshape(planes, slots, quarter), dense_sum], 1)
+    back = exchange(back.astype(jnp.bfloat16), "z").reshape(planes * (slots + part), quarter)
+    branch = jax.nn.sigmoid(jnp.dot(x_mid, branch_gate, preferred_element_type=jnp.float32))
+    factors = jnp.sum(jnp.where(slot_match, route_weights[:, :, None], 0.0), 1)
+    factors = factors + jnp.where(row_match, branch[:, None], 0.0)
+    second_sum = residual_scale * own_columns.astype(jnp.float32) + jnp.dot(
+        factors,
+        back.astype(jnp.float32),
         precision=lax.Precision.HIGHEST,
         preferred_element_type=jnp.float32,
-    )
-    branch = jax.nn.sigmoid(jnp.dot(x_mid, branch_gate, preferred_element_type=jnp.float32))
-    second_sum = (
-        residual_scale * own_columns.astype(jnp.float32)
-        + routed_part
-        + branch[:, None] * dense_part
     )
     row_sums, square_sums = in_one(
         (jnp.sum(second_sum, 1), jnp.sum(second_sum * second_sum, 1)), "tp"

time: 162 us -> 132 us (0.81)
  waiting for transfers between devices: 78.5 us -> 46.7 us
  starting transfers between devices: 25.5 us -> 34.6 us
  blocking collectives: 35.8 us -> 27.6 us
    all_to_all x4 -> x3, waiting for transfers between devices: 72.9 us -> 25.8 us  [exchange(): return lax.all_to_all(parts, axis, split_axis=0, concat_axis=0, tiled=True)]
    ppermute x0 -> x2, waiting for transfers between devices: none -> 15.1 us  [with_neighbour(): other = lax.ppermute(units, 'z', [(i, i ^ step) for i in range(planes)])]
    all_to_all x1, blocking collectives: 27.6 us -> 20 us  [exchange(): return lax.all_to_all(parts, axis, split_axis=0, concat_axis=0, tiled=True)]
    ppermute x0 -> x2, starting transfers between devices: none -> 6.79 us  [with_neighbour(): other = lax.ppermute(units, 'z', [(i, i ^ step) for i in range(planes)])]
    all_to_all x4 -> x3, starting transfers between devices: 21 us -> 23.4 us  [exchange(): return lax.all_to_all(parts, axis, split_axis=0, concat_axis=0, tiled=True)]
    broadcast_in_dim x3 -> x4, local copies, waits for them, and re-layouts: 1.86 us -> 0.09 us  [the longest x2 0.06 us: shards(): jnp.broadcast_to(routed_rows, (*wide, rows, quarter))]
  transfers between devices with their start and end apart: 5 -> 6, of which waited for: 5 -> 4; matrix products, arithmetic and copies ran while one was open for 3% -> 2% of each run, Pallas kernels for 0% -> 0%
where the time goes in v2:
time: 132 us; the launch traced here: 131 us
  waiting for transfers between devices  46.7 us (35%)
  starting transfers between devices  34.6 us (26%)
  blocking collectives  27.6 us (21%)
  matrix products  13.3 us (10%)
  local copies, waits for them, and re-layouts  4.35 us (3%)
  other arithmetic  3.71 us (3%)
    all_to_all x3, waiting for transfers between devices, exchange(): return lax.all_to_all(parts, axis, split_axis=0, concat_axis=0, tiled=True)  25.8 us
    all_to_all x3, starting transfers between devices, exchange(): return lax.all_to_all(parts, axis, split_axis=0, concat_axis=0, tiled=True)  23.4 us
    all_to_all x1, blocking collectives, exchange(): return lax.all_to_all(parts, axis, split_axis=0, concat_axis=0, tiled=True)  20 us
    ppermute x2, waiting for transfers between devices, with_neighbour(): other = lax.ppermute(units, 'z', [(i, i ^ step) for i in range(planes)])  15.1 us
    all_to_all x1, blocking collectives, sent_to_all(): return lax.all_to_all(copies, axis, split_axis=0, concat_axis=0, tiled=True)  7.66 us
    ppermute x2, starting transfers between devices, with_neighbour(): other = lax.ppermute(units, 'z', [(i, i ^ step) for i in range(planes)])  6.79 us
    all_to_all x1, waiting for transfers between devices, sent_to_all(): return lax.all_to_all(copies, axis, split_axis=0, concat_axis=0, tiled=True)  5.77 us
    all_to_all x1, starting transfers between devices, sent_to_all(): return lax.all_to_all(copies, axis, split_axis=0, concat_axis=0, tiled=True)  4.46 us
  transfers between devices with their start and end apart: 6, of which 4 were waited for; matrix products, arithmetic and copies ran while one was open for 2% of the time, Pallas kernels for 0%

profile of v2, /device:TPU:2, one launch (start us, length us, event | category | flops | bytes accessed | tf_op | source)
XLA Modules:
  0.0 131.0 jit_solution(4823534398919487118)
XLA Ops:
  0.0 1.4 %fusion.69 = f32[16,256]{1,0:T(8,128)S(1)} fusion(bf16[16,1024]{1,0:T(8,128)(2,1)} %param.24, bf16[1024,256]{1,0:T(8,128)(2,1)} %param.27), kind=kOutput, calls=%fused_computation.146 | convolution fusion | flops 8388608 | bytes 573440 | tf_op jit(solution)/shard_map/dot_general | solution.py:71
  1.4 0.1 reshape.213
  1.5 0.1 multiply_reduce_fusion.2
  1.6 1.2 fusion.11
  2.8 0.1 reshape.214
  2.9 1.2 fusion.72
  4.1 0.7 reshape.241
  4.8 1.2 fusion.48
  6.0 0.7 mul.175
  6.7 1.2 fusion.71
  7.9 0.7 mul.185
  8.6 0.1 multiply_negate_fusion
  8.7 0.6 fusion.70
  9.4 0.0 copy-done.7
  9.4 0.0 copy-done.8
  9.4 0.0 copy-done.9
  9.5 1.5 %fusion = f32[16,4,1,64]{3,2,1,0:T(1,128)S(1)} fusion(f32[16,4,64,1]{2,3,1,0:T(1,128)S(1)} %bitcast.140, f32[16,4,64,64]{3,2,1,0:T(8,128)S(1)} %copy-done.2, f32[16,4,64]{2,1,0:T(4,128)S(1)} %reshape.213, f32[16,4,64]{2,1,0:T(4,128)S(1)} %copy-done.9, f32[16,4,64]{2,1,0:T(4,128)S(1)} %get-tuple-element.20, f32[16,4,64]{2,1,0:T(4,128)S(1)} %bitcast.139, ...), kind=kOutput, calls=%fused_computation | convolution fusion | flops 1835008 | bytes 1163264 | tf_op jit(solution)/shard_map/bhij,bhj->bhi/dot_general | solution.py:94
  10.9 0.1 reduce_sum.127
  11.1 0.2 multiply_reduce_fusion.1
  11.2 0.1 subtract_multiply_fusion
  11.3 0.1 reshape.216
  11.4 0.9 convolution_convert_fusion.6
  12.3 0.7 broadcast_in_dim.32
  13.0 4.5 %all-to-all-start = ((bf16[4,88,256]{2,1,0:T(8,128)(2,1)}), bf16[4,88,256]{2,1,0:T(8,128)(2,1)S(1)}, u32[]{:S(2)}, u32[]{:S(2)}) async-start(bf16[4,88,256]{2,1,0:T(8,128)(2,1)} %broadcast_in_dim.32), calls=%async_computation | async-start | bytes 360448 | tf_op jit(solution)/shard_map/all_to_all | solution.py:20
  17.5 0.1 convert_reduce_fusion.1
  17.6 0.2 select_reduce_fusion
  17.9 0.1 compare_reduce_fusion
  18.0 5.8 %all-to-all-done = bf16[4,88,256]{2,1,0:T(8,128)(2,1)S(1)} async-done(((bf16[4,88,256]{2,1,0:T(8,128)(2,1)}), bf16[4,88,256]{2,1,0:T(8,128)(2,1)S(1)}, u32[]{:S(2)}, u32[]{:S(2)}) %all-to-all-start) | async-done | bytes 180256 | tf_op jit(solution)/shard_map/all_to_all | solution.py:20
  23.8 3.8 %collective-permute-start = (bf16[24,3072]{1,0:T(8,128)(2,1)S(1)}, bf16[24,3072]{1,0:T(8,128)(2,1)S(1)}, u32[]{:S(2)}, u32[]{:S(2)}) collective-permute-start(bf16[24,3072]{1,0:T(8,128)(2,1)S(1)} %constant_dynamic-update-slice_fusion.5), channel_id=1, source_target_pairs={{0,32},{32,0},{64,96},{96,64},{128,160},{160,128},{192,224},{224,1... | collective-permute-start | bytes 442376 | tf_op jit(solution)/shard_map/ppermute | solution.py:46
  27.6 0.1 fusion.65
  27.8 0.2 multiply_reduce_fusion
  28.0 0.1 multiply_convert_fusion
  28.1 0.8 fusion.7
  28.9 14.3 %all-to-all-start.1 = ((bf16[16,8,256]{2,1,0:T(8,128)(2,1)}), bf16[16,8,256]{2,1,0:T(8,128)(2,1)S(1)}, u32[]{:S(2)}, u32[]{:S(2)}) async-start(bf16[16,8,256]{2,1,0:T(8,128)(2,1)} %fusion.7), calls=%async_computation.1 | async-start | bytes 131072 | tf_op jit(solution)/shard_map/all_to_all | solution.py:28
  43.3 12.8 %all-to-all-done.1 = bf16[16,8,256]{2,1,0:T(8,128)(2,1)S(1)} async-done(((bf16[16,8,256]{2,1,0:T(8,128)(2,1)}), bf16[16,8,256]{2,1,0:T(8,128)(2,1)S(1)}, u32[]{:S(2)}, u32[]{:S(2)}) %all-to-all-start.1) | async-done | bytes 65568 | tf_op jit(solution)/shard_map/all_to_all | solution.py:28
  56.2 0.1 broadcast_in_dim.42
  56.3 0.9 pad_maximum_fusion
  57.2 5.6 %all-to-all-start.2 = ((bf16[32,48,256]{2,1,0:T(8,128)(2,1)}), bf16[32,48,256]{2,1,0:T(8,128)(2,1)S(1)}, u32[]{:S(2)}, u32[]{:S(2)}) async-start(bf16[32,48,256]{2,1,0:T(8,128)(2,1)} %bitcast.16), calls=%async_computation.2 | async-start | bytes 1572864 | tf_op jit(solution)/shard_map/all_to_all | solution.py:28
  62.9 3.0 %collective-permute-start.1 = (bf16[48,3072]{1,0:T(8,128)(2,1)S(1)}, bf16[48,3072]{1,0:T(8,128)(2,1)S(1)}, u32[]{:S(2)}, u32[]{:S(2)}) collective-permute-start(bf16[48,3072]{1,0:T(8,128)(2,1)S(1)} %pad_maximum_fusion.2), channel_id=1, source_target_pairs={{0,64},{32,96},{64,0},{96,32},{128,192},{160,224},{192,128},{224,1... | collective-permute-start | bytes 884744 | tf_op jit(solution)/shard_map/ppermute | solution.py:46
  65.9 15.1 %collective-permute-done.1 = bf16[48,3072]{1,0:T(8,128)(2,1)S(1)} collective-permute-done((bf16[48,3072]{1,0:T(8,128)(2,1)S(1)}, bf16[48,3072]{1,0:T(8,128)(2,1)S(1)}, u32[]{:S(2)}, u32[]{:S(2)}) %collective-permute-start.1) | collective-permute-done | bytes 294944 | tf_op jit(solution)/shard_map/ppermute | solution.py:46
  81.0 0.1 copy.103
  81.2 0.2 fusion.35
  81.4 0.2 multiply_convert_fusion.1
  81.6 0.2 convolution_convert_fusion.3
  81.8 0.2 convolution_convert_fusion.4
  82.0 0.1 slice.144
  82.1 0.2 convolution_convert_fusion.1
  82.3 0.2 convolution_convert_fusion.2
  82.5 0.4 fusion.26
  82.9 1.2 convolution_convert_fusion
  84.2 0.1 pad_maximum_fusion.1
  84.3 20.0 %all_to_all.31 = bf16[32,48,256]{2,1,0:T(8,128)(2,1)S(1)} all-to-all(bf16[32,48,256]{2,1,0:T(8,128)(2,1)S(1)} %bitcast.117), channel_id=1, replica_groups=mesh['z'=16,'x'=4,'c'=2,'tp'=4] {'x','c','tp'}, dimensions={0} | all-to-all | bytes 1572864 | tf_op jit(solution)/shard_map/all_to_all | solution.py:28
  104.3 0.2 convert_element_type.82
  104.5 0.1 bitcast_reduce_fusion
  104.8 0.6 copy.95
  105.4 3.5 %all-to-all-start.4 = ((bf16[16,8,256]{2,1,0:T(8,128)(2,1)}), bf16[16,8,256]{2,1,0:T(8,128)(2,1)S(1)}, u32[]{:S(2)}, u32[]{:S(2)}) async-start(bf16[16,8,256]{2,1,0:T(8,128)(2,1)} %copy.95), calls=%async_computation.4 | async-start | bytes 131072 | tf_op jit(solution)/shard_map/all_to_all | solution.py:28
  109.0 0.1 fusion.43
  109.0 0.1 fusion.17
  109.2 13.0 %all-to-all-done.4 = bf16[16,8,256]{2,1,0:T(8,128)(2,1)S(1)} async-done(((bf16[16,8,256]{2,1,0:T(8,128)(2,1)}), bf16[16,8,256]{2,1,0:T(8,128)(2,1)S(1)}, u32[]{:S(2)}, u32[]{:S(2)}) %all-to-all-start.4) | async-done | bytes 65568 | tf_op jit(solution)/shard_map/all_to_all | solution.py:28
  122.2 0.3 fusion.66
  122.5 0.1 pad_maximum_fusion.4
  122.6 7.7 %all_to_all.32 = f32[4,1,32]{2,1,0:T(1,128)S(1)} all-to-all(f32[4,1,32]{2,1,0:T(1,128)S(1)} %broadcast_in_dim.49), channel_id=1, replica_groups=mesh['z'=16,'x'=4,'c'=2,'tp'=4] {'tp'}, dimensions={0} | all-to-all | bytes 1024 | tf_op jit(solution)/shard_map/all_to_all | solution.py:20
  130.2 0.1 slice_multiply_fusion
  130.3 0.7 multiply_convert_fusion.2
  (80 shorter events, 0.7 us)
Async XLA Ops:
  0.0 82.9 %copy-start = (bf16[1,352,1024]{2,1,0:T(8,128)(2,1)S(1)}, bf16[1,352,1024]{2,1,0:T(8,128)(2,1)}, u32[]{:S(2)}) copy-start(bf16[1,352,1024]{2,1,0:T(8,128)(2,1)} %param.40) | copy-start | bytes 2162692
  0.0 8.7 %copy-start.2 = (f32[16,4,64,64]{3,2,1,0:T(8,128)S(1)}, f32[16,4,64,64]{3,2,1,0:T(8,128)}, u32[]{:S(2)}) copy-start(f32[16,4,64,64]{3,2,1,0:T(8,128)} %param.25) | copy-start | bytes 3145732
  8.6 0.8 copy-start.7
  8.6 0.8 copy-start.8
  8.6 0.8 copy-start.9
  9.4 2.1 %copy-start.4 = (bf16[256,1024]{1,0:T(8,128)(2,1)S(1)}, bf16[256,1024]{1,0:T(8,128)(2,1)}, u32[]{:S(2)}) copy-start(bf16[256,1024]{1,0:T(8,128)(2,1)} %param.29) | copy-start | bytes 1572868
  9.4 2.9 %copy-start.10 = (bf16[22,256]{1,0:T(8,128)(2,1)S(1)}, bf16[22,256]{1,0:T(8,128)(2,1)}, u32[]{:S(2)}) copy-start(bf16[22,256]{1,0:T(8,128)(2,1)} %param.43) | copy-start | bytes 33796
  9.4 8.1 %copy-start.5 = (bf16[22,1024]{1,0:T(8,128)(2,1)S(1)}, bf16[22,1024]{1,0:T(8,128)(2,1)}, u32[]{:S(2)}) copy-start(bf16[22,1024]{1,0:T(8,128)(2,1)} %param.41) | copy-start | bytes 135172
  9.4 8.1 %copy-start.11 = (s32[16,2]{0,1:T(2,128)S(1)}, s32[16,2]{0,1:T(2,128)}, u32[]{:S(2)}) copy-start(s32[16,2]{0,1:T(2,128)} %param.46) | copy-start | bytes 388
  9.4 8.4 %copy-start.6 = (bf16[22,1024]{1,0:T(8,128)(2,1)S(1)}, bf16[22,1024]{1,0:T(8,128)(2,1)}, u32[]{:S(2)}) copy-start(bf16[22,1024]{1,0:T(8,128)(2,1)} %param.42) | copy-start | bytes 135172
  9.5 18.2 %copy-start.1 = (bf16[16,1024]{1,0:T(8,128)(2,1)S(1)}, bf16[16,1024]{1,0:T(8,128)(2,1)}, u32[]{:S(2)}) copy-start(bf16[16,1024]{1,0:T(8,128)(2,1)} %param.24) | copy-start | bytes 98308
  10.9 17.0 %copy-start.12 = (f32[1024]{0:T(1024)S(1)}, f32[1024]{0:T(1024)}, u32[]{:S(2)}) copy-start(f32[1024]{0:T(1024)} %param.37) | copy-start | bytes 12292
  13.0 10.7 %all-to-all-start = ((bf16[4,88,256]{2,1,0:T(8,128)(2,1)}), bf16[4,88,256]{2,1,0:T(8,128)(2,1)S(1)}, u32[]{:S(2)}, u32[]{:S(2)}) async-start(bf16[4,88,256]{2,1,0:T(8,128)(2,1)} %broadcast_in_dim.32), calls=%async_computation | async-start | bytes 360448 | tf_op jit(solution)/shard_map/all_to_all | solution.py:20
  23.8 19.5 %collective-permute-start = (bf16[24,3072]{1,0:T(8,128)(2,1)S(1)}, bf16[24,3072]{1,0:T(8,128)(2,1)S(1)}, u32[]{:S(2)}, u32[]{:S(2)}) collective-permute-start(bf16[24,3072]{1,0:T(8,128)(2,1)S(1)} %constant_dynamic-update-slice_fusion.5), channel_id=1, source_target_pairs={{0,32},{32,0},{64,96},{96,64},{128,160},{160,128},{192,224},{224,1... | collective-permute-start | bytes 442376 | tf_op jit(solution)/shard_map/ppermute | solution.py:46
  28.9 27.2 %all-to-all-start.1 = ((bf16[16,8,256]{2,1,0:T(8,128)(2,1)}), bf16[16,8,256]{2,1,0:T(8,128)(2,1)S(1)}, u32[]{:S(2)}, u32[]{:S(2)}) async-start(bf16[16,8,256]{2,1,0:T(8,128)(2,1)} %fusion.7), calls=%async_computation.1 | async-start | bytes 131072 | tf_op jit(solution)/shard_map/all_to_all | solution.py:28
  57.2 23.8 %all-to-all-start.2 = ((bf16[32,48,256]{2,1,0:T(8,128)(2,1)}), bf16[32,48,256]{2,1,0:T(8,128)(2,1)S(1)}, u32[]{:S(2)}, u32[]{:S(2)}) async-start(bf16[32,48,256]{2,1,0:T(8,128)(2,1)} %bitcast.16), calls=%async_computation.2 | async-start | bytes 1572864 | tf_op jit(solution)/shard_map/all_to_all | solution.py:28
  62.9 18.1 %collective-permute-start.1 = (bf16[48,3072]{1,0:T(8,128)(2,1)S(1)}, bf16[48,3072]{1,0:T(8,128)(2,1)S(1)}, u32[]{:S(2)}, u32[]{:S(2)}) collective-permute-start(bf16[48,3072]{1,0:T(8,128)(2,1)S(1)} %pad_maximum_fusion.2), channel_id=1, source_target_pairs={{0,64},{32,96},{64,0},{96,32},{128,192},{160,224},{192,128},{224,1... | collective-permute-start | bytes 884744 | tf_op jit(solution)/shard_map/ppermute | solution.py:46
  81.0 1.5 %copy-start.3 = (bf16[1,1024,352]{1,2,0:T(8,128)(2,1)S(1)}, bf16[1,1024,352]{1,2,0:T(8,128)(2,1)}, u32[]{:S(2)}) copy-start(bf16[1,1024,352]{1,2,0:T(8,128)(2,1)} %param.38) | copy-start | bytes 2162692
  81.2 1.8 %copy-start.16 = (bf16[1,1024,352]{1,2,0:T(8,128)(2,1)S(1)}, bf16[1,1024,352]{1,2,0:T(8,128)(2,1)}, u32[]{:S(2)}) copy-start(bf16[1,1024,352]{1,2,0:T(8,128)(2,1)} %param.39) | copy-start | bytes 2162692
  104.5 4.5 %copy-start.14 = (f32[16,2]{0,1:T(2,128)S(1)}, f32[16,2]{0,1:T(2,128)}, u32[]{:S(2)}) copy-start(f32[16,2]{0,1:T(2,128)} %param.47) | copy-start | bytes 388
  104.5 4.5 %copy-start.13 = (bf16[1024]{0:T(1024)(128)(2,1)S(1)}, bf16[1024]{0:T(1024)(128)(2,1)}, u32[]{:S(2)}) copy-start(bf16[1024]{0:T(1024)(128)(2,1)} %param.44) | copy-start | bytes 6148
  104.5 25.8 %copy-start.15 = (f32[256]{0:T(256)S(1)}, f32[256]{0:T(256)}, u32[]{:S(2)}) copy-start(f32[256]{0:T(256)} %param.45) | copy-start | bytes 3076
  105.4 16.7 %all-to-all-start.4 = ((bf16[16,8,256]{2,1,0:T(8,128)(2,1)}), bf16[16,8,256]{2,1,0:T(8,128)(2,1)S(1)}, u32[]{:S(2)}, u32[]{:S(2)}) async-start(bf16[16,8,256]{2,1,0:T(8,128)(2,1)} %copy.95), calls=%async_computation.4 | async-start | bytes 131072 | tf_op jit(solution)/shard_map/all_to_all | solution.py:28

commit v3 on v2

--- a/solution.py
+++ b/solution.py
@@ -1,8 +1,13 @@
+import math
+
 import jax
 import jax.numpy as jnp
 from jax import lax
+from jax.experimental import pallas as pl
+from jax.experimental.pallas import tpu as pltpu
 from jax.sharding import Mesh
 from jax.sharding import PartitionSpec as P
+
 
 SPLIT = 4
 EP = ("z", "x", "c")
@@ -47,7 +52,135 @@
     return jnp.concatenate([units, other], 0)
 
 
-def time_mixer(
+def mixer_kernel(
+    tokens_ref,
+    down_ref,
+    decay_base_ref,
+    decay_up_ref,
+    rate_base_ref,
+    rate_up_ref,
+    head_gain_ref,
+    decay_down_any,
+    rate_down_any,
+    w_key_any,
+    w_recep_any,
+    w_value_any,
+    state_any,
+    w_out_any,
+    message_ref,
+    decay_down_ref,
+    rate_down_ref,
+    w_key_ref,
+    w_recep_ref,
+    w_value_ref,
+    state_ref,
+    w_out_ref,
+    query_ref,
+    answer_ref,
+    arrival,
+):
+    copies = []
+    for source, target in (
+        (decay_down_any, decay_down_ref),
+        (rate_down_any, rate_down_ref),
+        (w_key_any, w_key_ref),
+        (w_recep_any, w_recep_ref),
+        (w_value_any, w_value_ref),
+        (state_any, state_ref),
+        (w_out_any, w_out_ref),
+    ):
+        copies.append(pltpu.make_async_copy(source, target, arrival.at[len(copies)]))
+    for copy in copies:
+        copy.start()
+    row_count, heads, head_size = state_ref.shape[0], state_ref.shape[1], state_ref.shape[3]
+    width = heads * head_size
+    tokens = tokens_ref[...]
+    f32 = jnp.float32
+
+    def turned(a, b):
+        return lax.dot_general(a, b, (((1,), (1,)), ((), ())), preferred_element_type=f32)
+
+    channel_head = lax.broadcasted_iota(jnp.int32, (width, width), 0) // head_size
+    same_head = (
+        channel_head == lax.broadcasted_iota(jnp.int32, (width, width), 1) // head_size
+    ).astype(f32)
+
+    def over_head(values):
+        return jnp.dot(
+            values, same_head, precision=lax.Precision.HIGHEST, preferred_element_type=f32
+        )
+
+    copies[0].wait()
+    decay_low = jnp.tanh(turned(tokens, decay_down_ref[...])).astype(jnp.bfloat16)
+    copies[1].wait()
+    rate_low = turned(tokens, rate_down_ref[...]).astype(jnp.bfloat16)
+    decay_pre = decay_base_ref[...] + jnp.dot(
+        decay_low, decay_up_ref[...], preferred_element_type=f32
+    )
+    decay = jnp.exp(-(math.exp(-0.5) * jax.nn.sigmoid(decay_pre)))
+    in_rate = jax.nn.sigmoid(
+        rate_base_ref[...] + jnp.dot(rate_low, rate_up_ref[...], preferred_element_type=f32)
+    )
+    copies[2].wait()
+    key_vecs = jnp.dot(tokens, w_key_ref[...], preferred_element_type=f32)
+    copies[3].wait()
+    recep = jnp.dot(tokens, w_recep_ref[...], preferred_element_type=f32)
+    sums = over_head(
+        jnp.concatenate([key_vecs * key_vecs, key_vecs * in_rate * recep, key_vecs * recep], 0)
+    )
+    scale = lax.rsqrt(sums[:row_count] + key_epsilon)
+    removed_factor = scale * sums[row_count : 2 * row_count]
+    value_factor = sums[2 * row_count :]
+    for which, vectors in enumerate((decay * recep, key_vecs * scale)):
+        for h in range(heads):
+            pair = vectors[:, h // 2 * 128 : h // 2 * 128 + 128]
+            query_ref[pl.ds(which * heads + h, row_count, stride=2 * heads), :] = (
+                pair if h % 2 == 0 else pltpu.roll(pair, head_size, 1)
+            )
+    copies[4].wait()
+    value_vecs = jnp.dot(tokens, w_value_ref[...], preferred_element_type=f32)
+    copies[5].wait()
+    for t in range(row_count):
+        queries = query_ref[2 * heads * t : 2 * heads * (t + 1), :head_size].astype(jnp.bfloat16)
+        matrix = state_ref[t].reshape(width, head_size).astype(jnp.bfloat16)
+        answers = turned(queries, matrix)
+        for pair in range(heads // 2):
+            answer_ref[pair, 2 * heads * t : 2 * heads * (t + 1), :] = answers[
+                :, pair * 128 : (pair + 1) * 128
+            ]
+    first_of_pair = lax.broadcasted_iota(jnp.int32, (row_count, 128), 1) < head_size
+
+    def picked(which):
+        pairs = []
+        for pair in range(heads // 2):
+            of_pair = answer_ref.at[pair]
+            rows = [
+                of_pair[pl.ds(which * heads + 2 * pair + i, row_count, stride=2 * heads), :]
+                for i in range(2)
+            ]
+            pairs.append(jnp.where(first_of_pair, rows[0], rows[1]))
+        return jnp.concatenate(pairs, 1)
+
+    read_out = picked(0) - picked(1) * removed_factor + value_vecs * value_factor
+    centred = read_out - over_head(read_out) * (1.0 / head_size)
+    spread = over_head(centred * centred) * (1.0 / head_size)
+    normed = centred * lax.rsqrt(spread + head_epsilon) * head_gain_ref[...]
+    copies[6].wait()
+    mixed = jnp.dot(normed.astype(jnp.bfloat16), w_out_ref[...], preferred_element_type=f32)
+    mixed = mixed.astype(jnp.bfloat16)
+    copies_out, mix_rows = message_ref.shape[0], row_count * heads
+    for c in range(copies_out):
+        for h in range(mixed.shape[1] // width):
+            message_ref[c, h * row_count : (h + 1) * row_count, :] = mixed[
+                :, h * width : (h + 1) * width
+            ]
+        message_ref[c, mix_rows:, :] = jnp.zeros_like(message_ref[c, mix_rows:, :])
+        message_ref[c, mix_rows : mix_rows + down_ref.shape[0], :] = down_ref[...]
+
+
+def mixer_message(
+    copies_out,
+    own_down,
     tokens,
     state,
     w_recep,
@@ -62,42 +195,34 @@
     rate_up,
     head_gain,
 ):
-    row_count = tokens.shape[0]
-    head_count = state.shape[1]
-    head_size = state.shape[3]
-    recep = jnp.dot(tokens, w_recep, preferred_element_type=jnp.float32).reshape(
-        row_count, head_count, head_size
-    )
-    key_vecs = jnp.dot(tokens, w_key, preferred_element_type=jnp.float32).reshape(
-        row_count, head_count, head_size
-    )
-    value_vecs = jnp.dot(tokens, w_value, preferred_element_type=jnp.float32).reshape(
-        row_count, head_count, head_size
-    )
-    decay_low = jnp.tanh(jnp.dot(tokens, decay_down, preferred_element_type=jnp.float32)).astype(
-        jnp.bfloat16
-    )
-    decay_pre = decay_base + jnp.dot(decay_low, decay_up, preferred_element_type=jnp.float32)
-    log_rate = -jax.nn.softplus(-decay_pre) - 0.5
-    decay = jnp.exp(-jnp.exp(log_rate)).reshape(row_count, head_count, head_size)
-    rate_low = jnp.dot(tokens, rate_down, preferred_element_type=jnp.float32).astype(jnp.bfloat16)
-    in_rate = jax.nn.sigmoid(
-        rate_base + jnp.dot(rate_low, rate_up, preferred_element_type=jnp.float32)
-    ).reshape(row_count, head_count, head_size)
-    unit_keys = key_vecs * lax.rsqrt(jnp.sum(key_vecs * key_vecs, -1, keepdims=True) + key_epsilon)
-    removed = jnp.einsum("bhij,bhj->bhi", state, -unit_keys)
-    updated = (
-        state * decay[:, :, None, :]
-        + removed[..., None] * (unit_keys * in_rate)[:, :, None, :]
-        + value_vecs[..., None] * key_vecs[:, :, None, :]
-    )
-    read_out = jnp.einsum("bhij,bhj->bhi", updated, recep)
-    centre = jnp.mean(read_out, -1, keepdims=True)
-    spread = jnp.mean(jnp.square(read_out - centre), -1, keepdims=True)
-    normed = ((read_out - centre) * lax.rsqrt(spread + head_epsilon)).reshape(
-        row_count, head_count * head_size
-    ) * head_gain
-    return jnp.dot(normed.astype(jnp.bfloat16), w_out, preferred_element_type=jnp.float32)
+    row_count, heads, head_size = state.shape[0], state.shape[1], state.shape[3]
+    width = heads * head_size
+    here = [
+        tokens,
+        own_down,
+        decay_base[None],
+        decay_up,
+        rate_base[None],
+        rate_up,
+        head_gain[None],
+    ]
+    far = [decay_down.T, rate_down.T, w_key, w_recep, w_value, state, w_out]
+    down_rows = own_down.shape[0] + -own_down.shape[0] % 8
+    rows = tokens.shape[1] // width * row_count + down_rows
+    return pl.pallas_call(
+        mixer_kernel,
+        out_shape=jax.ShapeDtypeStruct((copies_out, rows, width), jnp.bfloat16),
+        in_specs=[pl.BlockSpec(memory_space=pltpu.VMEM)] * len(here)
+        + [pl.BlockSpec(memory_space=pl.ANY)] * len(far),
+        out_specs=pl.BlockSpec(memory_space=pltpu.VMEM),
+        scratch_shapes=[pltpu.VMEM(a.shape, a.dtype) for a in far]
+        + [
+            pltpu.VMEM((2 * heads * row_count, 128), jnp.float32),
+            pltpu.VMEM((heads // 2, 2 * heads * row_count, 128), jnp.float32),
+            pltpu.SemaphoreType.DMA((len(far),)),
+        ],
+        name="mixer",
+    )(*here, *far)
 
 
 def first_norm(values, gain):
@@ -151,8 +276,9 @@
     plane_size = lax.axis_size(PLANE)
     tp_size = lax.axis_size("tp")
     shared = planes // tp_size
-    own_down = padded_units(dense_down, 8)
-    partial_mix = time_mixer(
+    message = mixer_message(
+        tp_size,
+        dense_down,
         tokens,
         state,
         w_recep,
@@ -166,13 +292,8 @@
         rate_down,
         rate_up,
         head_gain,
-    ).astype(jnp.bfloat16)
-    message = jnp.concatenate(
-        [partial_mix[:, i * quarter : (i + 1) * quarter] for i in range(tp_size)]
-        + [own_down],
-        0,
-    )
-    everyone = sent_to_all(message, "tp")
+    )
+    everyone = exchange(message, "tp")
     mix_rows = tp_size * row_count
     mixed = jnp.sum(everyone[:, :mix_rows].astype(jnp.float32), 0)
     mixed = jnp.concatenate(
@@ -183,6 +304,7 @@
         + [everyone[i, mix_rows:] for i in range(tp_size)],
         1,
     )
+    units = with_neighbour(units, 2)
     units = with_neighbour(units, 1)
     x_mid = first_norm(residual_scale * tokens.astype(jnp.float32) + mixed, first_gain)
     own_columns = lax.dynamic_slice_in_dim(x_mid, tp_index * quarter, quarter, 1)
@@ -203,8 +325,6 @@
         chosen, own_columns, (((0,), (0,)), ((), ())), preferred_element_type=jnp.float32
     ).astype(jnp.bfloat16)
     arrived = exchange(packed_rows.reshape(planes, slots + part, quarter), "z")
-    arrived, units = lax.optimization_barrier((arrived, units))
-    units = with_neighbour(units, 2)
     rows = planes * capacity
     dense_count = shared * part
     height = rows + dense_count

time: 132 us -> 117 us (0.89)
  matrix products: 13.3 us -> 5.2 us
  waiting for transfers between devices: 46.7 us -> 39.2 us
  Pallas kernels: 0 us -> 5.28 us
  local copies, waits for them, and re-layouts: 4.35 us -> 1.77 us
  blocking collectives: 27.6 us -> 26.1 us
    dot_general x8 -> x0, matrix products: 9.21 us -> none  [the longest x1 1.47 us: time_mixer(): read_out = jnp.einsum('bhij,bhj->bhi', updated, recep)]
    ppermute x2, waiting for transfers between devices: 15.1 us -> 9 us  [with_neighbour(): other = lax.ppermute(units, 'z', [(i, i ^ step) for i in range(planes)])]
    all_to_all x1 -> x0, waiting for transfers between devices: 5.77 us -> none  [sent_to_all(): return lax.all_to_all(copies, axis, split_axis=0, concat_axis=0, tiled=True)]
    all_to_all x3 -> x4, starting transfers between devices: 23.4 us -> 28.9 us  [exchange(): return lax.all_to_all(parts, axis, split_axis=0, concat_axis=0, tiled=True)]
    pallas_call x0 -> x1, Pallas kernels: none -> 5.28 us  [mixer_message(): pl.pallas_call(mixer_kernel, out_shape=jax.ShapeDtypeStruct((copies_out,...]
    all_to_all x1 -> x0, starting transfers between devices: 4.46 us -> none  [sent_to_all(): return lax.all_to_all(copies, axis, split_axis=0, concat_axis=0, tiled=True)]
    all_to_all x3 -> x4, waiting for transfers between devices: 25.8 us -> 30.2 us  [exchange(): return lax.all_to_all(parts, axis, split_axis=0, concat_axis=0, tiled=True)]
    all_to_all x1, blocking collectives: 20 us -> 18.2 us  [exchange(): return lax.all_to_all(parts, axis, split_axis=0, concat_axis=0, tiled=True)]
  transfers between devices with their start and end apart: 6 -> 6, of which waited for: 4 -> 5; matrix products, arithmetic and copies ran while one was open for 2% -> 2% of each run, Pallas kernels for 0% -> 0%
where the time goes in v3:
time: 117 us
  waiting for transfers between devices  39.2 us (34%)
  starting transfers between devices  35.6 us (30%)
  blocking collectives  26.1 us (22%)
  Pallas kernels  5.28 us (5%)
  matrix products  5.2 us (4%)
  other arithmetic  3.21 us (3%)
  local copies, waits for them, and re-layouts  1.77 us (2%)
    all_to_all x4, waiting for transfers between devices, exchange(): return lax.all_to_all(parts, axis, split_axis=0, concat_axis=0, tiled=True)  30.2 us
    all_to_all x4, starting transfers between devices, exchange(): return lax.all_to_all(parts, axis, split_axis=0, concat_axis=0, tiled=True)  28.9 us
    all_to_all x1, blocking collectives, exchange(): return lax.all_to_all(parts, axis, split_axis=0, concat_axis=0, tiled=True)  18.2 us
    ppermute x2, waiting for transfers between devices, with_neighbour(): other = lax.ppermute(units, 'z', [(i, i ^ step) for i in range(planes)])  9 us
    all_to_all x1, blocking collectives, sent_to_all(): return lax.all_to_all(copies, axis, split_axis=0, concat_axis=0, tiled=True)  7.92 us
    ppermute x2, starting transfers between devices, with_neighbour(): other = lax.ppermute(units, 'z', [(i, i ^ step) for i in range(planes)])  6.65 us
    pallas_call x1, Pallas kernels, mixer_message(): pl.pallas_call(mixer_kernel, out_shape=jax.ShapeDtypeStruct((copies_out,...  5.28 us
  transfers between devices with their start and end apart: 6, of which 5 were waited for; matrix products, arithmetic and copies ran while one was open for 2% of the time, Pallas kernels for 0%

profile of v3, /device:TPU:2, one launch (start us, length us, event | category | flops | bytes accessed | tf_op | source)
XLA Modules:
  0.0 116.8 jit_solution(4229501523739261606)
XLA Ops:
  0.0 0.0 copy-start
  0.0 0.0 copy-start.5
  0.0 0.0 copy-start.3
  0.0 0.0 copy-start.4
  0.0 0.0 copy-start.2
  0.0 0.0 copy-start.6
  0.0 5.3 %mixer.1 = bf16[4,88,256]{2,1,0:T(8,128)(2,1)} custom-call(bf16[16,1024]{1,0:T(8,128)(2,1)} %tokens_ref.1, bf16[22,256]{1,0:T(8,128)(2,1)} %down_ref.1, f32[1,256]{1,0:T(1,128)} %bitcast.119, bf16[64,256]{1,0:T(8,128)(2,1)} %decay_up_ref.1, f32[1,256]{1,0:T(1,128)} %bitcast.120, bf16[64,256]{1,0:T(8,128)(2,1)} %rate_up_ref.1, f32[1,256]{1,0:T(1,128)} %bitcast.121, ...), custom_call_target="tpu_custom_call" | custom-call | tf_op jit(solution)/shard_map/mixer/pallas_call | solution.py:212
  5.3 4.5 %all-to-all-start = ((bf16[4,88,256]{2,1,0:T(8,128)(2,1)}), bf16[4,88,256]{2,1,0:T(8,128)(2,1)S(1)}, u32[]{:S(2)}, u32[]{:S(2)}) async-start(bf16[4,88,256]{2,1,0:T(8,128)(2,1)} %mixer.1), calls=%async_computation | async-start | bytes 360448 | tf_op jit(solution)/shard_map/all_to_all | solution.py:33
  9.8 0.0 copy-done.5
  9.8 0.1 convert_reduce_fusion.1
  9.9 0.2 select_reduce_fusion
  10.1 0.0 copy-done.3
  10.2 0.0 copy-done.4
  10.2 0.1 compare_reduce_fusion
  10.3 5.8 %all-to-all-done = bf16[4,88,256]{2,1,0:T(8,128)(2,1)S(1)} async-done(((bf16[4,88,256]{2,1,0:T(8,128)(2,1)}), bf16[4,88,256]{2,1,0:T(8,128)(2,1)S(1)}, u32[]{:S(2)}, u32[]{:S(2)}) %all-to-all-start) | async-done | bytes 180256 | tf_op jit(solution)/shard_map/all_to_all | solution.py:33
  16.1 0.0 copy-done.2
  16.1 0.1 fusion.62
  16.2 0.2 multiply_reduce_fusion
  16.4 0.0 copy-done.6
  16.4 0.1 multiply_convert_fusion
  16.5 0.8 fusion.1
  17.4 15.2 %all-to-all-start.1 = ((bf16[16,8,256]{2,1,0:T(8,128)(2,1)}), bf16[16,8,256]{2,1,0:T(8,128)(2,1)S(1)}, u32[]{:S(2)}, u32[]{:S(2)}) async-start(bf16[16,8,256]{2,1,0:T(8,128)(2,1)} %fusion.1), calls=%async_computation.1 | async-start | bytes 131072 | tf_op jit(solution)/shard_map/all_to_all | solution.py:33
  32.6 4.7 %collective-permute-start = (bf16[24,3072]{1,0:T(8,128)(2,1)S(1)}, bf16[24,3072]{1,0:T(8,128)(2,1)S(1)}, u32[]{:S(2)}, u32[]{:S(2)}) collective-permute-start(bf16[24,3072]{1,0:T(8,128)(2,1)S(1)} %constant_dynamic-update-slice_fusion), channel_id=1, source_target_pairs={{0,64},{32,96},{64,0},{96,32},{128,192},{160,224},{192,128},{224,1... | collective-permute-start | bytes 442376 | tf_op jit(solution)/shard_map/ppermute | solution.py:51
  37.4 9.9 %all-to-all-done.1 = bf16[16,8,256]{2,1,0:T(8,128)(2,1)S(1)} async-done(((bf16[16,8,256]{2,1,0:T(8,128)(2,1)}), bf16[16,8,256]{2,1,0:T(8,128)(2,1)S(1)}, u32[]{:S(2)}, u32[]{:S(2)}) %all-to-all-start.1) | async-done | bytes 65568 | tf_op jit(solution)/shard_map/all_to_all | solution.py:33
  47.3 0.1 broadcast_in_dim.77
  47.4 0.9 pad_maximum_fusion
  48.4 5.6 %all-to-all-start.2 = ((bf16[32,48,256]{2,1,0:T(8,128)(2,1)}), bf16[32,48,256]{2,1,0:T(8,128)(2,1)S(1)}, u32[]{:S(2)}, u32[]{:S(2)}) async-start(bf16[32,48,256]{2,1,0:T(8,128)(2,1)} %bitcast.10), calls=%async_computation.2 | async-start | bytes 1572864 | tf_op jit(solution)/shard_map/all_to_all | solution.py:33
  54.0 0.0 collective-permute-done
  54.0 1.9 %collective-permute-start.1 = (bf16[48,3072]{1,0:T(8,128)(2,1)S(1)}, bf16[48,3072]{1,0:T(8,128)(2,1)S(1)}, u32[]{:S(2)}, u32[]{:S(2)}) collective-permute-start(bf16[48,3072]{1,0:T(8,128)(2,1)S(1)} %pad_maximum_fusion.3), channel_id=1, source_target_pairs={{0,32},{32,0},{64,96},{96,64},{128,160},{160,128},{192,224},{224,1... | collective-permute-start | bytes 884744 | tf_op jit(solution)/shard_map/ppermute | solution.py:51
  55.9 9.0 %collective-permute-done.1 = bf16[48,3072]{1,0:T(8,128)(2,1)S(1)} collective-permute-done((bf16[48,3072]{1,0:T(8,128)(2,1)S(1)}, bf16[48,3072]{1,0:T(8,128)(2,1)S(1)}, u32[]{:S(2)}, u32[]{:S(2)}) %collective-permute-start.1) | collective-permute-done | bytes 294944 | tf_op jit(solution)/shard_map/ppermute | solution.py:51
  65.0 1.8 %all-to-all-done.2 = bf16[32,48,256]{2,1,0:T(8,128)(2,1)S(1)} async-done(((bf16[32,48,256]{2,1,0:T(8,128)(2,1)}), bf16[32,48,256]{2,1,0:T(8,128)(2,1)S(1)}, u32[]{:S(2)}, u32[]{:S(2)}) %all-to-all-start.2) | async-done | bytes 786464 | tf_op jit(solution)/shard_map/all_to_all | solution.py:33
  66.7 0.1 copy.82
  66.8 0.0 copy-start.1
  66.9 0.2 fusion.18
  67.1 0.2 multiply_convert_fusion.1
  67.4 0.6 copy-done.1
  67.9 0.4 fusion.9
  68.3 0.0 copy-done
  68.3 2.3 %convolution_convert_fusion = bf16[256,1024]{1,0:T(8,128)(2,1)S(1)} fusion(bf16[256,1024]{1,0:T(8,128)(2,1)S(1)} %bitcast.100, bf16[1,352,1024]{2,1,0:T(8,128)(2,1)S(1)} %copy-done, bf16[1,1024,352]{1,2,0:T(8,128)(2,1)} %param.39, f32[256,352]{0,1:T(8,128)S(1)} %fusion.9), kind=kOutput, calls=%fused_computation | convolution fusion | flops 369901568 | bytes 2850816 | tf_op jit(solution)/shard_map/dot_general | solution.py:350
  70.7 0.2 convolution_convert_fusion.3
  70.9 0.2 convolution_convert_fusion.4
  71.1 0.2 convolution_convert_fusion.1
  71.3 0.2 convolution_convert_fusion.2
  71.6 0.1 pad_maximum_fusion.1
  71.7 18.2 %all_to_all.31 = bf16[32,48,256]{2,1,0:T(8,128)(2,1)S(1)} all-to-all(bf16[32,48,256]{2,1,0:T(8,128)(2,1)S(1)} %bitcast.96), channel_id=1, replica_groups=mesh['z'=16,'x'=4,'c'=2,'tp'=4] {'x','c','tp'}, dimensions={0} | all-to-all | bytes 1572864 | tf_op jit(solution)/shard_map/all_to_all | solution.py:33
  89.9 0.2 convert_element_type.64
  90.1 0.0 copy-start.8
  90.1 0.0 copy-start.7
  90.1 0.0 copy-start.9
  90.1 0.1 bitcast_reduce_fusion
  90.4 0.6 copy.79
  91.0 3.7 %all-to-all-start.4 = ((bf16[16,8,256]{2,1,0:T(8,128)(2,1)}), bf16[16,8,256]{2,1,0:T(8,128)(2,1)S(1)}, u32[]{:S(2)}, u32[]{:S(2)}) async-start(bf16[16,8,256]{2,1,0:T(8,128)(2,1)} %copy.79), calls=%async_computation.4 | async-start | bytes 131072 | tf_op jit(solution)/shard_map/all_to_all | solution.py:33
  94.7 0.0 copy-done.8
  94.7 0.1 fusion.42
  94.8 0.0 copy-done.7
  94.8 0.1 fusion.5
  94.9 12.8 %all-to-all-done.4 = bf16[16,8,256]{2,1,0:T(8,128)(2,1)S(1)} async-done(((bf16[16,8,256]{2,1,0:T(8,128)(2,1)}), bf16[16,8,256]{2,1,0:T(8,128)(2,1)S(1)}, u32[]{:S(2)}, u32[]{:S(2)}) %all-to-all-start.4) | async-done | bytes 65568 | tf_op jit(solution)/shard_map/all_to_all | solution.py:33
  107.7 0.3 fusion.63
  108.0 0.1 pad_maximum_fusion.5
  108.1 7.9 %all_to_all.32 = f32[4,1,32]{2,1,0:T(1,128)S(1)} all-to-all(f32[4,1,32]{2,1,0:T(1,128)S(1)} %broadcast_in_dim.80), channel_id=1, replica_groups=mesh['z'=16,'x'=4,'c'=2,'tp'=4] {'tp'}, dimensions={0} | all-to-all | bytes 1024 | tf_op jit(solution)/shard_map/all_to_all | solution.py:25
  116.0 0.1 slice_multiply_fusion
  116.1 0.0 copy-done.9
  116.1 0.7 multiply_convert_fusion.2
  (38 shorter events, 0.7 us)
Async XLA Ops:
  0.0 68.3 %copy-start = (bf16[1,352,1024]{2,1,0:T(8,128)(2,1)S(1)}, bf16[1,352,1024]{2,1,0:T(8,128)(2,1)}, u32[]{:S(2)}) copy-start(bf16[1,352,1024]{2,1,0:T(8,128)(2,1)} %param.40) | copy-start | bytes 2162692
  0.0 9.8 %copy-start.5 = (s32[16,2]{0,1:T(2,128)S(1)}, s32[16,2]{0,1:T(2,128)}, u32[]{:S(2)}) copy-start(s32[16,2]{0,1:T(2,128)} %param.46) | copy-start | bytes 388
  0.0 10.1 %copy-start.3 = (bf16[22,1024]{1,0:T(8,128)(2,1)S(1)}, bf16[22,1024]{1,0:T(8,128)(2,1)}, u32[]{:S(2)}) copy-start(bf16[22,1024]{1,0:T(8,128)(2,1)} %param.41) | copy-start | bytes 135172
  0.0 10.1 %copy-start.4 = (bf16[22,1024]{1,0:T(8,128)(2,1)S(1)}, bf16[22,1024]{1,0:T(8,128)(2,1)}, u32[]{:S(2)}) copy-start(bf16[22,1024]{1,0:T(8,128)(2,1)} %param.42) | copy-start | bytes 135172
  0.0 16.1 %copy-start.2 = (bf16[16,1024]{1,0:T(8,128)(2,1)S(1)}, bf16[16,1024]{1,0:T(8,128)(2,1)}, u32[]{:S(2)}) copy-start(bf16[16,1024]{1,0:T(8,128)(2,1)} %tokens_ref.1) | copy-start | bytes 98308
  0.0 16.4 %copy-start.6 = (f32[1024]{0:T(1024)S(1)}, f32[1024]{0:T(1024)}, u32[]{:S(2)}) copy-start(f32[1024]{0:T(1024)} %param.37) | copy-start | bytes 12292
  5.3 10.7 %all-to-all-start = ((bf16[4,88,256]{2,1,0:T(8,128)(2,1)}), bf16[4,88,256]{2,1,0:T(8,128)(2,1)S(1)}, u32[]{:S(2)}, u32[]{:S(2)}) async-start(bf16[4,88,256]{2,1,0:T(8,128)(2,1)} %mixer.1), calls=%async_computation | async-start | bytes 360448 | tf_op jit(solution)/shard_map/all_to_all | solution.py:33
  17.4 29.8 %all-to-all-start.1 = ((bf16[16,8,256]{2,1,0:T(8,128)(2,1)}), bf16[16,8,256]{2,1,0:T(8,128)(2,1)S(1)}, u32[]{:S(2)}, u32[]{:S(2)}) async-start(bf16[16,8,256]{2,1,0:T(8,128)(2,1)} %fusion.1), calls=%async_computation.1 | async-start | bytes 131072 | tf_op jit(solution)/shard_map/all_to_all | solution.py:33
  32.6 21.3 %collective-permute-start = (bf16[24,3072]{1,0:T(8,128)(2,1)S(1)}, bf16[24,3072]{1,0:T(8,128)(2,1)S(1)}, u32[]{:S(2)}, u32[]{:S(2)}) collective-permute-start(bf16[24,3072]{1,0:T(8,128)(2,1)S(1)} %constant_dynamic-update-slice_fusion), channel_id=1, source_target_pairs={{0,64},{32,96},{64,0},{96,32},{128,192},{160,224},{192,128},{224,1... | collective-permute-start | bytes 442376 | tf_op jit(solution)/shard_map/ppermute | solution.py:51
  48.4 18.4 %all-to-all-start.2 = ((bf16[32,48,256]{2,1,0:T(8,128)(2,1)}), bf16[32,48,256]{2,1,0:T(8,128)(2,1)S(1)}, u32[]{:S(2)}, u32[]{:S(2)}) async-start(bf16[32,48,256]{2,1,0:T(8,128)(2,1)} %bitcast.10), calls=%async_computation.2 | async-start | bytes 1572864 | tf_op jit(solution)/shard_map/all_to_all | solution.py:33
  54.0 10.9 %collective-permute-start.1 = (bf16[48,3072]{1,0:T(8,128)(2,1)S(1)}, bf16[48,3072]{1,0:T(8,128)(2,1)S(1)}, u32[]{:S(2)}, u32[]{:S(2)}) collective-permute-start(bf16[48,3072]{1,0:T(8,128)(2,1)S(1)} %pad_maximum_fusion.3), channel_id=1, source_target_pairs={{0,32},{32,0},{64,96},{96,64},{128,160},{160,128},{192,224},{224,1... | collective-permute-start | bytes 884744 | tf_op jit(solution)/shard_map/ppermute | solution.py:51
  66.8 1.1 copy-start.1
  90.1 4.6 %copy-start.8 = (f32[16,2]{0,1:T(2,128)S(1)}, f32[16,2]{0,1:T(2,128)}, u32[]{:S(2)}) copy-start(f32[16,2]{0,1:T(2,128)} %param.47) | copy-start | bytes 388
  90.1 4.7 %copy-start.7 = (bf16[1024]{0:T(1024)(128)(2,1)S(1)}, bf16[1024]{0:T(1024)(128)(2,1)}, u32[]{:S(2)}) copy-start(bf16[1024]{0:T(1024)(128)(2,1)} %param.44) | copy-start | bytes 6148
  90.1 26.0 %copy-start.9 = (f32[256]{0:T(256)S(1)}, f32[256]{0:T(256)}, u32[]{:S(2)}) copy-start(f32[256]{0:T(256)} %param.45) | copy-start | bytes 3076
  91.0 16.7 %all-to-all-start.4 = ((bf16[16,8,256]{2,1,0:T(8,128)(2,1)}), bf16[16,8,256]{2,1,0:T(8,128)(2,1)S(1)}, u32[]{:S(2)}, u32[]{:S(2)}) async-start(bf16[16,8,256]{2,1,0:T(8,128)(2,1)} %copy.79), calls=%async_computation.4 | async-start | bytes 131072 | tf_op jit(solution)/shard_map/all_to_all | solution.py:33

commit v4 on v3

v4 whole, which is shorter than its diff:
```python
import math
from functools import partial

import jax
import jax.numpy as jnp
from jax import lax
from jax.experimental import pallas as pl
from jax.experimental.pallas import tpu as pltpu
from jax.sharding import Mesh
from jax.sharding import PartitionSpec as P


SPLIT = 4
EP = ("z", "x", "c")
PLANE = ("x", "c", "tp")


residual_scale = 1.4142135623730951
norm_epsilon = 1e-05
head_epsilon = 0.00064
key_epsilon = 1e-06


def sent_to_all(value, axis):
    copies = jnp.broadcast_to(value, (lax.axis_size(axis), *value.shape))
    return lax.all_to_all(copies, axis, split_axis=0, concat_axis=0, tiled=True)


def of_everyone(value, axis):
    return sent_to_all(value, axis).astype(jnp.float32).sum(axis=0)


def exchange(parts, axis):
    return lax.all_to_all(parts, axis, split_axis=0, concat_axis=0, tiled=True)


def in_one(arrays, axis):
    vector, at, done = (jnp.concatenate([a.reshape(-1) for a in arrays]), 0, [])
    running = of_everyone(vector, axis)
    for a in arrays:
        done.append(running[at : at + a.size].reshape(a.shape))
        at += a.size
    return tuple(done)


def padded_units(columns, multiple):
    return jnp.pad(columns, ((0, -columns.shape[0] % multiple), (0, 0)))


def with_neighbour(units, step):
    planes = lax.axis_size("z")
    other = lax.ppermute(units, "z", [(i, i ^ step) for i in range(planes)])
    return jnp.concatenate([units, other], 0)


def mixer_kernel(*refs, chunks):
    count = (len(refs) - 4) // 2
    sources, message_ref, targets = refs[:count], refs[count], refs[count + 1 : 2 * count + 1]
    query_ref, answer_ref, arrival = refs[2 * count + 1 :]
    (
        tokens_ref,
        decay_down_ref,
        rate_down_ref,
        decay_up_ref,
        decay_base_ref,
        rate_up_ref,
        rate_base_ref,
        w_key_ref,
        w_recep_ref,
        state_ref,
        w_value_ref,
        head_gain_ref,
        w_out_ref,
        down_ref,
    ) = targets
    copies = {}
    for source, target in zip(sources, targets):
        parts = chunks if target is state_ref else 1
        size = target.shape[0] // parts
        for i in range(parts):
            at = pl.ds(i * size, size) if parts > 1 else slice(None)
            copies[id(target), i] = pltpu.make_async_copy(
                source.at[at], target.at[at], arrival.at[len(copies)]
            )
    for copy in copies.values():
        copy.start()

    def landed(target, part=0):
        copies[id(target), part].wait()
        return target

    row_count, heads, head_size = state_ref.shape[0], state_ref.shape[1], state_ref.shape[3]
    width = heads * head_size
    tokens = landed(tokens_ref)[...]
    f32 = jnp.float32

    def turned(a, b):
        return lax.dot_general(a, b, (((1,), (1,)), ((), ())), preferred_element_type=f32)

    channel_head = lax.broadcasted_iota(jnp.int32, (width, width), 0) // head_size
    same_head = (
        channel_head == lax.broadcasted_iota(jnp.int32, (width, width), 1) // head_size
    ).astype(f32)

    def over_head(values):
        return jnp.dot(
            values, same_head, precision=lax.Precision.HIGHEST, preferred_element_type=f32
        )

    decay_low = jnp.tanh(turned(tokens, landed(decay_down_ref)[...])).astype(jnp.bfloat16)
    rate_low = turned(tokens, landed(rate_down_ref)[...]).astype(jnp.bfloat16)
    decay_pre = landed(decay_base_ref)[...] + jnp.dot(
        decay_low, landed(decay_up_ref)[...], preferred_element_type=f32
    )
    decay = jnp.exp(-(math.exp(-0.5) * jax.nn.sigmoid(decay_pre)))
    in_rate = jax.nn.sigmoid(
        landed(rate_base_ref)[...]
        + jnp.dot(rate_low, landed(rate_up_ref)[...], preferred_element_type=f32)
    )
    key_vecs = jnp.dot(tokens, landed(w_key_ref)[...], preferred_element_type=f32)
    recep = jnp.dot(tokens, landed(w_recep_ref)[...], preferred_element_type=f32)
    sums = over_head(
        jnp.concatenate([key_vecs * key_vecs, key_vecs * in_rate * recep, key_vecs * recep], 0)
    )
    scale = lax.rsqrt(sums[:row_count] + key_epsilon)
    removed_factor = scale * sums[row_count : 2 * row_count]
    value_factor = sums[2 * row_count :]
    for which, vectors in enumerate((decay * recep, key_vecs * scale)):
        for h in range(heads):
            pair = vectors[:, h // 2 * 128 : h // 2 * 128 + 128]
            query_ref[pl.ds(which * heads + h, row_count, stride=2 * heads), :] = (
                pair if h % 2 == 0 else pltpu.roll(pair, head_size, 1)
            )
    for t in range(row_count):
        if t % (row_count // chunks) == 0:
            landed(state_ref, t // (row_count // chunks))
        queries = query_ref[2 * heads * t : 2 * heads * (t + 1), :head_size].astype(jnp.bfloat16)
        matrix = state_ref[t].reshape(width, head_size).astype(jnp.bfloat16)
        answers = turned(queries, matrix)
        for pair in range(heads // 2):
            answer_ref[pair, 2 * heads * t : 2 * heads * (t + 1), :] = answers[
                :, pair * 128 : (pair + 1) * 128
            ]
    first_of_pair = lax.broadcasted_iota(jnp.int32, (row_count, 128), 1) < head_size

    def picked(which):
        pairs = []
        for pair in range(heads // 2):
            of_pair = answer_ref.at[pair]
            rows = [
                of_pair[pl.ds(which * heads + 2 * pair + i, row_count, stride=2 * heads), :]
                for i in range(2)
            ]
            pairs.append(jnp.where(first_of_pair, rows[0], rows[1]))
        return jnp.concatenate(pairs, 1)

    value_vecs = jnp.dot(tokens, landed(w_value_ref)[...], preferred_element_type=f32)
    read_out = picked(0) - picked(1) * removed_factor + value_vecs * value_factor
    centred = read_out - over_head(read_out) * (1.0 / head_size)
    spread = over_head(centred * centred) * (1.0 / head_size)
    normed = centred * lax.rsqrt(spread + head_epsilon) * landed(head_gain_ref)[...]
    mixed = jnp.dot(normed.astype(jnp.bfloat16), landed(w_out_ref)[...], preferred_element_type=f32)
    mixed = mixed.astype(jnp.bfloat16)
    copies_out, mix_rows = message_ref.shape[0], row_count * heads
    landed(down_ref)
    for c in range(copies_out):
        for h in range(mixed.shape[1] // width):
            message_ref[c, h * row_count : (h + 1) * row_count, :] = mixed[
                :, h * width : (h + 1) * width
            ]
        message_ref[c, mix_rows:, :] = jnp.zeros_like(message_ref[c, mix_rows:, :])
        message_ref[c, mix_rows : mix_rows + down_ref.shape[0], :] = down_ref[...]


def mixer_message(
    copies_out,
    own_down,
    tokens,
    state,
    w_recep,
    w_key,
    w_value,
    w_out,
    decay_base,
    decay_down,
    decay_up,
    rate_base,
    rate_down,
    rate_up,
    head_gain,
):
    row_count, heads, head_size = state.shape[0], state.shape[1], state.shape[3]
    width = heads * head_size
    far = [
        tokens,
        decay_down.T,
        rate_down.T,
        decay_up,
        decay_base[None],
        rate_up,
        rate_base[None],
        w_key,
        w_recep,
        state,
        w_value,
        head_gain[None],
        w_out,
        own_down,
    ]
    chunks = 4
    down_rows = own_down.shape[0] + -own_down.shape[0] % 8
    rows = tokens.shape[1] // width * row_count + down_rows
    return pl.pallas_call(
        partial(mixer_kernel, chunks=chunks),
        out_shape=pltpu.VMEM((copies_out, rows, width), jnp.bfloat16),
        in_specs=[pl.BlockSpec(memory_space=pl.ANY)] * len(far),
        out_specs=pl.BlockSpec(memory_space=pltpu.VMEM),
        scratch_shapes=[pltpu.VMEM(a.shape, a.dtype) for a in far]
        + [
            pltpu.VMEM((2 * heads * row_count, 128), jnp.float32),
            pltpu.VMEM((heads // 2, 2 * heads * row_count, 128), jnp.float32),
            pltpu.SemaphoreType.DMA((len(far) - 1 + chunks,)),
        ],
        name="mixer",
    )(*far)


def expert_kernel(
    rows_ref,
    units_ref,
    gate_any,
    up_any,
    down_any,
    out_ref,
    gate_ref,
    up_ref,
    down_ref,
    arrival,
    *,
    rows,
):
    copies = [
        pltpu.make_async_copy(source, target, arrival.at[i])
        for i, (source, target) in enumerate(
            ((gate_any, gate_ref), (up_any, up_ref), (down_any, down_ref))
        )
    ]
    for copy in copies:
        copy.start()
    blocks, splits, height, quarter = rows_ref.shape
    width = splits * quarter
    f32 = jnp.float32

    def turned(a, b):
        return lax.dot_general(a, b, (((1,), (1,)), ((), ())), preferred_element_type=f32)

    def whole_rows(low, high):
        return jnp.concatenate(
            [
                rows_ref[:, i, low:high, :].reshape(blocks * (high - low), quarter)
                for i in range(splits)
            ],
            1,
        )

    dense = whole_rows(rows, height)
    gate_pre = turned(dense, units_ref[:, :width])
    up_pre = turned(dense, units_ref[:, width : 2 * width])
    hidden = (jax.nn.silu(gate_pre) * up_pre).astype(jnp.bfloat16)
    for i in range(splits):
        down = units_ref[:, 2 * width + i * quarter : 2 * width + (i + 1) * quarter]
        part = jnp.dot(hidden, down, preferred_element_type=f32).astype(jnp.bfloat16)
        out_ref[:, i, rows:, :] = part.reshape(blocks, height - rows, quarter)
    routed = whole_rows(0, rows)
    copies[0].wait()
    gate_pre = turned(routed, gate_ref[...])
    copies[1].wait()
    up_pre = turned(routed, up_ref[...])
    hidden = (jax.nn.silu(gate_pre) * up_pre).astype(jnp.bfloat16)
    copies[2].wait()
    for i in range(splits):
        down = down_ref[:, i * quarter : (i + 1) * quarter]
        part = jnp.dot(hidden, down, preferred_element_type=f32).astype(jnp.bfloat16)
        out_ref[:, i, :rows, :] = part.reshape(blocks, rows, quarter)


def run_experts(everything, units, expert_gate, expert_up, expert_down, rows):
    far = [expert_gate.T, expert_up.T, expert_down]
    vmem = pl.BlockSpec(memory_space=pltpu.VMEM)
    return pl.pallas_call(
        partial(expert_kernel, rows=rows),
        out_shape=pltpu.VMEM(everything.shape, jnp.bfloat16),
        in_specs=[vmem, vmem] + [pl.BlockSpec(memory_space=pl.ANY)] * len(far),
        out_specs=vmem,
        scratch_shapes=[pltpu.VMEM(a.shape, a.dtype) for a in far]
        + [pltpu.SemaphoreType.DMA((len(far),))],
        name="experts",
    )(on_chip(everything), on_chip(units), *far)


def on_chip(value):
    return pltpu.with_memory_space_constraint(value, pltpu.VMEM)


def norm_kernel(
    everyone_ref,
    tokens_ref,
    gain_ref,
    branch_gate_ref,
    routes_ref,
    route_weights_ref,
    packed_ref,
    own_ref,
    factors_ref,
    *,
    experts,
    capacity,
    slots,
    shared,
):
    splits, _, quarter = everyone_ref.shape
    row_count = tokens_ref.shape[0]
    f32, i32 = jnp.float32, jnp.int32
    mixed = everyone_ref[0, : splits * row_count, :].astype(f32)
    for s in range(1, splits):
        mixed = mixed + everyone_ref[s, : splits * row_count, :].astype(f32)
    mixed = jnp.concatenate(
        [mixed[i * row_count : (i + 1) * row_count] for i in range(splits)], 1
    )
    x_mid = first_norm(residual_scale * tokens_ref[...].astype(f32) + mixed, gain_ref[...])
    own = jnp.zeros((row_count, quarter), f32)
    for i in range(splits):
        columns = x_mid[:, i * quarter : (i + 1) * quarter].astype(f32)
        own = jnp.where(lax.axis_index("tp") == i, columns, own)
    own_ref[...] = own
    branch = jax.nn.sigmoid(
        lax.dot_general(
            branch_gate_ref[...], x_mid, (((1,), (1,)), ((), ())), preferred_element_type=f32
        )
    )
    first, second = routes_ref[0:1, :], routes_ref[1:2, :]
    expert = lax.broadcasted_iota(i32, (experts, row_count), 0)
    hit_first, hit_second = (expert == first).astype(f32), (expert == second).astype(f32)
    before = (
        lax.broadcasted_iota(i32, (row_count, row_count), 0)
        < lax.broadcasted_iota(i32, (row_count, row_count), 1)
    ).astype(f32)
    earlier = jnp.dot(hit_first + hit_second, before, preferred_element_type=f32)
    slot_first = jnp.sum(earlier * hit_first, 0, keepdims=True).astype(i32)
    slot_second = jnp.sum(earlier * hit_second, 0, keepdims=True).astype(i32)
    lines = packed_ref.shape[0]
    height = lines * slots // (experts * capacity)
    place = lax.broadcasted_iota(i32, (lines, row_count), 0)
    row = lax.broadcasted_iota(i32, (lines, row_count), 1)
    plane, inner = place // height, place % height
    routed_place = jnp.where(inner < slots, plane * slots + inner, -1)
    dense_place = jnp.where(
        inner < slots, -1, plane % shared * (height - slots) + inner - slots
    )
    at_first = routed_place == first * capacity + slot_first
    at_second = routed_place == second * capacity + slot_second
    at_row = dense_place == row
    chosen = (at_first | at_second | at_row).astype(jnp.bfloat16)
    packed_ref[...] = jnp.dot(
        chosen, own.astype(jnp.bfloat16), preferred_element_type=f32
    ).astype(jnp.bfloat16)
    factors = (
        jnp.where(at_first, route_weights_ref[0:1, :], 0.0)
        + jnp.where(at_second, route_weights_ref[1:2, :], 0.0)
        + jnp.where(at_row, branch, 0.0)
    )
    factors_ref[...] = factors


def norm_and_pack(
    everyone,
    tokens,
    first_gain,
    branch_gate,
    routes,
    route_weights,
    lines,
    experts,
    capacity,
    slots,
    shared,
):
    row_count, quarter = tokens.shape[0], everyone.shape[2]
    vmem = pl.BlockSpec(memory_space=pltpu.VMEM)
    return pl.pallas_call(
        partial(norm_kernel, experts=experts, capacity=capacity, slots=slots, shared=shared),
        out_shape=(
            pltpu.VMEM((lines, quarter), jnp.bfloat16),
            pltpu.VMEM((row_count, quarter), jnp.float32),
            pltpu.VMEM((lines, row_count), jnp.float32),
        ),
        in_specs=[vmem] * 6,
        out_specs=(vmem, vmem, vmem),
        name="norm_and_pack",
    )(
        on_chip(everyone),
        on_chip(tokens),
        on_chip(first_gain[None]),
        on_chip(branch_gate[None]),
        on_chip(routes.T),
        on_chip(route_weights.T),
    )


def fan_kernel(arrived_ref, out_ref, *, capacity, shared):
    planes, slots_part, quarter = arrived_ref.shape
    here, copies, splits, height, _ = out_ref.shape
    part = slots_part - here * capacity
    rows = planes * capacity
    shape = (here * splits * height, planes * slots_part)
    line = lax.broadcasted_iota(jnp.int32, shape, 0)
    column = lax.broadcasted_iota(jnp.int32, shape, 1)
    index, group = line % height, line // height
    expert, split = group // splits, group % splits
    dense = index - rows
    routed_from = index // capacity * slots_part + expert * capacity + index % capacity
    dense_from = (
        (split * shared + dense // part) * slots_part + here * capacity + dense % part
    )
    chosen = (column == jnp.where(index < rows, routed_from, dense_from)).astype(jnp.bfloat16)
    arrived = arrived_ref[...].reshape(planes * slots_part, quarter)
    laid = jnp.dot(chosen, arrived, preferred_element_type=jnp.float32).astype(jnp.bfloat16)
    for e in range(here):
        for i in range(splits):
            at = (e * splits + i) * height
            for c in range(copies):
                out_ref[e, c, i, :, :] = laid[at : at + height]


def fan_out(arrived, capacity, here, copies, splits, shared):
    planes, slots_part, quarter = arrived.shape
    height = planes * capacity + shared * (slots_part - here * capacity)
    vmem = pl.BlockSpec(memory_space=pltpu.VMEM)
    return pl.pallas_call(
        partial(fan_kernel, capacity=capacity, shared=shared),
        out_shape=pltpu.VMEM((here, copies, splits, height, quarter), jnp.bfloat16),
        in_specs=[vmem],
        out_specs=vmem,
        name="fan_out",
    )(on_chip(arrived))


def gather_kernel(returned_ref, out_ref, *, capacity, here, splits, shared):
    planes, slots_part, quarter = out_ref.shape
    sources, height, _ = returned_ref.shape
    part = slots_part - here * capacity
    rows = planes * capacity
    f32 = jnp.float32
    routed = []
    for e in range(here):
        total = jnp.zeros((rows, quarter), f32)
        for s in range(e * (sources // here), (e + 1) * (sources // here)):
            total = total + returned_ref[s, :rows, :].astype(f32)
        routed.append(total)
    dense = []
    for i in range(splits):
        total = jnp.zeros((height - rows, quarter), f32)
        for s in range(i, sources, splits):
            total = total + returned_ref[s, rows:, :].astype(f32)
        dense.append(total)
    sums = jnp.concatenate(routed + dense, 0).astype(jnp.bfloat16)
    shape = (planes * slots_part, sums.shape[0])
    line = lax.broadcasted_iota(jnp.int32, shape, 0)
    column = lax.broadcasted_iota(jnp.int32, shape, 1)
    z, inner = line // slots_part, line % slots_part
    routed_from = inner // capacity * rows + z * capacity + inner % capacity
    dense_from = here * rows + z * part + inner - here * capacity
    chosen = (
        column == jnp.where(inner < here * capacity, routed_from, dense_from)
    ).astype(jnp.bfloat16)
    laid = jnp.dot(chosen, sums, preferred_element_type=f32).astype(jnp.bfloat16)
    out_ref[...] = laid.reshape(planes, slots_part, quarter)


def gather_back(returned, planes, slots_part, capacity, here, splits, shared):
    vmem = pl.BlockSpec(memory_space=pltpu.VMEM)
    return pl.pallas_call(
        partial(gather_kernel, capacity=capacity, here=here, splits=splits, shared=shared),
        out_shape=pltpu.VMEM((planes, slots_part, returned.shape[2]), jnp.bfloat16),
        in_specs=[vmem],
        out_specs=vmem,
        name="gather_back",
    )(on_chip(returned))


def first_norm(values, gain):
    centre = jnp.mean(values, -1, keepdims=True)
    spread = jnp.mean(jnp.square(values - centre), -1, keepdims=True)
    return ((values - centre) * lax.rsqrt(spread + norm_epsilon) * gain).astype(jnp.bfloat16)


def shards(
    tokens,
    state,
    w_recep,
    w_key,
    w_value,
    w_out,
    decay_base,
    decay_down,
    decay_up,
    rate_base,
    rate_down,
    rate_up,
    head_gain,
    first_gain,
    expert_gate,
    expert_up,
    expert_down,
    dense_gate,
    dense_up,
    dense_down,
    branch_gate,
    second_gain,
    routes,
    route_weights,
):
    row_count = tokens.shape[0]
    model_width = tokens.shape[1]
    quarter = w_recep.shape[1]
    planes = lax.axis_size("z")
    plane_blocks = lax.axis_size(("x", "c"))
    plane_size = lax.axis_size(PLANE)
    tp_size = lax.axis_size("tp")
    shared = planes // tp_size
    message = mixer_message(
        tp_size,
        dense_down,
        tokens,
        state,
        w_recep,
        w_key,
        w_value,
        w_out,
        decay_base,
        decay_down,
        decay_up,
        rate_base,
        rate_down,
        rate_up,
        head_gain,
    )
    everyone = exchange(message, "tp")
    everyone, dense_gate, dense_up, branch_gate = lax.optimization_barrier(
        (everyone, dense_gate, dense_up, branch_gate)
    )
    mix_rows = tp_size * row_count
    units = jnp.concatenate(
        [padded_units(dense_gate, 8), padded_units(dense_up, 8)]
        + [everyone[i, mix_rows:] for i in range(tp_size)],
        1,
    )
    units = with_neighbour(units, 2)
    units = with_neighbour(units, 1)
    experts = lax.axis_size(EP) // SPLIT
    here = experts // planes
    capacity = min(row_count, max(2, 2 * row_count * routes.shape[1] // experts))
    slots = here * capacity
    part = row_count // shared
    packed_rows, own_columns, factors = norm_and_pack(
        everyone,
        tokens,
        first_gain,
        branch_gate,
        routes,
        route_weights,
        planes * (slots + part),
        experts,
        capacity,
        slots,
        shared,
    )
    arrived = exchange(packed_rows.reshape(planes, slots + part, quarter), "z")
    rows = planes * capacity
    dense_count = shared * part
    height = rows + dense_count
    outgoing = fan_out(arrived, capacity, here, plane_blocks // here, tp_size, shared)
    everything = exchange(outgoing.reshape(plane_size, height, quarter), PLANE)
    everything = everything.reshape(plane_blocks, tp_size, height, quarter)
    returning = run_experts(
        everything, units, expert_gate[0], expert_up[0], expert_down[0], rows
    )
    returned = exchange(returning.reshape(plane_size, height, quarter), PLANE)
    back = gather_back(returned, planes, slots + part, capacity, here, tp_size, shared)
    back = exchange(back, "z").reshape(planes * (slots + part), quarter)
    second_sum = residual_scale * own_columns + lax.dot_general(
        factors,
        back.astype(jnp.float32),
        (((0,), (0,)), ((), ())),
        precision=lax.Precision.HIGHEST,
        preferred_element_type=jnp.float32,
    )
    row_sums, square_sums = in_one(
        (jnp.sum(second_sum, 1), jnp.sum(second_sum * second_sum, 1)), "tp"
    )
    average = row_sums / model_width
    spread = square_sums / model_width - average * average
    return (
        (second_sum - average[:, None]) * lax.rsqrt(spread + norm_epsilon)[:, None] * second_gain
    ).astype(jnp.bfloat16)


def solution(mesh):
    finer = Mesh(mesh.devices.reshape(16, 4, 2, mesh.shape["tp"]), ("z", "x", "c", "tp"))
    return jax.shard_map(
        shards,
        mesh=finer,
        in_specs=(
            P(EP, None),
            P(EP, "tp", None, None),
            P(None, "tp"),
            P(None, "tp"),
            P(None, "tp"),
            P("tp", None),
            P("tp"),
            P(),
            P(None, "tp"),
            P("tp"),
            P(),
            P(None, "tp"),
            P("tp"),
            P(),
            P(EP, None, "tp"),
            P(EP, None, "tp"),
            P(EP, "tp", None),
            P(EP, None),
            P(EP, None),
            P(EP, "tp"),
            P(),
            P("tp"),
            P(EP, None),
            P(EP, None),
        ),
        out_specs=P(EP, "tp"),
        check_vma=False,
    )
```

time: 117 us -> 112 us (0.957)
  blocking collectives: 26.1 us -> 52.2 us
  waiting for transfers between devices: 39.2 us -> 20.6 us
  starting transfers between devices: 35.6 us -> 27.4 us
  matrix products: 5.2 us -> 0.36 us
  Pallas kernels: 5.28 us -> 9.95 us
  other arithmetic: 3.21 us -> 0.91 us
  local copies, waits for them, and re-layouts: 1.77 us -> 0.08 us
    all_to_all x1 -> x3, blocking collectives: 18.2 us -> 44.6 us  [exchange(): return lax.all_to_all(parts, axis, split_axis=0, concat_axis=0, tiled=True)]
    all_to_all x4 -> x2, waiting for transfers between devices: 30.2 us -> 11.6 us  [exchange(): return lax.all_to_all(parts, axis, split_axis=0, concat_axis=0, tiled=True)]
    all_to_all x4 -> x2, starting transfers between devices: 28.9 us -> 20.8 us  [exchange(): return lax.all_to_all(parts, axis, split_axis=0, concat_axis=0, tiled=True)]
    dot_general x11 -> x1, matrix products: 5.2 us -> 0.36 us  [shards(): lax.dot_general(factors, back.astype(jnp.float32), (((0,), (0,)), ((), ()...]
    pallas_call x1 -> x5, Pallas kernels: 5.28 us -> 9.95 us  [the longest x1 4.6 us: mixer_message(): pl.pallas_call(partial(mixer_kernel, chunks=chunks), out_shape=pltpu.VMEM...]
  transfers between devices with their start and end apart: 6 -> 4, of which waited for: 5 -> 3; matrix products, arithmetic and copies ran while one was open for 2% -> 0% of each run, Pallas kernels for 0% -> 1%
where the time goes in v4:
time: 112 us
  blocking collectives  52.2 us (47%)
  starting transfers between devices  27.4 us (24%)
  waiting for transfers between devices  20.6 us (18%)
  Pallas kernels  9.95 us (9%)
    all_to_all x3, blocking collectives, exchange(): return lax.all_to_all(parts, axis, split_axis=0, concat_axis=0, tiled=True)  44.6 us
    all_to_all x2, starting transfers between devices, exchange(): return lax.all_to_all(parts, axis, split_axis=0, concat_axis=0, tiled=True)  20.8 us
    all_to_all x2, waiting for transfers between devices, exchange(): return lax.all_to_all(parts, axis, split_axis=0, concat_axis=0, tiled=True)  11.6 us
    ppermute x2, waiting for transfers between devices, with_neighbour(): other = lax.ppermute(units, 'z', [(i, i ^ step) for i in range(planes)])  9 us
    all_to_all x1, blocking collectives, sent_to_all(): return lax.all_to_all(copies, axis, split_axis=0, concat_axis=0, tiled=True)  7.66 us
    ppermute x2, starting transfers between devices, with_neighbour(): other = lax.ppermute(units, 'z', [(i, i ^ step) for i in range(planes)])  6.65 us
    pallas_call x1, Pallas kernels, mixer_message(): pl.pallas_call(partial(mixer_kernel, chunks=chunks), out_shape=pltpu.VMEM...  4.6 us
    pallas_call x1, Pallas kernels, run_experts(): pl.pallas_call(partial(expert_kernel, rows=rows), out_shape=pltpu.VMEM(ev...  2.48 us
  transfers between devices with their start and end apart: 4, of which 3 were waited for; matrix products, arithmetic and copies ran while one was open for 0% of the time, Pallas kernels for 1%

profile of v4, /device:TPU:2, one launch (start us, length us, event | category | flops | bytes accessed | tf_op | source)
XLA Modules:
  0.0 111.7 jit_solution(8473813722192494955)
XLA Ops:
  0.0 0.0 copy-start.6
  0.0 0.0 copy-start
  0.0 0.0 copy-start.1
  0.0 0.0 copy-start.2
  0.0 0.0 copy-start.3
  0.0 0.0 copy-start.4
  0.0 0.0 copy-start.5
  0.0 4.6 %mixer.1 = bf16[4,88,256]{2,1,0:T(8,128)(2,1)S(1)} custom-call(bf16[16,1024]{1,0:T(8,128)(2,1)} %tokens_ref.1, bf16[64,1024]{1,0:T(8,128)(2,1)} %bitcast.42, bf16[64,1024]{1,0:T(8,128)(2,1)} %bitcast.43, bf16[64,256]{1,0:T(8,128)(2,1)} %refs_3_.1, f32[1,256]{1,0:T(1,128)} %bitcast.45, bf16[64,256]{1,0:T(8,128)(2,1)} %refs_5_.1, f32[1,256]{1,0:T(1,128)} %bitcast.46, ...), custom_call_target="tpu_custom_call" | custom-call | tf_op jit(solution)/shard_map/mixer/pallas_call | solution.py:213
  4.7 10.5 %all_to_all.31.everyone_ref = bf16[4,88,256]{2,1,0:T(8,128)(2,1)S(1)} all-to-all(bf16[4,88,256]{2,1,0:T(8,128)(2,1)S(1)} %mixer.1), channel_id=1, replica_groups=mesh['z'=16,'x'=4,'c'=2,'tp'=4] {'tp'}, dimensions={0} | all-to-all | bytes 360448 | tf_op jit(solution)/shard_map/all_to_all | solution.py:34
  15.2 0.0 copy-done.6
  15.2 0.0 copy-done
  15.2 0.0 copy-done.1
  15.2 0.0 copy-done.2
  15.2 0.0 copy-done.3
  15.2 1.0 norm_and_pack.1
  16.2 15.2 %all-to-all-start.1 = ((bf16[16,8,256]{2,1,0:T(8,128)(2,1)}), bf16[16,8,256]{2,1,0:T(8,128)(2,1)S(1)}, u32[]{:S(2)}, u32[]{:S(2)}) async-start(bf16[16,8,256]{2,1,0:T(8,128)(2,1)} %bitcast.8), calls=%async_computation.1 | async-start | bytes 131072 | tf_op jit(solution)/shard_map/all_to_all | solution.py:34
  31.4 0.0 copy-done.4
  31.4 0.0 copy-done.5
  31.5 4.7 %collective-permute-start = (bf16[24,3072]{1,0:T(8,128)(2,1)S(1)}, bf16[24,3072]{1,0:T(8,128)(2,1)S(1)}, u32[]{:S(2)}, u32[]{:S(2)}) collective-permute-start(bf16[24,3072]{1,0:T(8,128)(2,1)S(1)} %constant_dynamic-update-slice_fusion), channel_id=1, source_target_pairs={{0,64},{32,96},{64,0},{96,32},{128,192},{160,224},{192,128},{224,1... | collective-permute-start | bytes 442376 | tf_op jit(solution)/shard_map/ppermute | solution.py:52
  36.3 9.8 %all-to-all-done.1.arrived_ref = bf16[16,8,256]{2,1,0:T(8,128)(2,1)S(1)} async-done(((bf16[16,8,256]{2,1,0:T(8,128)(2,1)}), bf16[16,8,256]{2,1,0:T(8,128)(2,1)S(1)}, u32[]{:S(2)}, u32[]{:S(2)}) %all-to-all-start.1) | async-done | bytes 65568 | tf_op jit(solution)/shard_map/all_to_all | solution.py:34
  46.1 1.6 %fan_out.1 = bf16[2,4,4,48,256]{4,3,2,1,0:T(8,128)(2,1)} custom-call(bf16[16,8,256]{2,1,0:T(8,128)(2,1)S(1)} %all-to-all-done.1.arrived_ref), custom_call_target="tpu_custom_call" | custom-call | tf_op jit(solution)/shard_map/fan_out/pallas_call | solution.py:439
  47.7 5.6 %all-to-all-start.2 = ((bf16[32,48,256]{2,1,0:T(8,128)(2,1)}), bf16[32,48,256]{2,1,0:T(8,128)(2,1)S(1)}, u32[]{:S(2)}, u32[]{:S(2)}) async-start(bf16[32,48,256]{2,1,0:T(8,128)(2,1)} %bitcast.9), calls=%async_computation.2 | async-start | bytes 1572864 | tf_op jit(solution)/shard_map/all_to_all | solution.py:34
  53.3 0.0 collective-permute-done
  53.3 1.9 %collective-permute-start.1 = (bf16[48,3072]{1,0:T(8,128)(2,1)S(1)}, bf16[48,3072]{1,0:T(8,128)(2,1)S(1)}, u32[]{:S(2)}, u32[]{:S(2)}) collective-permute-start(bf16[48,3072]{1,0:T(8,128)(2,1)S(1)} %pad_maximum_fusion.1), channel_id=1, source_target_pairs={{0,32},{32,0},{64,96},{96,64},{128,160},{160,128},{192,224},{224,1... | collective-permute-start | bytes 884744 | tf_op jit(solution)/shard_map/ppermute | solution.py:52
  55.2 9.0 %collective-permute-done.1 = bf16[48,3072]{1,0:T(8,128)(2,1)S(1)} collective-permute-done((bf16[48,3072]{1,0:T(8,128)(2,1)S(1)}, bf16[48,3072]{1,0:T(8,128)(2,1)S(1)}, u32[]{:S(2)}, u32[]{:S(2)}) %collective-permute-start.1) | collective-permute-done | bytes 294944 | tf_op jit(solution)/shard_map/ppermute | solution.py:52
  64.3 1.8 %all-to-all-done.2 = bf16[32,48,256]{2,1,0:T(8,128)(2,1)S(1)} async-done(((bf16[32,48,256]{2,1,0:T(8,128)(2,1)}), bf16[32,48,256]{2,1,0:T(8,128)(2,1)S(1)}, u32[]{:S(2)}, u32[]{:S(2)}) %all-to-all-start.2) | async-done | bytes 786464 | tf_op jit(solution)/shard_map/all_to_all | solution.py:34
  66.0 2.5 %experts.1 = bf16[8,4,48,256]{3,2,1,0:T(8,128)(2,1)S(1)} custom-call(bf16[8,4,48,256]{3,2,1,0:T(8,128)(2,1)S(1)} %bitcast.34, bf16[96,3072]{1,0:T(8,128)(2,1)S(1)} %pad_maximum_fusion.units_ref, bf16[352,1024]{1,0:T(8,128)(2,1)} %bitcast.39, bf16[352,1024]{1,0:T(8,128)(2,1)} %bitcast.40, bf16[352,1024]{1,0:T(8,128)(2,1)} %bitcast.41), custom_call_target="tpu_custom_call" | custom-call | tf_op jit(solution)/shard_map/experts/pallas_call | solution.py:290
  68.5 0.0 copy-start.7
  68.5 18.2 %all_to_all.32.returned_ref = bf16[32,48,256]{2,1,0:T(8,128)(2,1)S(1)} all-to-all(bf16[32,48,256]{2,1,0:T(8,128)(2,1)S(1)} %bitcast.35), channel_id=1, replica_groups=mesh['z'=16,'x'=4,'c'=2,'tp'=4] {'x','c','tp'}, dimensions={0} | all-to-all | bytes 1572864 | tf_op jit(solution)/shard_map/all_to_all | solution.py:34
  86.8 0.3 gather_back.1
  87.0 15.8 %all_to_all.33 = bf16[16,8,256]{2,1,0:T(8,128)(2,1)S(1)} all-to-all(bf16[16,8,256]{2,1,0:T(8,128)(2,1)S(1)} %gather_back.1), channel_id=1, replica_groups=mesh['z'=16,'x'=4,'c'=2,'tp'=4] {'z'}, dimensions={0} | all-to-all | bytes 131072 | tf_op jit(solution)/shard_map/all_to_all | solution.py:34
  102.9 0.4 fusion.1
  103.2 0.1 pad_maximum_fusion.2
  103.3 7.7 %all_to_all.34 = f32[4,1,32]{2,1,0:T(1,128)S(1)} all-to-all(f32[4,1,32]{2,1,0:T(1,128)S(1)} %broadcast_in_dim.26), channel_id=1, replica_groups=mesh['z'=16,'x'=4,'c'=2,'tp'=4] {'tp'}, dimensions={0} | all-to-all | bytes 1024 | tf_op jit(solution)/shard_map/all_to_all | solution.py:26
  111.0 0.1 slice_multiply_fusion
  111.1 0.0 copy-done.7
  111.1 0.7 multiply_convert_fusion
  (11 shorter events, 0.1 us)
Async XLA Ops:
  0.0 15.2 %copy-start.6 = (bf16[1024]{0:T(1024)(128)(2,1)S(1)}, bf16[1024]{0:T(1024)(128)(2,1)}, u32[]{:S(2)}) copy-start(bf16[1024]{0:T(1024)(128)(2,1)} %param.44) | copy-start | bytes 6148
  0.0 15.2 %copy-start = (bf16[16,1024]{1,0:T(8,128)(2,1)S(1)}, bf16[16,1024]{1,0:T(8,128)(2,1)}, u32[]{:S(2)}) copy-start(bf16[16,1024]{1,0:T(8,128)(2,1)} %tokens_ref.1) | copy-start | bytes 98308
  0.0 15.2 %copy-start.1 = (f32[1024]{0:T(1024)S(1)}, f32[1024]{0:T(1024)}, u32[]{:S(2)}) copy-start(f32[1024]{0:T(1024)} %param.37) | copy-start | bytes 12292
  0.0 15.2 %copy-start.2 = (s32[16,2]{0,1:T(2,128)S(1)}, s32[16,2]{0,1:T(2,128)}, u32[]{:S(2)}) copy-start(s32[16,2]{0,1:T(2,128)} %param.46) | copy-start | bytes 388
  0.0 15.2 %copy-start.3 = (f32[16,2]{0,1:T(2,128)S(1)}, f32[16,2]{0,1:T(2,128)}, u32[]{:S(2)}) copy-start(f32[16,2]{0,1:T(2,128)} %param.47) | copy-start | bytes 388
  0.0 31.4 %copy-start.4 = (bf16[22,1024]{1,0:T(8,128)(2,1)S(1)}, bf16[22,1024]{1,0:T(8,128)(2,1)}, u32[]{:S(2)}) copy-start(bf16[22,1024]{1,0:T(8,128)(2,1)} %param.41) | copy-start | bytes 135172
  0.0 31.4 %copy-start.5 = (bf16[22,1024]{1,0:T(8,128)(2,1)S(1)}, bf16[22,1024]{1,0:T(8,128)(2,1)}, u32[]{:S(2)}) copy-start(bf16[22,1024]{1,0:T(8,128)(2,1)} %param.42) | copy-start | bytes 135172
  16.2 29.8 %all-to-all-start.1 = ((bf16[16,8,256]{2,1,0:T(8,128)(2,1)}), bf16[16,8,256]{2,1,0:T(8,128)(2,1)S(1)}, u32[]{:S(2)}, u32[]{:S(2)}) async-start(bf16[16,8,256]{2,1,0:T(8,128)(2,1)} %bitcast.8), calls=%async_computation.1 | async-start | bytes 131072 | tf_op jit(solution)/shard_map/all_to_all | solution.py:34
  31.5 21.8 %collective-permute-start = (bf16[24,3072]{1,0:T(8,128)(2,1)S(1)}, bf16[24,3072]{1,0:T(8,128)(2,1)S(1)}, u32[]{:S(2)}, u32[]{:S(2)}) collective-permute-start(bf16[24,3072]{1,0:T(8,128)(2,1)S(1)} %constant_dynamic-update-slice_fusion), channel_id=1, source_target_pairs={{0,64},{32,96},{64,0},{96,32},{128,192},{160,224},{192,128},{224,1... | collective-permute-start | bytes 442376 | tf_op jit(solution)/shard_map/ppermute | solution.py:52
  47.7 18.4 %all-to-all-start.2 = ((bf16[32,48,256]{2,1,0:T(8,128)(2,1)}), bf16[32,48,256]{2,1,0:T(8,128)(2,1)S(1)}, u32[]{:S(2)}, u32[]{:S(2)}) async-start(bf16[32,48,256]{2,1,0:T(8,128)(2,1)} %bitcast.9), calls=%async_computation.2 | async-start | bytes 1572864 | tf_op jit(solution)/shard_map/all_to_all | solution.py:34
  53.3 10.9 %collective-permute-start.1 = (bf16[48,3072]{1,0:T(8,128)(2,1)S(1)}, bf16[48,3072]{1,0:T(8,128)(2,1)S(1)}, u32[]{:S(2)}, u32[]{:S(2)}) collective-permute-start(bf16[48,3072]{1,0:T(8,128)(2,1)S(1)} %pad_maximum_fusion.1), channel_id=1, source_target_pairs={{0,32},{32,0},{64,96},{96,64},{128,160},{160,128},{192,224},{224,1... | collective-permute-start | bytes 884744 | tf_op jit(solution)/shard_map/ppermute | solution.py:52
  68.5 42.5 %copy-start.7 = (f32[256]{0:T(256)S(1)}, f32[256]{0:T(256)}, u32[]{:S(2)}) copy-start(f32[256]{0:T(256)} %param.45) | copy-start | bytes 3076

commit v5 on v4

--- a/solution.py
+++ b/solution.py
@@ -3,6 +3,7 @@
 
 import jax
 import jax.numpy as jnp
+import numpy as np
 from jax import lax
 from jax.experimental import pallas as pl
 from jax.experimental.pallas import tpu as pltpu
@@ -100,12 +101,18 @@
     channel_head = lax.broadcasted_iota(jnp.int32, (width, width), 0) // head_size
     same_head = (
         channel_head == lax.broadcasted_iota(jnp.int32, (width, width), 1) // head_size
-    ).astype(f32)
+    ).astype(jnp.bfloat16)
 
     def over_head(values):
-        return jnp.dot(
-            values, same_head, precision=lax.Precision.HIGHEST, preferred_element_type=f32
+        high = values.astype(jnp.bfloat16)
+        rest = values - high.astype(f32)
+        middle = rest.astype(jnp.bfloat16)
+        low = (rest - middle.astype(f32)).astype(jnp.bfloat16)
+        sums = jnp.dot(
+            jnp.concatenate([high, middle, low], 0), same_head, preferred_element_type=f32
         )
+        size = values.shape[0]
+        return sums[:size] + sums[size : 2 * size] + sums[2 * size :]
 
     decay_low = jnp.tanh(turned(tokens, landed(decay_down_ref)[...])).astype(jnp.bfloat16)
     rate_low = turned(tokens, landed(rate_down_ref)[...]).astype(jnp.bfloat16)
@@ -207,7 +214,7 @@
         w_out,
         own_down,
     ]
-    chunks = 4
+    chunks = 1
     down_rows = own_down.shape[0] + -own_down.shape[0] % 8
     rows = tokens.shape[1] // width * row_count + down_rows
     return pl.pallas_call(
@@ -226,24 +233,11 @@
 
 
 def expert_kernel(
-    rows_ref,
-    units_ref,
-    gate_any,
-    up_any,
-    down_any,
-    out_ref,
-    gate_ref,
-    up_ref,
-    down_ref,
-    arrival,
-    *,
-    rows,
+    rows_ref, units_ref, gate_ref, up_ref, down_any, out_ref, down_ref, arrival, *, rows
 ):
     copies = [
         pltpu.make_async_copy(source, target, arrival.at[i])
-        for i, (source, target) in enumerate(
-            ((gate_any, gate_ref), (up_any, up_ref), (down_any, down_ref))
-        )
+        for i, (source, target) in enumerate(((down_any, down_ref),))
     ]
     for copy in copies:
         copy.start()
@@ -263,21 +257,22 @@
             1,
         )
 
-    dense = whole_rows(rows, height)
-    gate_pre = turned(dense, units_ref[:, :width])
-    up_pre = turned(dense, units_ref[:, width : 2 * width])
-    hidden = (jax.nn.silu(gate_pre) * up_pre).astype(jnp.bfloat16)
-    for i in range(splits):
-        down = units_ref[:, 2 * width + i * quarter : 2 * width + (i + 1) * quarter]
-        part = jnp.dot(hidden, down, preferred_element_type=f32).astype(jnp.bfloat16)
-        out_ref[:, i, rows:, :] = part.reshape(blocks, height - rows, quarter)
+    @pl.when(lax.axis_index("tp") >= 0)
+    def _():
+        dense = whole_rows(rows, height)
+        gate_pre = turned(dense, units_ref[:, :width])
+        up_pre = turned(dense, units_ref[:, width : 2 * width])
+        hidden = (jax.nn.silu(gate_pre) * up_pre).astype(jnp.bfloat16)
+        for i in range(splits):
+            down = units_ref[:, 2 * width + i * quarter : 2 * width + (i + 1) * quarter]
+            part = jnp.dot(hidden, down, preferred_element_type=f32).astype(jnp.bfloat16)
+            out_ref[:, i, rows:, :] = part.reshape(blocks, height - rows, quarter)
+
     routed = whole_rows(0, rows)
-    copies[0].wait()
     gate_pre = turned(routed, gate_ref[...])
-    copies[1].wait()
     up_pre = turned(routed, up_ref[...])
     hidden = (jax.nn.silu(gate_pre) * up_pre).astype(jnp.bfloat16)
-    copies[2].wait()
+    copies[0].wait()
     for i in range(splits):
         down = down_ref[:, i * quarter : (i + 1) * quarter]
         part = jnp.dot(hidden, down, preferred_element_type=f32).astype(jnp.bfloat16)
@@ -285,17 +280,19 @@
 
 
 def run_experts(everything, units, expert_gate, expert_up, expert_down, rows):
-    far = [expert_gate.T, expert_up.T, expert_down]
     vmem = pl.BlockSpec(memory_space=pltpu.VMEM)
+    held = [everything, units, expert_gate.T, expert_up.T]
+    far = [expert_down]
     return pl.pallas_call(
         partial(expert_kernel, rows=rows),
         out_shape=pltpu.VMEM(everything.shape, jnp.bfloat16),
-        in_specs=[vmem, vmem] + [pl.BlockSpec(memory_space=pl.ANY)] * len(far),
+        in_specs=[vmem] * len(held) + [pl.BlockSpec(memory_space=pl.ANY)] * len(far),
         out_specs=vmem,
         scratch_shapes=[pltpu.VMEM(a.shape, a.dtype) for a in far]
         + [pltpu.SemaphoreType.DMA((len(far),))],
+        input_output_aliases={0: 0},
         name="experts",
-    )(on_chip(everything), on_chip(units), *far)
+    )(*[on_chip(a) for a in held], *far)
 
 
 def on_chip(value):
@@ -407,42 +404,54 @@
     )
 
 
-def fan_kernel(arrived_ref, out_ref, *, capacity, shared):
-    planes, slots_part, quarter = arrived_ref.shape
-    here, copies, splits, height, _ = out_ref.shape
+def fan_choice(planes, slots_part, capacity, here, splits, shared):
     part = slots_part - here * capacity
     rows = planes * capacity
-    shape = (here * splits * height, planes * slots_part)
-    line = lax.broadcasted_iota(jnp.int32, shape, 0)
-    column = lax.broadcasted_iota(jnp.int32, shape, 1)
-    index, group = line % height, line // height
-    expert, split = group // splits, group % splits
-    dense = index - rows
-    routed_from = index // capacity * slots_part + expert * capacity + index % capacity
-    dense_from = (
-        (split * shared + dense // part) * slots_part + here * capacity + dense % part
-    )
-    chosen = (column == jnp.where(index < rows, routed_from, dense_from)).astype(jnp.bfloat16)
-    arrived = arrived_ref[...].reshape(planes * slots_part, quarter)
-    laid = jnp.dot(chosen, arrived, preferred_element_type=jnp.float32).astype(jnp.bfloat16)
+    index = np.arange(rows + shared * part)
+    choice = np.zeros((here, splits, len(index), planes * slots_part), np.float32)
     for e in range(here):
         for i in range(splits):
-            at = (e * splits + i) * height
-            for c in range(copies):
-                out_ref[e, c, i, :, :] = laid[at : at + height]
+            dense = index - rows
+            routed_from = index // capacity * slots_part + e * capacity + index % capacity
+            dense_from = (
+                (i * shared + dense // part) * slots_part + here * capacity + dense % part
+            )
+            choice[e, i, index, np.where(index < rows, routed_from, dense_from)] = 1
+    return choice.reshape(here * splits * len(index), planes * slots_part)
+
+
+def fan_kernel(arrived_ref, choice_ref, out_any, laid_ref, sent):
+    planes, slots_part, quarter = arrived_ref.shape
+    here, copies, splits, height, _ = out_any.shape
+    arrived = arrived_ref[...].reshape(planes * slots_part, quarter)
+    started = []
+    for e in range(here):
+        size = splits * height
+        laid = jnp.dot(
+            choice_ref[e * size : (e + 1) * size, :], arrived, preferred_element_type=jnp.float32
+        ).astype(jnp.bfloat16)
+        for c in range(copies):
+            laid_ref[e, c] = laid.reshape(splits, height, quarter)
+        started.append(pltpu.make_async_copy(laid_ref.at[e], out_any.at[e], sent.at[e]))
+        started[e].start()
+    for copy in started:
+        copy.wait()
 
 
 def fan_out(arrived, capacity, here, copies, splits, shared):
     planes, slots_part, quarter = arrived.shape
-    height = planes * capacity + shared * (slots_part - here * capacity)
+    choice = fan_choice(planes, slots_part, capacity, here, splits, shared)
+    height = choice.shape[0] // (here * splits)
     vmem = pl.BlockSpec(memory_space=pltpu.VMEM)
+    shape = (here, copies, splits, height, quarter)
     return pl.pallas_call(
-        partial(fan_kernel, capacity=capacity, shared=shared),
-        out_shape=pltpu.VMEM((here, copies, splits, height, quarter), jnp.bfloat16),
-        in_specs=[vmem],
-        out_specs=vmem,
+        fan_kernel,
+        out_shape=jax.ShapeDtypeStruct(shape, jnp.bfloat16),
+        in_specs=[vmem, vmem],
+        out_specs=pl.BlockSpec(memory_space=pl.ANY),
+        scratch_shapes=[pltpu.VMEM(shape, jnp.bfloat16), pltpu.SemaphoreType.DMA((here,))],
         name="fan_out",
-    )(on_chip(arrived))
+    )(on_chip(arrived), on_chip(jnp.asarray(choice, jnp.bfloat16)))
 
 
 def gather_kernel(returned_ref, out_ref, *, capacity, here, splits, shared):
@@ -546,8 +555,10 @@
         head_gain,
     )
     everyone = exchange(message, "tp")
-    everyone, dense_gate, dense_up, branch_gate = lax.optimization_barrier(
-        (everyone, dense_gate, dense_up, branch_gate)
+    everyone, dense_gate, dense_up, branch_gate, expert_gate, expert_up, expert_down = (
+        lax.optimization_barrier(
+            (everyone, dense_gate, dense_up, branch_gate, expert_gate, expert_up, expert_down)
+        )
     )
     mix_rows = tp_size * row_count
     units = jnp.concatenate(

time: 112 us -> 110 us (0.982)
  Pallas kernels: 9.95 us -> 7.69 us
where the time goes in v5:
time: 110 us
  blocking collectives  52.4 us (48%)
  starting transfers between devices  27.6 us (25%)
  waiting for transfers between devices  20.4 us (19%)
  Pallas kernels  7.69 us (7%)
    all_to_all x3, blocking collectives, exchange(): return lax.all_to_all(parts, axis, split_axis=0, concat_axis=0, tiled=True)  44.7 us
    all_to_all x2, starting transfers between devices, exchange(): return lax.all_to_all(parts, axis, split_axis=0, concat_axis=0, tiled=True)  20.8 us
    all_to_all x2, waiting for transfers between devices, exchange(): return lax.all_to_all(parts, axis, split_axis=0, concat_axis=0, tiled=True)  11.4 us
    ppermute x2, waiting for transfers between devices, with_neighbour(): other = lax.ppermute(units, 'z', [(i, i ^ step) for i in range(planes)])  9 us
    all_to_all x1, blocking collectives, sent_to_all(): return lax.all_to_all(copies, axis, split_axis=0, concat_axis=0, tiled=True)  7.66 us
    ppermute x2, starting transfers between devices, with_neighbour(): other = lax.ppermute(units, 'z', [(i, i ^ step) for i in range(planes)])  6.78 us
    pallas_call x1, Pallas kernels, mixer_message(): pl.pallas_call(partial(mixer_kernel, chunks=chunks), out_shape=pltpu.VMEM...  3.68 us
  transfers between devices with their start and end apart: 4, of which 3 were waited for; matrix products, arithmetic and copies ran while one was open for 0% of the time, Pallas kernels for 1%

profile of v5, /device:TPU:2, one launch (start us, length us, event | category | flops | bytes accessed | tf_op | source)
XLA Modules:
  0.0 109.7 jit_solution(2451633954258834010)
XLA Ops:
  0.0 0.0 copy-start.9
  0.0 0.0 copy-start.2
  0.0 0.0 copy-start.4
  0.0 0.0 copy-start.5
  0.0 0.0 copy-start.6
  0.0 0.0 copy-start.7
  0.0 0.0 copy-start.8
  0.0 0.0 copy-start.3
  0.1 3.7 %mixer.1 = bf16[4,88,256]{2,1,0:T(8,128)(2,1)S(1)} custom-call(bf16[16,1024]{1,0:T(8,128)(2,1)} %tokens_ref.1, bf16[64,1024]{1,0:T(8,128)(2,1)} %bitcast.43, bf16[64,1024]{1,0:T(8,128)(2,1)} %bitcast.44, bf16[64,256]{1,0:T(8,128)(2,1)} %refs_3_.1, f32[1,256]{1,0:T(1,128)} %bitcast.46, bf16[64,256]{1,0:T(8,128)(2,1)} %refs_5_.1, f32[1,256]{1,0:T(1,128)} %bitcast.47, ...), custom_call_target="tpu_custom_call" | custom-call | tf_op jit(solution)/shard_map/mixer/pallas_call | solution.py:220
  3.7 10.5 %all_to_all.31.everyone_ref = bf16[4,88,256]{2,1,0:T(8,128)(2,1)S(1)} all-to-all(bf16[4,88,256]{2,1,0:T(8,128)(2,1)S(1)} %mixer.1), channel_id=1, replica_groups=mesh['z'=16,'x'=4,'c'=2,'tp'=4] {'tp'}, dimensions={0} | all-to-all | bytes 360448 | tf_op jit(solution)/shard_map/all_to_all | solution.py:35
  14.2 0.0 copy-done.9
  14.3 0.0 copy-done.2
  14.3 0.0 copy-done.4
  14.3 0.0 copy-done.5
  14.3 0.0 copy-done.6
  14.3 1.0 norm_and_pack.1
  15.3 15.2 %all-to-all-start.1 = ((bf16[16,8,256]{2,1,0:T(8,128)(2,1)}), bf16[16,8,256]{2,1,0:T(8,128)(2,1)S(1)}, u32[]{:S(2)}, u32[]{:S(2)}) async-start(bf16[16,8,256]{2,1,0:T(8,128)(2,1)} %bitcast.8), calls=%async_computation.1 | async-start | bytes 131072 | tf_op jit(solution)/shard_map/all_to_all | solution.py:35
  30.5 0.0 copy-done.7
  30.5 0.0 copy-done.8
  30.6 4.7 %collective-permute-start = (bf16[24,3072]{1,0:T(8,128)(2,1)S(1)}, bf16[24,3072]{1,0:T(8,128)(2,1)S(1)}, u32[]{:S(2)}, u32[]{:S(2)}) collective-permute-start(bf16[24,3072]{1,0:T(8,128)(2,1)S(1)} %constant_dynamic-update-slice_fusion), channel_id=1, source_target_pairs={{0,64},{32,96},{64,0},{96,32},{128,192},{160,224},{192,128},{224,1... | collective-permute-start | bytes 442376 | tf_op jit(solution)/shard_map/ppermute | solution.py:53
  35.3 9.8 %all-to-all-done.1.arrived_ref = bf16[16,8,256]{2,1,0:T(8,128)(2,1)S(1)} async-done(((bf16[16,8,256]{2,1,0:T(8,128)(2,1)}), bf16[16,8,256]{2,1,0:T(8,128)(2,1)S(1)}, u32[]{:S(2)}, u32[]{:S(2)}) %all-to-all-start.1) | async-done | bytes 65568 | tf_op jit(solution)/shard_map/all_to_all | solution.py:35
  45.1 0.0 copy-done.3
  45.1 1.1 %fan_out.1 = bf16[2,4,4,48,256]{4,3,2,1,0:T(8,128)(2,1)} custom-call(bf16[16,8,256]{2,1,0:T(8,128)(2,1)S(1)} %all-to-all-done.1.arrived_ref, bf16[384,128]{1,0:T(8,128)(2,1)S(1)} %copy-done.3), custom_call_target="tpu_custom_call" | custom-call | tf_op jit(solution)/shard_map/fan_out/pallas_call | solution.py:447
  46.2 5.6 %all-to-all-start.2 = ((bf16[32,48,256]{2,1,0:T(8,128)(2,1)}), bf16[32,48,256]{2,1,0:T(8,128)(2,1)S(1)}, u32[]{:S(2)}, u32[]{:S(2)}) async-start(bf16[32,48,256]{2,1,0:T(8,128)(2,1)} %bitcast.41), calls=%async_computation.2 | async-start | bytes 1572864 | tf_op jit(solution)/shard_map/all_to_all | solution.py:35
  51.9 0.0 copy-start
  51.9 0.0 copy-start.1
  51.9 0.0 collective-permute-done
  51.9 2.1 %collective-permute-start.1 = (bf16[48,3072]{1,0:T(8,128)(2,1)S(1)}, bf16[48,3072]{1,0:T(8,128)(2,1)S(1)}, u32[]{:S(2)}, u32[]{:S(2)}) collective-permute-start(bf16[48,3072]{1,0:T(8,128)(2,1)S(1)} %pad_maximum_fusion.1), channel_id=1, source_target_pairs={{0,32},{32,0},{64,96},{96,64},{128,160},{160,128},{192,224},{224,1... | collective-permute-start | bytes 884744 | tf_op jit(solution)/shard_map/ppermute | solution.py:53
  54.0 9.0 %collective-permute-done.1 = bf16[48,3072]{1,0:T(8,128)(2,1)S(1)} collective-permute-done((bf16[48,3072]{1,0:T(8,128)(2,1)S(1)}, bf16[48,3072]{1,0:T(8,128)(2,1)S(1)}, u32[]{:S(2)}, u32[]{:S(2)}) %collective-permute-start.1) | collective-permute-done | bytes 294944 | tf_op jit(solution)/shard_map/ppermute | solution.py:53
  63.0 1.6 %all-to-all-done.2 = bf16[32,48,256]{2,1,0:T(8,128)(2,1)S(1)} async-done(((bf16[32,48,256]{2,1,0:T(8,128)(2,1)}), bf16[32,48,256]{2,1,0:T(8,128)(2,1)S(1)}, u32[]{:S(2)}, u32[]{:S(2)}) %all-to-all-start.2) | async-done | bytes 786464 | tf_op jit(solution)/shard_map/all_to_all | solution.py:35
  64.6 0.0 copy-done
  64.6 0.0 copy-done.1
  64.6 1.7 %experts.1 = bf16[8,4,48,256]{3,2,1,0:T(8,128)(2,1)S(1)} custom-call(bf16[8,4,48,256]{3,2,1,0:T(8,128)(2,1)S(1)} %bitcast.34, bf16[96,3072]{1,0:T(8,128)(2,1)S(1)} %pad_maximum_fusion.units_ref, bf16[352,1024]{1,0:T(8,128)(2,1)S(1)} %bitcast.36, bf16[352,1024]{1,0:T(8,128)(2,1)S(1)} %bitcast.37, ...), custom_call_target="tpu_custom_call", output_to_operand_aliasing={{}: (0, {})} | custom-call | tf_op jit(solution)/shard_map/experts/pallas_call | solution.py:286
  66.3 0.0 copy-start.10
  66.3 18.4 %all_to_all.32.returned_ref = bf16[32,48,256]{2,1,0:T(8,128)(2,1)S(1)} all-to-all(bf16[32,48,256]{2,1,0:T(8,128)(2,1)S(1)} %bitcast.35), channel_id=1, replica_groups=mesh['z'=16,'x'=4,'c'=2,'tp'=4] {'x','c','tp'}, dimensions={0} | all-to-all | bytes 1572864 | tf_op jit(solution)/shard_map/all_to_all | solution.py:35
  84.7 0.3 gather_back.1
  85.0 15.8 %all_to_all.33 = bf16[16,8,256]{2,1,0:T(8,128)(2,1)S(1)} all-to-all(bf16[16,8,256]{2,1,0:T(8,128)(2,1)S(1)} %gather_back.1), channel_id=1, replica_groups=mesh['z'=16,'x'=4,'c'=2,'tp'=4] {'z'}, dimensions={0} | all-to-all | bytes 131072 | tf_op jit(solution)/shard_map/all_to_all | solution.py:35
  100.8 0.4 fusion.1
  101.2 0.1 pad_maximum_fusion.2
  101.3 7.7 %all_to_all.34 = f32[4,1,32]{2,1,0:T(1,128)S(1)} all-to-all(f32[4,1,32]{2,1,0:T(1,128)S(1)} %broadcast_in_dim.26), channel_id=1, replica_groups=mesh['z'=16,'x'=4,'c'=2,'tp'=4] {'tp'}, dimensions={0} | all-to-all | bytes 1024 | tf_op jit(solution)/shard_map/all_to_all | solution.py:27
  108.9 0.1 slice_multiply_fusion
  109.0 0.0 copy-done.10
  109.0 0.7 multiply_convert_fusion
  (11 shorter events, 0.1 us)
Async XLA Ops:
  0.0 14.3 %copy-start.9 = (bf16[1024]{0:T(1024)(128)(2,1)S(1)}, bf16[1024]{0:T(1024)(128)(2,1)}, u32[]{:S(2)}) copy-start(bf16[1024]{0:T(1024)(128)(2,1)} %param.45) | copy-start | bytes 6148
  0.0 14.3 %copy-start.2 = (bf16[16,1024]{1,0:T(8,128)(2,1)S(1)}, bf16[16,1024]{1,0:T(8,128)(2,1)}, u32[]{:S(2)}) copy-start(bf16[16,1024]{1,0:T(8,128)(2,1)} %tokens_ref.1) | copy-start | bytes 98308
  0.0 14.3 %copy-start.4 = (f32[1024]{0:T(1024)S(1)}, f32[1024]{0:T(1024)}, u32[]{:S(2)}) copy-start(f32[1024]{0:T(1024)} %param.38) | copy-start | bytes 12292
  0.0 14.3 %copy-start.5 = (s32[16,2]{0,1:T(2,128)S(1)}, s32[16,2]{0,1:T(2,128)}, u32[]{:S(2)}) copy-start(s32[16,2]{0,1:T(2,128)} %param.47) | copy-start | bytes 388
  0.0 14.3 %copy-start.6 = (f32[16,2]{0,1:T(2,128)S(1)}, f32[16,2]{0,1:T(2,128)}, u32[]{:S(2)}) copy-start(f32[16,2]{0,1:T(2,128)} %param.48) | copy-start | bytes 388
  0.0 30.5 %copy-start.7 = (bf16[22,1024]{1,0:T(8,128)(2,1)S(1)}, bf16[22,1024]{1,0:T(8,128)(2,1)}, u32[]{:S(2)}) copy-start(bf16[22,1024]{1,0:T(8,128)(2,1)} %param.42) | copy-start | bytes 135172
  0.0 30.5 %copy-start.8 = (bf16[22,1024]{1,0:T(8,128)(2,1)S(1)}, bf16[22,1024]{1,0:T(8,128)(2,1)}, u32[]{:S(2)}) copy-start(bf16[22,1024]{1,0:T(8,128)(2,1)} %param.43) | copy-start | bytes 135172
  0.0 45.1 %copy-start.3 = (bf16[384,128]{1,0:T(8,128)(2,1)S(1)}, bf16[384,128]{1,0:T(8,128)(2,1)}, u32[]{:S(2)}) copy-start(bf16[384,128]{1,0:T(8,128)(2,1)} %constant.15.clone.choice_ref) | copy-start | bytes 294916
  15.3 29.8 %all-to-all-start.1 = ((bf16[16,8,256]{2,1,0:T(8,128)(2,1)}), bf16[16,8,256]{2,1,0:T(8,128)(2,1)S(1)}, u32[]{:S(2)}, u32[]{:S(2)}) async-start(bf16[16,8,256]{2,1,0:T(8,128)(2,1)} %bitcast.8), calls=%async_computation.1 | async-start | bytes 131072 | tf_op jit(solution)/shard_map/all_to_all | solution.py:35
  30.6 21.3 %collective-permute-start = (bf16[24,3072]{1,0:T(8,128)(2,1)S(1)}, bf16[24,3072]{1,0:T(8,128)(2,1)S(1)}, u32[]{:S(2)}, u32[]{:S(2)}) collective-permute-start(bf16[24,3072]{1,0:T(8,128)(2,1)S(1)} %constant_dynamic-update-slice_fusion), channel_id=1, source_target_pairs={{0,64},{32,96},{64,0},{96,32},{128,192},{160,224},{192,128},{224,1... | collective-permute-start | bytes 442376 | tf_op jit(solution)/shard_map/ppermute | solution.py:53
  46.2 18.4 %all-to-all-start.2 = ((bf16[32,48,256]{2,1,0:T(8,128)(2,1)}), bf16[32,48,256]{2,1,0:T(8,128)(2,1)S(1)}, u32[]{:S(2)}, u32[]{:S(2)}) async-start(bf16[32,48,256]{2,1,0:T(8,128)(2,1)} %bitcast.41), calls=%async_computation.2 | async-start | bytes 1572864 | tf_op jit(solution)/shard_map/all_to_all | solution.py:35
  51.9 12.8 %copy-start = (bf16[1,1024,352]{1,2,0:T(8,128)(2,1)S(1)}, bf16[1,1024,352]{1,2,0:T(8,128)(2,1)}, u32[]{:S(2)}) copy-start(bf16[1,1024,352]{1,2,0:T(8,128)(2,1)} %param.39) | copy-start | bytes 2162692
  51.9 12.8 %copy-start.1 = (bf16[1,1024,352]{1,2,0:T(8,128)(2,1)S(1)}, bf16[1,1024,352]{1,2,0:T(8,128)(2,1)}, u32[]{:S(2)}) copy-start(bf16[1,1024,352]{1,2,0:T(8,128)(2,1)} %param.40) | copy-start | bytes 2162692
  51.9 11.1 %collective-permute-start.1 = (bf16[48,3072]{1,0:T(8,128)(2,1)S(1)}, bf16[48,3072]{1,0:T(8,128)(2,1)S(1)}, u32[]{:S(2)}, u32[]{:S(2)}) collective-permute-start(bf16[48,3072]{1,0:T(8,128)(2,1)S(1)} %pad_maximum_fusion.1), channel_id=1, source_target_pairs={{0,32},{32,0},{64,96},{96,64},{128,160},{160,128},{192,224},{224,1... | collective-permute-start | bytes 884744 | tf_op jit(solution)/shard_map/ppermute | solution.py:53
  66.3 42.7 %copy-start.10 = (f32[256]{0:T(256)S(1)}, f32[256]{0:T(256)}, u32[]{:S(2)}) copy-start(f32[256]{0:T(256)} %param.46) | copy-start | bytes 3076

commit v6 on v5

--- a/solution.py
+++ b/solution.py
@@ -54,40 +54,22 @@
     return jnp.concatenate([units, other], 0)
 
 
-def mixer_kernel(*refs, chunks):
-    count = (len(refs) - 4) // 2
-    sources, message_ref, targets = refs[:count], refs[count], refs[count + 1 : 2 * count + 1]
-    query_ref, answer_ref, arrival = refs[2 * count + 1 :]
-    (
-        tokens_ref,
-        decay_down_ref,
-        rate_down_ref,
-        decay_up_ref,
-        decay_base_ref,
-        rate_up_ref,
-        rate_base_ref,
-        w_key_ref,
-        w_recep_ref,
-        state_ref,
-        w_value_ref,
-        head_gain_ref,
-        w_out_ref,
-        down_ref,
-    ) = targets
-    copies = {}
-    for source, target in zip(sources, targets):
-        parts = chunks if target is state_ref else 1
-        size = target.shape[0] // parts
-        for i in range(parts):
-            at = pl.ds(i * size, size) if parts > 1 else slice(None)
-            copies[id(target), i] = pltpu.make_async_copy(
-                source.at[at], target.at[at], arrival.at[len(copies)]
-            )
-    for copy in copies.values():
-        copy.start()
-
-    def landed(target, part=0):
-        copies[id(target), part].wait()
+def mixer_kernel(*refs, groups):
+    count = sum(groups)
+    sources, message_ref = refs[:count], refs[count]
+    targets = refs[count + 1 : count + 1 + len(groups)]
+    query_ref, answer_ref, arrival = refs[count + 1 + len(groups) :]
+    tokens_ref, low_ref, up_ref, base_ref, w_ref, state_ref, gain_ref, w_out_ref, down_ref = targets
+    at = 0
+    for group, (target, members) in enumerate(zip(targets, groups)):
+        for i in range(members):
+            part = target if members == 1 else target.at[i]
+            pltpu.make_async_copy(sources[at], part, arrival.at[group]).start()
+            at += 1
+
+    def landed(target):
+        group = [i for i, other in enumerate(targets) if other is target][0]
+        pltpu.make_async_copy(target, target, arrival.at[group]).wait()
         return target
 
     row_count, heads, head_size = state_ref.shape[0], state_ref.shape[1], state_ref.shape[3]
@@ -114,18 +96,18 @@
         size = values.shape[0]
         return sums[:size] + sums[size : 2 * size] + sums[2 * size :]
 
-    decay_low = jnp.tanh(turned(tokens, landed(decay_down_ref)[...])).astype(jnp.bfloat16)
-    rate_low = turned(tokens, landed(rate_down_ref)[...]).astype(jnp.bfloat16)
-    decay_pre = landed(decay_base_ref)[...] + jnp.dot(
-        decay_low, landed(decay_up_ref)[...], preferred_element_type=f32
+    decay_low = jnp.tanh(turned(tokens, landed(low_ref)[0])).astype(jnp.bfloat16)
+    rate_low = turned(tokens, low_ref[1]).astype(jnp.bfloat16)
+    decay_pre = landed(base_ref)[0] + jnp.dot(
+        decay_low, landed(up_ref)[0], preferred_element_type=f32
     )
     decay = jnp.exp(-(math.exp(-0.5) * jax.nn.sigmoid(decay_pre)))
     in_rate = jax.nn.sigmoid(
-        landed(rate_base_ref)[...]
-        + jnp.dot(rate_low, landed(rate_up_ref)[...], preferred_element_type=f32)
-    )
-    key_vecs = jnp.dot(tokens, landed(w_key_ref)[...], preferred_element_type=f32)
-    recep = jnp.dot(tokens, landed(w_recep_ref)[...], preferred_element_type=f32)
+        base_ref[1]
+        + jnp.dot(rate_low, up_ref[1], preferred_element_type=f32)
+    )
+    key_vecs = jnp.dot(tokens, landed(w_ref)[0], preferred_element_type=f32)
+    recep = jnp.dot(tokens, w_ref[1], preferred_element_type=f32)
     sums = over_head(
         jnp.concatenate([key_vecs * key_vecs, key_vecs * in_rate * recep, key_vecs * recep], 0)
     )
@@ -138,9 +120,8 @@
             query_ref[pl.ds(which * heads + h, row_count, stride=2 * heads), :] = (
                 pair if h % 2 == 0 else pltpu.roll(pair, head_size, 1)
             )
+    landed(state_ref)
     for t in range(row_count):
-        if t % (row_count // chunks) == 0:
-            landed(state_ref, t // (row_count // chunks))
         queries = query_ref[2 * heads * t : 2 * heads * (t + 1), :head_size].astype(jnp.bfloat16)
         matrix = state_ref[t].reshape(width, head_size).astype(jnp.bfloat16)
         answers = turned(queries, matrix)
@@ -161,11 +142,11 @@
             pairs.append(jnp.where(first_of_pair, rows[0], rows[1]))
         return jnp.concatenate(pairs, 1)
 
-    value_vecs = jnp.dot(tokens, landed(w_value_ref)[...], preferred_element_type=f32)
+    value_vecs = jnp.dot(tokens, w_ref[2], preferred_element_type=f32)
     read_out = picked(0) - picked(1) * removed_factor + value_vecs * value_factor
     centred = read_out - over_head(read_out) * (1.0 / head_size)
     spread = over_head(centred * centred) * (1.0 / head_size)
-    normed = centred * lax.rsqrt(spread + head_epsilon) * landed(head_gain_ref)[...]
+    normed = centred * lax.rsqrt(spread + head_epsilon) * landed(gain_ref)[...]
     mixed = jnp.dot(normed.astype(jnp.bfloat16), landed(w_out_ref)[...], preferred_element_type=f32)
     mixed = mixed.astype(jnp.bfloat16)
     copies_out, mix_rows = message_ref.shape[0], row_count * heads
@@ -199,37 +180,34 @@
     row_count, heads, head_size = state.shape[0], state.shape[1], state.shape[3]
     width = heads * head_size
     far = [
-        tokens,
-        decay_down.T,
-        rate_down.T,
-        decay_up,
-        decay_base[None],
-        rate_up,
-        rate_base[None],
-        w_key,
-        w_recep,
-        state,
-        w_value,
-        head_gain[None],
-        w_out,
-        own_down,
+        [tokens],
+        [decay_down.T, rate_down.T],
+        [decay_up, rate_up],
+        [decay_base[None], rate_base[None]],
+        [w_key, w_recep, w_value],
+        [state],
+        [head_gain[None]],
+        [w_out],
+        [own_down],
     ]
-    chunks = 1
     down_rows = own_down.shape[0] + -own_down.shape[0] % 8
     rows = tokens.shape[1] // width * row_count + down_rows
     return pl.pallas_call(
-        partial(mixer_kernel, chunks=chunks),
+        partial(mixer_kernel, groups=[len(group) for group in far]),
         out_shape=pltpu.VMEM((copies_out, rows, width), jnp.bfloat16),
-        in_specs=[pl.BlockSpec(memory_space=pl.ANY)] * len(far),
+        in_specs=[pl.BlockSpec(memory_space=pl.ANY)] * sum(len(group) for group in far),
         out_specs=pl.BlockSpec(memory_space=pltpu.VMEM),
-        scratch_shapes=[pltpu.VMEM(a.shape, a.dtype) for a in far]
+        scratch_shapes=[
+            pltpu.VMEM((len(g), *g[0].shape) if len(g) > 1 else g[0].shape, g[0].dtype)
+            for g in far
+        ]
         + [
             pltpu.VMEM((2 * heads * row_count, 128), jnp.float32),
             pltpu.VMEM((heads // 2, 2 * heads * row_count, 128), jnp.float32),
-            pltpu.SemaphoreType.DMA((len(far) - 1 + chunks,)),
+            pltpu.SemaphoreType.DMA((len(far),)),
         ],
         name="mixer",
-    )(*far)
+    )(*[a for group in far for a in group])
 
 
 def expert_kernel(

time: 110 us -> 110 us (level)
  no operation moved by 1% of the time
where the time goes in v6:
time: 110 us; the launch traced here: 109 us
  blocking collectives  52.4 us (48%)
  starting transfers between devices  27.6 us (25%)
  waiting for transfers between devices  20.4 us (19%)
  Pallas kernels  7.43 us (7%)
    all_to_all x3, blocking collectives, exchange(): return lax.all_to_all(parts, axis, split_axis=0, concat_axis=0, tiled=True)  44.7 us
    all_to_all x2, starting transfers between devices, exchange(): return lax.all_to_all(parts, axis, split_axis=0, concat_axis=0, tiled=True)  20.8 us
    all_to_all x2, waiting for transfers between devices, exchange(): return lax.all_to_all(parts, axis, split_axis=0, concat_axis=0, tiled=True)  11.4 us
    ppermute x2, waiting for transfers between devices, with_neighbour(): other = lax.ppermute(units, 'z', [(i, i ^ step) for i in range(planes)])  9 us
    all_to_all x1, blocking collectives, sent_to_all(): return lax.all_to_all(copies, axis, split_axis=0, concat_axis=0, tiled=True)  7.66 us
    ppermute x2, starting transfers between devices, with_neighbour(): other = lax.ppermute(units, 'z', [(i, i ^ step) for i in range(planes)])  6.78 us
    pallas_call x1, Pallas kernels, mixer_message(): pl.pallas_call(partial(mixer_kernel, groups=[len(group) for group in far]...  3.42 us
  transfers between devices with their start and end apart: 4, of which 3 were waited for; matrix products, arithmetic and copies ran while one was open for 0% of the time, Pallas kernels for 1%

profile of v6, /device:TPU:2, one launch (start us, length us, event | category | flops | bytes accessed | tf_op | source)
XLA Modules:
  0.0 109.4 jit_solution(8688302903091431011)
XLA Ops:
  0.0 0.0 copy-start.9
  0.0 0.0 copy-start.2
  0.0 0.0 copy-start.4
  0.0 0.0 copy-start.5
  0.0 0.0 copy-start.6
  0.0 0.0 copy-start.7
  0.0 0.0 copy-start.8
  0.0 0.0 copy-start.3
  0.1 3.4 %mixer.1 = bf16[4,88,256]{2,1,0:T(8,128)(2,1)S(1)} custom-call(bf16[16,1024]{1,0:T(8,128)(2,1)} %tokens_ref.1, bf16[64,1024]{1,0:T(8,128)(2,1)} %bitcast.43, bf16[64,1024]{1,0:T(8,128)(2,1)} %bitcast.44, bf16[64,256]{1,0:T(8,128)(2,1)} %refs_3_.1, bf16[64,256]{1,0:T(8,128)(2,1)} %refs_4_.1, f32[1,256]{1,0:T(1,128)} %bitcast.46, f32[1,256]{1,0:T(1,128)} %bitcast.47, ...), custom_call_target="tpu_custom_call" | custom-call | tf_op jit(solution)/shard_map/mixer/pallas_call | solution.py:195
  3.5 10.5 %all_to_all.31.everyone_ref = bf16[4,88,256]{2,1,0:T(8,128)(2,1)S(1)} all-to-all(bf16[4,88,256]{2,1,0:T(8,128)(2,1)S(1)} %mixer.1), channel_id=1, replica_groups=mesh['z'=16,'x'=4,'c'=2,'tp'=4] {'tp'}, dimensions={0} | all-to-all | bytes 360448 | tf_op jit(solution)/shard_map/all_to_all | solution.py:35
  14.0 0.0 copy-done.9
  14.0 0.0 copy-done.2
  14.0 0.0 copy-done.4
  14.0 0.0 copy-done.5
  14.0 0.0 copy-done.6
  14.0 1.0 norm_and_pack.1
  15.0 15.2 %all-to-all-start.1 = ((bf16[16,8,256]{2,1,0:T(8,128)(2,1)}), bf16[16,8,256]{2,1,0:T(8,128)(2,1)S(1)}, u32[]{:S(2)}, u32[]{:S(2)}) async-start(bf16[16,8,256]{2,1,0:T(8,128)(2,1)} %bitcast.8), calls=%async_computation.1 | async-start | bytes 131072 | tf_op jit(solution)/shard_map/all_to_all | solution.py:35
  30.2 0.0 copy-done.7
  30.3 0.0 copy-done.8
  30.3 4.7 %collective-permute-start = (bf16[24,3072]{1,0:T(8,128)(2,1)S(1)}, bf16[24,3072]{1,0:T(8,128)(2,1)S(1)}, u32[]{:S(2)}, u32[]{:S(2)}) collective-permute-start(bf16[24,3072]{1,0:T(8,128)(2,1)S(1)} %constant_dynamic-update-slice_fusion), channel_id=1, source_target_pairs={{0,64},{32,96},{64,0},{96,32},{128,192},{160,224},{192,128},{224,1... | collective-permute-start | bytes 442376 | tf_op jit(solution)/shard_map/ppermute | solution.py:53
  35.1 9.8 %all-to-all-done.1.arrived_ref = bf16[16,8,256]{2,1,0:T(8,128)(2,1)S(1)} async-done(((bf16[16,8,256]{2,1,0:T(8,128)(2,1)}), bf16[16,8,256]{2,1,0:T(8,128)(2,1)S(1)}, u32[]{:S(2)}, u32[]{:S(2)}) %all-to-all-start.1) | async-done | bytes 65568 | tf_op jit(solution)/shard_map/all_to_all | solution.py:35
  44.9 0.0 copy-done.3
  44.9 1.1 %fan_out.1 = bf16[2,4,4,48,256]{4,3,2,1,0:T(8,128)(2,1)} custom-call(bf16[16,8,256]{2,1,0:T(8,128)(2,1)S(1)} %all-to-all-done.1.arrived_ref, bf16[384,128]{1,0:T(8,128)(2,1)S(1)} %copy-done.3), custom_call_target="tpu_custom_call" | custom-call | tf_op jit(solution)/shard_map/fan_out/pallas_call | solution.py:425
  46.0 5.6 %all-to-all-start.2 = ((bf16[32,48,256]{2,1,0:T(8,128)(2,1)}), bf16[32,48,256]{2,1,0:T(8,128)(2,1)S(1)}, u32[]{:S(2)}, u32[]{:S(2)}) async-start(bf16[32,48,256]{2,1,0:T(8,128)(2,1)} %bitcast.41), calls=%async_computation.2 | async-start | bytes 1572864 | tf_op jit(solution)/shard_map/all_to_all | solution.py:35
  51.6 0.0 copy-start
  51.6 0.0 copy-start.1
  51.6 0.0 collective-permute-done
  51.7 2.1 %collective-permute-start.1 = (bf16[48,3072]{1,0:T(8,128)(2,1)S(1)}, bf16[48,3072]{1,0:T(8,128)(2,1)S(1)}, u32[]{:S(2)}, u32[]{:S(2)}) collective-permute-start(bf16[48,3072]{1,0:T(8,128)(2,1)S(1)} %pad_maximum_fusion.1), channel_id=1, source_target_pairs={{0,32},{32,0},{64,96},{96,64},{128,160},{160,128},{192,224},{224,1... | collective-permute-start | bytes 884744 | tf_op jit(solution)/shard_map/ppermute | solution.py:53
  53.7 9.0 %collective-permute-done.1 = bf16[48,3072]{1,0:T(8,128)(2,1)S(1)} collective-permute-done((bf16[48,3072]{1,0:T(8,128)(2,1)S(1)}, bf16[48,3072]{1,0:T(8,128)(2,1)S(1)}, u32[]{:S(2)}, u32[]{:S(2)}) %collective-permute-start.1) | collective-permute-done | bytes 294944 | tf_op jit(solution)/shard_map/ppermute | solution.py:53
  62.8 1.6 %all-to-all-done.2 = bf16[32,48,256]{2,1,0:T(8,128)(2,1)S(1)} async-done(((bf16[32,48,256]{2,1,0:T(8,128)(2,1)}), bf16[32,48,256]{2,1,0:T(8,128)(2,1)S(1)}, u32[]{:S(2)}, u32[]{:S(2)}) %all-to-all-start.2) | async-done | bytes 786464 | tf_op jit(solution)/shard_map/all_to_all | solution.py:35
  64.4 0.0 copy-done
  64.4 0.0 copy-done.1
  64.4 1.7 %experts.1 = bf16[8,4,48,256]{3,2,1,0:T(8,128)(2,1)S(1)} custom-call(bf16[8,4,48,256]{3,2,1,0:T(8,128)(2,1)S(1)} %bitcast.34, bf16[96,3072]{1,0:T(8,128)(2,1)S(1)} %pad_maximum_fusion.units_ref, bf16[352,1024]{1,0:T(8,128)(2,1)S(1)} %bitcast.36, bf16[352,1024]{1,0:T(8,128)(2,1)S(1)} %bitcast.37, ...), custom_call_target="tpu_custom_call", output_to_operand_aliasing={{}: (0, {})} | custom-call | tf_op jit(solution)/shard_map/experts/pallas_call | solution.py:264
  66.0 0.0 copy-start.10
  66.1 18.4 %all_to_all.32.returned_ref = bf16[32,48,256]{2,1,0:T(8,128)(2,1)S(1)} all-to-all(bf16[32,48,256]{2,1,0:T(8,128)(2,1)S(1)} %bitcast.35), channel_id=1, replica_groups=mesh['z'=16,'x'=4,'c'=2,'tp'=4] {'x','c','tp'}, dimensions={0} | all-to-all | bytes 1572864 | tf_op jit(solution)/shard_map/all_to_all | solution.py:35
  84.4 0.3 gather_back.1
  84.7 15.8 %all_to_all.33 = bf16[16,8,256]{2,1,0:T(8,128)(2,1)S(1)} all-to-all(bf16[16,8,256]{2,1,0:T(8,128)(2,1)S(1)} %gather_back.1), channel_id=1, replica_groups=mesh['z'=16,'x'=4,'c'=2,'tp'=4] {'z'}, dimensions={0} | all-to-all | bytes 131072 | tf_op jit(solution)/shard_map/all_to_all | solution.py:35
  100.5 0.4 fusion.1
  100.9 0.1 pad_maximum_fusion.2
  101.0 7.7 %all_to_all.34 = f32[4,1,32]{2,1,0:T(1,128)S(1)} all-to-all(f32[4,1,32]{2,1,0:T(1,128)S(1)} %broadcast_in_dim.26), channel_id=1, replica_groups=mesh['z'=16,'x'=4,'c'=2,'tp'=4] {'tp'}, dimensions={0} | all-to-all | bytes 1024 | tf_op jit(solution)/shard_map/all_to_all | solution.py:27
  108.7 0.1 slice_multiply_fusion
  108.7 0.0 copy-done.10
  108.7 0.7 multiply_convert_fusion
  (11 shorter events, 0.1 us)
Async XLA Ops:
  0.0 14.0 %copy-start.9 = (bf16[1024]{0:T(1024)(128)(2,1)S(1)}, bf16[1024]{0:T(1024)(128)(2,1)}, u32[]{:S(2)}) copy-start(bf16[1024]{0:T(1024)(128)(2,1)} %param.45) | copy-start | bytes 6148
  0.0 14.0 %copy-start.2 = (bf16[16,1024]{1,0:T(8,128)(2,1)S(1)}, bf16[16,1024]{1,0:T(8,128)(2,1)}, u32[]{:S(2)}) copy-start(bf16[16,1024]{1,0:T(8,128)(2,1)} %tokens_ref.1) | copy-start | bytes 98308
  0.0 14.0 %copy-start.4 = (f32[1024]{0:T(1024)S(1)}, f32[1024]{0:T(1024)}, u32[]{:S(2)}) copy-start(f32[1024]{0:T(1024)} %param.38) | copy-start | bytes 12292
  0.0 14.0 %copy-start.5 = (s32[16,2]{0,1:T(2,128)S(1)}, s32[16,2]{0,1:T(2,128)}, u32[]{:S(2)}) copy-start(s32[16,2]{0,1:T(2,128)} %param.47) | copy-start | bytes 388
  0.0 14.0 %copy-start.6 = (f32[16,2]{0,1:T(2,128)S(1)}, f32[16,2]{0,1:T(2,128)}, u32[]{:S(2)}) copy-start(f32[16,2]{0,1:T(2,128)} %param.48) | copy-start | bytes 388
  0.0 30.2 %copy-start.7 = (bf16[22,1024]{1,0:T(8,128)(2,1)S(1)}, bf16[22,1024]{1,0:T(8,128)(2,1)}, u32[]{:S(2)}) copy-start(bf16[22,1024]{1,0:T(8,128)(2,1)} %param.42) | copy-start | bytes 135172
  0.0 30.2 %copy-start.8 = (bf16[22,1024]{1,0:T(8,128)(2,1)S(1)}, bf16[22,1024]{1,0:T(8,128)(2,1)}, u32[]{:S(2)}) copy-start(bf16[22,1024]{1,0:T(8,128)(2,1)} %param.43) | copy-start | bytes 135172
  0.0 44.8 %copy-start.3 = (bf16[384,128]{1,0:T(8,128)(2,1)S(1)}, bf16[384,128]{1,0:T(8,128)(2,1)}, u32[]{:S(2)}) copy-start(bf16[384,128]{1,0:T(8,128)(2,1)} %constant.15.clone.choice_ref) | copy-start | bytes 294916
  15.0 29.8 %all-to-all-start.1 = ((bf16[16,8,256]{2,1,0:T(8,128)(2,1)}), bf16[16,8,256]{2,1,0:T(8,128)(2,1)S(1)}, u32[]{:S(2)}, u32[]{:S(2)}) async-start(bf16[16,8,256]{2,1,0:T(8,128)(2,1)} %bitcast.8), calls=%async_computation.1 | async-start | bytes 131072 | tf_op jit(solution)/shard_map/all_to_all | solution.py:35
  30.3 21.3 %collective-permute-start = (bf16[24,3072]{1,0:T(8,128)(2,1)S(1)}, bf16[24,3072]{1,0:T(8,128)(2,1)S(1)}, u32[]{:S(2)}, u32[]{:S(2)}) collective-permute-start(bf16[24,3072]{1,0:T(8,128)(2,1)S(1)} %constant_dynamic-update-slice_fusion), channel_id=1, source_target_pairs={{0,64},{32,96},{64,0},{96,32},{128,192},{160,224},{192,128},{224,1... | collective-permute-start | bytes 442376 | tf_op jit(solution)/shard_map/ppermute | solution.py:53
  46.0 18.4 %all-to-all-start.2 = ((bf16[32,48,256]{2,1,0:T(8,128)(2,1)}), bf16[32,48,256]{2,1,0:T(8,128)(2,1)S(1)}, u32[]{:S(2)}, u32[]{:S(2)}) async-start(bf16[32,48,256]{2,1,0:T(8,128)(2,1)} %bitcast.41), calls=%async_computation.2 | async-start | bytes 1572864 | tf_op jit(solution)/shard_map/all_to_all | solution.py:35
  51.6 12.8 %copy-start = (bf16[1,1024,352]{1,2,0:T(8,128)(2,1)S(1)}, bf16[1,1024,352]{1,2,0:T(8,128)(2,1)}, u32[]{:S(2)}) copy-start(bf16[1,1024,352]{1,2,0:T(8,128)(2,1)} %param.39) | copy-start | bytes 2162692
  51.6 12.8 %copy-start.1 = (bf16[1,1024,352]{1,2,0:T(8,128)(2,1)S(1)}, bf16[1,1024,352]{1,2,0:T(8,128)(2,1)}, u32[]{:S(2)}) copy-start(bf16[1,1024,352]{1,2,0:T(8,128)(2,1)} %param.40) | copy-start | bytes 2162692
  51.7 11.1 %collective-permute-start.1 = (bf16[48,3072]{1,0:T(8,128)(2,1)S(1)}, bf16[48,3072]{1,0:T(8,128)(2,1)S(1)}, u32[]{:S(2)}, u32[]{:S(2)}) collective-permute-start(bf16[48,3072]{1,0:T(8,128)(2,1)S(1)} %pad_maximum_fusion.1), channel_id=1, source_target_pairs={{0,32},{32,0},{64,96},{96,64},{128,160},{160,128},{192,224},{224,1... | collective-permute-start | bytes 884744 | tf_op jit(solution)/shard_map/ppermute | solution.py:53
  66.0 42.7 %copy-start.10 = (f32[256]{0:T(256)S(1)}, f32[256]{0:T(256)}, u32[]{:S(2)}) copy-start(f32[256]{0:T(256)} %param.46) | copy-start | bytes 3076

commit v7 on v6

--- a/solution.py
+++ b/solution.py
@@ -59,7 +59,7 @@
     sources, message_ref = refs[:count], refs[count]
     targets = refs[count + 1 : count + 1 + len(groups)]
     query_ref, answer_ref, arrival = refs[count + 1 + len(groups) :]
-    tokens_ref, low_ref, up_ref, base_ref, w_ref, state_ref, gain_ref, w_out_ref, down_ref = targets
+    tokens_ref, low_ref, up_ref, base_ref, w_ref, state_ref, w_out_ref, down_ref = targets
     at = 0
     for group, (target, members) in enumerate(zip(targets, groups)):
         for i in range(members):
@@ -146,7 +146,7 @@
     read_out = picked(0) - picked(1) * removed_factor + value_vecs * value_factor
     centred = read_out - over_head(read_out) * (1.0 / head_size)
     spread = over_head(centred * centred) * (1.0 / head_size)
-    normed = centred * lax.rsqrt(spread + head_epsilon) * landed(gain_ref)[...]
+    normed = centred * lax.rsqrt(spread + head_epsilon) * base_ref[2]
     mixed = jnp.dot(normed.astype(jnp.bfloat16), landed(w_out_ref)[...], preferred_element_type=f32)
     mixed = mixed.astype(jnp.bfloat16)
     copies_out, mix_rows = message_ref.shape[0], row_count * heads
@@ -183,10 +183,9 @@
         [tokens],
         [decay_down.T, rate_down.T],
         [decay_up, rate_up],
-        [decay_base[None], rate_base[None]],
+        [decay_base[None], rate_base[None], head_gain[None]],
         [w_key, w_recep, w_value],
         [state],
-        [head_gain[None]],
         [w_out],
         [own_down],
     ]
@@ -402,7 +401,6 @@
     planes, slots_part, quarter = arrived_ref.shape
     here, copies, splits, height, _ = out_any.shape
     arrived = arrived_ref[...].reshape(planes * slots_part, quarter)
-    started = []
     for e in range(here):
         size = splits * height
         laid = jnp.dot(
@@ -410,10 +408,8 @@
         ).astype(jnp.bfloat16)
         for c in range(copies):
             laid_ref[e, c] = laid.reshape(splits, height, quarter)
-        started.append(pltpu.make_async_copy(laid_ref.at[e], out_any.at[e], sent.at[e]))
-        started[e].start()
-    for copy in started:
-        copy.wait()
+        pltpu.make_async_copy(laid_ref.at[e], out_any.at[e], sent.at[0]).start()
+    pltpu.make_async_copy(laid_ref, out_any, sent.at[0]).wait()
 
 
 def fan_out(arrived, capacity, here, copies, splits, shared):
@@ -427,7 +423,7 @@
         out_shape=jax.ShapeDtypeStruct(shape, jnp.bfloat16),
         in_specs=[vmem, vmem],
         out_specs=pl.BlockSpec(memory_space=pl.ANY),
-        scratch_shapes=[pltpu.VMEM(shape, jnp.bfloat16), pltpu.SemaphoreType.DMA((here,))],
+        scratch_shapes=[pltpu.VMEM(shape, jnp.bfloat16), pltpu.SemaphoreType.DMA((1,))],
         name="fan_out",
     )(on_chip(arrived), on_chip(jnp.asarray(choice, jnp.bfloat16)))
 

time: 110 us -> 110 us (level)
  no operation moved by 1% of the time
where the time goes in v7:
time: 110 us; the launch traced here: 109 us
  blocking collectives  52.4 us (48%)
  starting transfers between devices  27.6 us (25%)
  waiting for transfers between devices  20.4 us (19%)
  Pallas kernels  7.41 us (7%)
    all_to_all x3, blocking collectives, exchange(): return lax.all_to_all(parts, axis, split_axis=0, concat_axis=0, tiled=True)  44.7 us
    all_to_all x2, starting transfers between devices, exchange(): return lax.all_to_all(parts, axis, split_axis=0, concat_axis=0, tiled=True)  20.8 us
    all_to_all x2, waiting for transfers between devices, exchange(): return lax.all_to_all(parts, axis, split_axis=0, concat_axis=0, tiled=True)  11.4 us
    ppermute x2, waiting for transfers between devices, with_neighbour(): other = lax.ppermute(units, 'z', [(i, i ^ step) for i in range(planes)])  9 us
    all_to_all x1, blocking collectives, sent_to_all(): return lax.all_to_all(copies, axis, split_axis=0, concat_axis=0, tiled=True)  7.66 us
    ppermute x2, starting transfers between devices, with_neighbour(): other = lax.ppermute(units, 'z', [(i, i ^ step) for i in range(planes)])  6.78 us
    pallas_call x1, Pallas kernels, mixer_message(): pl.pallas_call(partial(mixer_kernel, groups=[len(group) for group in far]...  3.41 us
  transfers between devices with their start and end apart: 4, of which 3 were waited for; matrix products, arithmetic and copies ran while one was open for 0% of the time, Pallas kernels for 1%

profile of v7, /device:TPU:2, one launch (start us, length us, event | category | flops | bytes accessed | tf_op | source)
XLA Modules:
  0.0 109.4 jit_solution(131468522777742350)
XLA Ops:
  0.0 0.0 copy-start.9
  0.0 0.0 copy-start.2
  0.0 0.0 copy-start.4
  0.0 0.0 copy-start.5
  0.0 0.0 copy-start.6
  0.0 0.0 copy-start.7
  0.0 0.0 copy-start.8
  0.0 0.0 copy-start.3
  0.1 3.4 %mixer.1 = bf16[4,88,256]{2,1,0:T(8,128)(2,1)S(1)} custom-call(bf16[16,1024]{1,0:T(8,128)(2,1)} %tokens_ref.1, bf16[64,1024]{1,0:T(8,128)(2,1)} %bitcast.43, bf16[64,1024]{1,0:T(8,128)(2,1)} %bitcast.44, bf16[64,256]{1,0:T(8,128)(2,1)} %refs_3_.1, bf16[64,256]{1,0:T(8,128)(2,1)} %refs_4_.1, f32[1,256]{1,0:T(1,128)} %bitcast.46, f32[1,256]{1,0:T(1,128)} %bitcast.47, ...), custom_call_target="tpu_custom_call" | custom-call | tf_op jit(solution)/shard_map/mixer/pallas_call | solution.py:194
  3.5 10.5 %all_to_all.31.everyone_ref = bf16[4,88,256]{2,1,0:T(8,128)(2,1)S(1)} all-to-all(bf16[4,88,256]{2,1,0:T(8,128)(2,1)S(1)} %mixer.1), channel_id=1, replica_groups=mesh['z'=16,'x'=4,'c'=2,'tp'=4] {'tp'}, dimensions={0} | all-to-all | bytes 360448 | tf_op jit(solution)/shard_map/all_to_all | solution.py:35
  14.0 0.0 copy-done.9
  14.0 0.0 copy-done.2
  14.0 0.0 copy-done.4
  14.0 0.0 copy-done.5
  14.0 0.0 copy-done.6
  14.0 1.0 norm_and_pack.1
  15.0 15.2 %all-to-all-start.1 = ((bf16[16,8,256]{2,1,0:T(8,128)(2,1)}), bf16[16,8,256]{2,1,0:T(8,128)(2,1)S(1)}, u32[]{:S(2)}, u32[]{:S(2)}) async-start(bf16[16,8,256]{2,1,0:T(8,128)(2,1)} %bitcast.8), calls=%async_computation.1 | async-start | bytes 131072 | tf_op jit(solution)/shard_map/all_to_all | solution.py:35
  30.2 0.0 copy-done.7
  30.2 0.0 copy-done.8
  30.3 4.7 %collective-permute-start = (bf16[24,3072]{1,0:T(8,128)(2,1)S(1)}, bf16[24,3072]{1,0:T(8,128)(2,1)S(1)}, u32[]{:S(2)}, u32[]{:S(2)}) collective-permute-start(bf16[24,3072]{1,0:T(8,128)(2,1)S(1)} %constant_dynamic-update-slice_fusion), channel_id=1, source_target_pairs={{0,64},{32,96},{64,0},{96,32},{128,192},{160,224},{192,128},{224,1... | collective-permute-start | bytes 442376 | tf_op jit(solution)/shard_map/ppermute | solution.py:53
  35.1 9.8 %all-to-all-done.1.arrived_ref = bf16[16,8,256]{2,1,0:T(8,128)(2,1)S(1)} async-done(((bf16[16,8,256]{2,1,0:T(8,128)(2,1)}), bf16[16,8,256]{2,1,0:T(8,128)(2,1)S(1)}, u32[]{:S(2)}, u32[]{:S(2)}) %all-to-all-start.1) | async-done | bytes 65568 | tf_op jit(solution)/shard_map/all_to_all | solution.py:35
  44.9 0.0 copy-done.3
  44.9 1.1 fan_out.1
  46.0 5.6 %all-to-all-start.2 = ((bf16[32,48,256]{2,1,0:T(8,128)(2,1)}), bf16[32,48,256]{2,1,0:T(8,128)(2,1)S(1)}, u32[]{:S(2)}, u32[]{:S(2)}) async-start(bf16[32,48,256]{2,1,0:T(8,128)(2,1)} %bitcast.41), calls=%async_computation.2 | async-start | bytes 1572864 | tf_op jit(solution)/shard_map/all_to_all | solution.py:35
  51.6 0.0 copy-start
  51.6 0.0 copy-start.1
  51.6 0.0 collective-permute-done
  51.6 2.1 %collective-permute-start.1 = (bf16[48,3072]{1,0:T(8,128)(2,1)S(1)}, bf16[48,3072]{1,0:T(8,128)(2,1)S(1)}, u32[]{:S(2)}, u32[]{:S(2)}) collective-permute-start(bf16[48,3072]{1,0:T(8,128)(2,1)S(1)} %pad_maximum_fusion.1), channel_id=1, source_target_pairs={{0,32},{32,0},{64,96},{96,64},{128,160},{160,128},{192,224},{224,1... | collective-permute-start | bytes 884744 | tf_op jit(solution)/shard_map/ppermute | solution.py:53
  53.7 9.0 %collective-permute-done.1 = bf16[48,3072]{1,0:T(8,128)(2,1)S(1)} collective-permute-done((bf16[48,3072]{1,0:T(8,128)(2,1)S(1)}, bf16[48,3072]{1,0:T(8,128)(2,1)S(1)}, u32[]{:S(2)}, u32[]{:S(2)}) %collective-permute-start.1) | collective-permute-done | bytes 294944 | tf_op jit(solution)/shard_map/ppermute | solution.py:53
  62.7 1.6 %all-to-all-done.2 = bf16[32,48,256]{2,1,0:T(8,128)(2,1)S(1)} async-done(((bf16[32,48,256]{2,1,0:T(8,128)(2,1)}), bf16[32,48,256]{2,1,0:T(8,128)(2,1)S(1)}, u32[]{:S(2)}, u32[]{:S(2)}) %all-to-all-start.2) | async-done | bytes 786464 | tf_op jit(solution)/shard_map/all_to_all | solution.py:35
  64.3 0.0 copy-done
  64.3 0.0 copy-done.1
  64.4 1.7 %experts.1 = bf16[8,4,48,256]{3,2,1,0:T(8,128)(2,1)S(1)} custom-call(bf16[8,4,48,256]{3,2,1,0:T(8,128)(2,1)S(1)} %bitcast.34, bf16[96,3072]{1,0:T(8,128)(2,1)S(1)} %pad_maximum_fusion.units_ref, bf16[352,1024]{1,0:T(8,128)(2,1)S(1)} %bitcast.36, bf16[352,1024]{1,0:T(8,128)(2,1)S(1)} %bitcast.37, ...), custom_call_target="tpu_custom_call", output_to_operand_aliasing={{}: (0, {})} | custom-call | tf_op jit(solution)/shard_map/experts/pallas_call | solution.py:263
  66.0 0.0 copy-start.10
  66.0 18.4 %all_to_all.32.returned_ref = bf16[32,48,256]{2,1,0:T(8,128)(2,1)S(1)} all-to-all(bf16[32,48,256]{2,1,0:T(8,128)(2,1)S(1)} %bitcast.35), channel_id=1, replica_groups=mesh['z'=16,'x'=4,'c'=2,'tp'=4] {'x','c','tp'}, dimensions={0} | all-to-all | bytes 1572864 | tf_op jit(solution)/shard_map/all_to_all | solution.py:35
  84.4 0.3 gather_back.1
  84.7 15.8 %all_to_all.33 = bf16[16,8,256]{2,1,0:T(8,128)(2,1)S(1)} all-to-all(bf16[16,8,256]{2,1,0:T(8,128)(2,1)S(1)} %gather_back.1), channel_id=1, replica_groups=mesh['z'=16,'x'=4,'c'=2,'tp'=4] {'z'}, dimensions={0} | all-to-all | bytes 131072 | tf_op jit(solution)/shard_map/all_to_all | solution.py:35
  100.5 0.4 fusion.1
  100.9 0.1 pad_maximum_fusion.2
  101.0 7.7 %all_to_all.34 = f32[4,1,32]{2,1,0:T(1,128)S(1)} all-to-all(f32[4,1,32]{2,1,0:T(1,128)S(1)} %broadcast_in_dim.26), channel_id=1, replica_groups=mesh['z'=16,'x'=4,'c'=2,'tp'=4] {'tp'}, dimensions={0} | all-to-all | bytes 1024 | tf_op jit(solution)/shard_map/all_to_all | solution.py:27
  108.7 0.1 slice_multiply_fusion
  108.7 0.0 copy-done.10
  108.7 0.7 multiply_convert_fusion
  (11 shorter events, 0.1 us)
Async XLA Ops:
  0.0 14.0 %copy-start.9 = (bf16[1024]{0:T(1024)(128)(2,1)S(1)}, bf16[1024]{0:T(1024)(128)(2,1)}, u32[]{:S(2)}) copy-start(bf16[1024]{0:T(1024)(128)(2,1)} %param.45) | copy-start | bytes 6148
  0.0 14.0 %copy-start.2 = (bf16[16,1024]{1,0:T(8,128)(2,1)S(1)}, bf16[16,1024]{1,0:T(8,128)(2,1)}, u32[]{:S(2)}) copy-start(bf16[16,1024]{1,0:T(8,128)(2,1)} %tokens_ref.1) | copy-start | bytes 98308
  0.0 14.0 %copy-start.4 = (f32[1024]{0:T(1024)S(1)}, f32[1024]{0:T(1024)}, u32[]{:S(2)}) copy-start(f32[1024]{0:T(1024)} %param.38) | copy-start | bytes 12292
  0.0 14.0 %copy-start.5 = (s32[16,2]{0,1:T(2,128)S(1)}, s32[16,2]{0,1:T(2,128)}, u32[]{:S(2)}) copy-start(s32[16,2]{0,1:T(2,128)} %param.47) | copy-start | bytes 388
  0.0 14.0 %copy-start.6 = (f32[16,2]{0,1:T(2,128)S(1)}, f32[16,2]{0,1:T(2,128)}, u32[]{:S(2)}) copy-start(f32[16,2]{0,1:T(2,128)} %param.48) | copy-start | bytes 388
  0.0 30.2 %copy-start.7 = (bf16[22,1024]{1,0:T(8,128)(2,1)S(1)}, bf16[22,1024]{1,0:T(8,128)(2,1)}, u32[]{:S(2)}) copy-start(bf16[22,1024]{1,0:T(8,128)(2,1)} %param.42) | copy-start | bytes 135172
  0.0 30.2 %copy-start.8 = (bf16[22,1024]{1,0:T(8,128)(2,1)S(1)}, bf16[22,1024]{1,0:T(8,128)(2,1)}, u32[]{:S(2)}) copy-start(bf16[22,1024]{1,0:T(8,128)(2,1)} %param.43) | copy-start | bytes 135172
  0.0 44.8 %copy-start.3 = (bf16[384,128]{1,0:T(8,128)(2,1)S(1)}, bf16[384,128]{1,0:T(8,128)(2,1)}, u32[]{:S(2)}) copy-start(bf16[384,128]{1,0:T(8,128)(2,1)} %constant.15.clone.choice_ref) | copy-start | bytes 294916
  15.0 29.8 %all-to-all-start.1 = ((bf16[16,8,256]{2,1,0:T(8,128)(2,1)}), bf16[16,8,256]{2,1,0:T(8,128)(2,1)S(1)}, u32[]{:S(2)}, u32[]{:S(2)}) async-start(bf16[16,8,256]{2,1,0:T(8,128)(2,1)} %bitcast.8), calls=%async_computation.1 | async-start | bytes 131072 | tf_op jit(solution)/shard_map/all_to_all | solution.py:35
  30.3 21.3 %collective-permute-start = (bf16[24,3072]{1,0:T(8,128)(2,1)S(1)}, bf16[24,3072]{1,0:T(8,128)(2,1)S(1)}, u32[]{:S(2)}, u32[]{:S(2)}) collective-permute-start(bf16[24,3072]{1,0:T(8,128)(2,1)S(1)} %constant_dynamic-update-slice_fusion), channel_id=1, source_target_pairs={{0,64},{32,96},{64,0},{96,32},{128,192},{160,224},{192,128},{224,1... | collective-permute-start | bytes 442376 | tf_op jit(solution)/shard_map/ppermute | solution.py:53
  46.0 18.4 %all-to-all-start.2 = ((bf16[32,48,256]{2,1,0:T(8,128)(2,1)}), bf16[32,48,256]{2,1,0:T(8,128)(2,1)S(1)}, u32[]{:S(2)}, u32[]{:S(2)}) async-start(bf16[32,48,256]{2,1,0:T(8,128)(2,1)} %bitcast.41), calls=%async_computation.2 | async-start | bytes 1572864 | tf_op jit(solution)/shard_map/all_to_all | solution.py:35
  51.6 12.8 %copy-start = (bf16[1,1024,352]{1,2,0:T(8,128)(2,1)S(1)}, bf16[1,1024,352]{1,2,0:T(8,128)(2,1)}, u32[]{:S(2)}) copy-start(bf16[1,1024,352]{1,2,0:T(8,128)(2,1)} %param.39) | copy-start | bytes 2162692
  51.6 12.8 %copy-start.1 = (bf16[1,1024,352]{1,2,0:T(8,128)(2,1)S(1)}, bf16[1,1024,352]{1,2,0:T(8,128)(2,1)}, u32[]{:S(2)}) copy-start(bf16[1,1024,352]{1,2,0:T(8,128)(2,1)} %param.40) | copy-start | bytes 2162692
  51.6 11.1 %collective-permute-start.1 = (bf16[48,3072]{1,0:T(8,128)(2,1)S(1)}, bf16[48,3072]{1,0:T(8,128)(2,1)S(1)}, u32[]{:S(2)}, u32[]{:S(2)}) collective-permute-start(bf16[48,3072]{1,0:T(8,128)(2,1)S(1)} %pad_maximum_fusion.1), channel_id=1, source_target_pairs={{0,32},{32,0},{64,96},{96,64},{128,160},{160,128},{192,224},{224,1... | collective-permute-start | bytes 884744 | tf_op jit(solution)/shard_map/ppermute | solution.py:53
  66.0 42.7 %copy-start.10 = (f32[256]{0:T(256)S(1)}, f32[256]{0:T(256)}, u32[]{:S(2)}) copy-start(f32[256]{0:T(256)} %param.46) | copy-start | bytes 3076
